TPU v7x, 128 devices: a whole 4x4x4 slice. The times are simulated.
128 devices in a mesh: kv: 16 (over z, y), tp: 8 (over x, core).
Axes of the slice: x: 4, y: 4, z: 4, core: 2. Of those that a mesh axis runs over, the one named last changes fastest.
Arguments:
- tokens: bfloat16 [512, 4096], P(None, ('kv', 'tp')), may hold values from -60 to 60
- past_state: float32 [512, 16, 128, 128], P('kv', 'tp'), may hold values from -4 to 4
- pre_gain: float32 [4096], replicated, may hold values from 0.1 to 1.9
- pre_gate: bfloat16 [4096, 11264], P(None, ('kv', 'tp')), may hold values from -0.09375 to 0.09375
- pre_up: bfloat16 [4096, 11264], P(None, ('kv', 'tp')), may hold values from -0.09375 to 0.09375
- pre_down: bfloat16 [11264, 4096], P(('kv', 'tp')), may hold values from -0.21875 to 0.21875
- mix_gain: float32 [4096], replicated, may hold values from 0.1 to 1.9
- query_weight: bfloat16 [4096, 2048], P('kv', 'tp'), may hold values from -0.09375 to 0.09375
- forget_weight: bfloat16 [4096, 2048], P('kv', 'tp'), may hold values from -0.09375 to 0.09375
- value_weight: bfloat16 [4096, 2048], P('kv', 'tp'), may hold values from -0.09375 to 0.09375
- output_gate_weight: bfloat16 [4096, 2048], P('kv', 'tp'), may hold values from -0.09375 to 0.09375
- forget_floor: float32 [2048], P('tp'), may hold values from 0.02 to 0.9
- head_gain: float32 [128], replicated, may hold values from 0.1 to 1.9
- proj_out: bfloat16 [2048, 4096], P('tp', 'kv'), may hold values from -0.125 to 0.125
- post_gain: float32 [4096], replicated, may hold values from 0.1 to 1.9
- post_gate: bfloat16 [4096, 11264], P(None, ('kv', 'tp')), may hold values from -0.09375 to 0.09375
- post_up: bfloat16 [4096, 11264], P(None, ('kv', 'tp')), may hold values from -0.09375 to 0.09375
- post_down: bfloat16 [11264, 4096], P(('kv', 'tp')), may hold values from -0.21875 to 0.21875
Outputs:
- result: bfloat16 [512, 4096], P(None, ('kv', 'tp'))
- new_state: float32 [512, 16, 128, 128], P('kv', 'tp')
All inputs are finite; a program needn't handle non-finite values.
Results may differ from a plain program's by a relative error of at most 0.014.
Values may be sent and summed in bfloat16 or wider, within the bound.
No kernel may reach another device: no remote copies, remote signals or barrier semaphores. Data moves between devices by JAX's collectives and lax.ppermute only.
A program may use at most 128 MiB of HBM per device.

v0:
```python
import functools

import jax
import jax.numpy as jnp
from jax import lax
from jax.experimental import pallas as pl
from jax.experimental.pallas import tpu as pltpu
from jax.sharding import Mesh
from jax.sharding import PartitionSpec as P


D = 4096
ALL = ("z", "y", "x", "c")
KV = ("z", "y")
TP = ("x", "c")
epsilon = 1e-06
f32 = jnp.float32
bf16 = jnp.bfloat16


def copy_for_each(value, axes):
    copies = jnp.broadcast_to(value, (lax.axis_size(axes), *value.shape))
    return lax.all_to_all(copies, axes, split_axis=0, concat_axis=0, tiled=True)


def exchange(pieces, axes):
    return lax.all_to_all(pieces, axes, split_axis=0, concat_axis=0, tiled=True)


def other_core(value):
    return lax.ppermute(value, "c", [(0, 1), (1, 0)])


def device(z, y, x, c):
    return ((z % 4 * 4 + y % 4) * 4 + x % 4) * 2 + c


PLACES = [(z, y, x, c) for z in range(4) for y in range(4) for x in range(4) for c in range(2)]
PLANES = [[device(z, m, x, 0) for z in range(4) for m in range(4)] for x in range(4)] + [
    [device(z, y, m, 1) for z in range(4) for m in range(4)] for y in range(4)
]


def shift(value, steps):
    pairs = [
        (device(z, y, x, c), device(z, y, x + steps, c) if c == 0 else device(z, y + steps, x, c))
        for z, y, x, c in PLACES
    ]
    return lax.ppermute(value, ALL, pairs)


def shift_x(value, steps):
    pairs = [(device(z, y, x, c), device(z, y, x + steps, c)) for z, y, x, c in PLACES]
    return lax.ppermute(value, ALL, pairs)


def plane_exchange(pieces):
    return lax.all_to_all(
        pieces, ALL, split_axis=0, concat_axis=0, axis_index_groups=PLANES, tiled=True
    )


PAD = 96


def in_hbm(value):
    return pltpu.with_memory_space_constraint(value, pltpu.HBM)


def sources(core):
    out = lax.broadcasted_iota(jnp.int32, (1, 512), 1)
    chunk, place, column = out // 128, out // 32 % 4, out % 32
    far_x = (lax.axis_index("x") + chunk) % 4
    far_y = (lax.axis_index("y") + chunk) % 4
    return column + jnp.where(
        core == 0, place * 256 + far_x * 64, far_y * 256 + place * 64 + 32
    )


def order_body(mine, theirs, gain, gate, up, down, near, far, gains, rows, picks):
    units = gate.shape[0]

    @pl.when(pl.program_id(0) == 0)
    def _():
        rows[...] = jnp.zeros_like(rows)
        place = lax.broadcasted_iota(jnp.int32, (1024, 512), 0)
        picks[0] = (place == mine[...]).astype(bf16)
        picks[1] = (place == theirs[...]).astype(bf16)

    for j, weight in enumerate((gate, up, down)):
        rows[PAD * j : PAD * j + units, :] = weight[...]
    rest, row = gain[0], lax.broadcasted_iota(jnp.int32, (16, gain.shape[2]), 0)
    split = jnp.zeros(row.shape, f32)
    for i in range(3):
        part = rest.astype(bf16).astype(f32)
        rest = rest - part
        split = jnp.where(row == i, part, split)
    rows[3 * PAD :, :] = split.astype(bf16)
    mine = jnp.dot(rows[...], picks[0], preferred_element_type=f32)
    theirs = jnp.dot(rows[: 3 * PAD, :], picks[1], preferred_element_type=f32)
    for chosen, out in ((mine, near), (theirs, far)):
        chosen = chosen[: 3 * PAD].astype(bf16)
        for k in range(4):
            for j in range(3):
                out[k, j] = chosen[PAD * j : PAD * (j + 1), 128 * k : 128 * (k + 1)]
    line = jnp.sum(mine[3 * PAD : 3 * PAD + 8], axis=0, keepdims=True)
    line = jnp.broadcast_to(line, (128, line.shape[1]))
    for k in range(4):
        gains[k] = line[:, 128 * k : 128 * (k + 1)].T


def order_weights(gain, gate, up, down):
    core = lax.axis_index("c")
    units = gate.shape[0]
    whole = pl.BlockSpec((1, 512), lambda z: (0, 0))
    piece = pl.BlockSpec((units, 1024), lambda z: (0, z))
    side = pl.BlockSpec((4, 3, PAD, 128), lambda z: (0, 0, 0, z))
    shape = jax.ShapeDtypeStruct((4, 3, PAD, 512), bf16)
    return pl.pallas_call(
        order_body,
        grid=(4,),
        in_specs=[
            whole,
            whole,
            pl.BlockSpec((1, 1, 1024), lambda z: (z, 0, 0)),
            piece,
            piece,
            piece,
        ],
        out_specs=[side, side, pl.BlockSpec((4, 128, 128), lambda z: (0, z, 0))],
        out_shape=[shape, shape, jax.ShapeDtypeStruct((4, 512, 128), f32)],
        scratch_shapes=[pltpu.VMEM((3 * PAD + 16, 1024), bf16), pltpu.VMEM((2, 1024, 512), bf16)],
        cost_estimate=pl.CostEstimate(flops=5 * 10**9, bytes_accessed=6 * 10**6, transcendentals=0),
        compiler_params=pltpu.CompilerParams(vmem_limit_bytes=20 * 2**20),
        name="order",
    )(sources(core), sources(1 - core), gain.reshape(4, 1, 1024), *(in_hbm(w) for w in (gate, up, down)))


def product_body(*refs, parts, starts, more):
    chunks = len(starts)
    pieces, refs = refs[: len(parts)], refs[len(parts) :]
    nears, fars, gains = refs[:chunks], refs[chunks : 2 * chunks], refs[2 * chunks : 3 * chunks]
    before, out, away, normed = refs[3 * chunks :] if more else (None, refs[-2], None, refs[-1])
    squares = 0.0
    for piece, (chunk, first) in zip(pieces, parts, strict=True):
        count, rows = piece.shape
        value = piece[...].astype(f32)
        squares = squares + jnp.sum(value * value, axis=0, keepdims=True)
        gain = gains[chunk][0, first : first + count, :]
        gain = jnp.concatenate([gain] * (rows // 128), axis=1)
        normed[512 * chunk + first : 512 * chunk + first + count, :] = (value * gain).astype(bf16)
    for side, weights in enumerate((nears, fars)):
        weights = jnp.concatenate([w[0].reshape(2 * PAD, 512) for w in weights], axis=1)
        total = jnp.dot(weights, normed[...], preferred_element_type=f32)
        where = slice(2 * PAD * side, 2 * PAD * (side + 1))
        if more:
            total = before[where, :] + total
            away[where, :] = total.astype(bf16)
        out[where, :] = total
    squares = jnp.broadcast_to(squares, (8, squares.shape[1]))
    where = slice(4 * PAD, 4 * PAD + 8)
    if more:
        squares = before[where, :] + squares
        high = squares.astype(bf16).astype(f32)
        away[4 * PAD :, :] = jnp.concatenate([high, squares - high], axis=0).astype(bf16)
    out[where, :] = squares


def products(pieces, chunks, near, far, gains, before=None):
    rows = pieces[0][0].shape[1]
    parts = tuple((chunks.index(k), first) for _, k, first in pieces)
    operands = [p for p, _, _ in pieces]
    specs = [pl.BlockSpec(p.shape, lambda i: (0, 0)) for p in operands]
    for weights in (near, far):
        for k in chunks:
            operands.append(weights)
            specs.append(pl.BlockSpec((1, 2, PAD, 512), lambda i, k=k: (k, 0, 0, 0)))
    for k in chunks:
        operands.append(gains)
        specs.append(pl.BlockSpec((1, 512, 128), lambda i, k=k: (k, 0, 0)))
    outs = [jax.ShapeDtypeStruct((4 * PAD + 8, rows), f32)]
    if before is not None:
        operands.append(before)
        specs.append(pl.BlockSpec(before.shape, lambda i: (0, 0)))
        outs.append(jax.ShapeDtypeStruct((4 * PAD + 16, rows), bf16))
    return pl.pallas_call(
        functools.partial(product_body, parts=parts, starts=chunks, more=before is not None),
        grid=(1,),
        in_specs=specs,
        out_specs=[pl.BlockSpec(o.shape, lambda i: (0, 0)) for o in outs],
        out_shape=outs,
        scratch_shapes=[pltpu.VMEM((512 * len(chunks), rows), bf16)],
        cost_estimate=pl.CostEstimate(
            flops=len(chunks) * 4 * 10**8, bytes_accessed=len(chunks) * 10**6, transcendentals=0
        ),
        compiler_params=pltpu.CompilerParams(vmem_limit_bytes=16 * 2**20),
        name="products",
    )(*operands)


def readout_body(arrived, past, floor, gain, mixed, forget, value, query, gate, readout):
    step = pl.program_id(0)
    group, heads, width, _ = past.shape

    @pl.when(step == 0)
    def _():
        total = arrived[0].astype(f32)
        for i in range(1, arrived.shape[0]):
            total = total + arrived[i].astype(f32)
        inner = heads * width
        squares = total[:, 4 * inner : 4 * inner + 1] + total[:, 4 * inner + 64 : 4 * inner + 65]
        total = total[:, : 4 * inner] * lax.rsqrt(squares / D + epsilon)
        query[...] = jax.nn.silu(total[:, :inner])
        value[...] = total[:, 2 * inner : 3 * inner]
        gate[...] = jax.nn.silu(total[:, 3 * inner :])
        bound = floor[...]
        forget[...] = bound + (1.0 - bound) * jax.nn.sigmoid(total[:, inner : 2 * inner])

    here = pl.ds(pl.multiple_of(group * step, group), group)
    for h in range(heads):
        lanes = slice(width * h, width * (h + 1))
        keep, ask = forget[here, lanes], query[here, lanes]
        both = keep * ask
        high = both.astype(bf16).astype(f32)
        both = jnp.concatenate([high, both - high], axis=0).astype(bf16)
        sums = []
        for j in range(group):
            state = past[j, h]
            top = state.astype(bf16)
            low = (state - top.astype(f32)).astype(bf16)
            dots = jnp.dot(both, top, preferred_element_type=f32) + jnp.dot(
                both, low, preferred_element_type=f32
            )
            sums.append(dots[j : j + 1] + dots[group + j : group + j + 1])
        share = jnp.sum((1.0 - keep) * ask, axis=1, keepdims=True)
        readout[here, lanes] = jnp.concatenate(sums, axis=0) + share * value[here, lanes]

    @pl.when(step == pl.num_programs(0) - 1)
    def _():
        for h in range(heads):
            lanes = slice(width * h, width * (h + 1))
            r = readout[:, lanes]
            r = r * lax.rsqrt(jnp.mean(r * r, axis=1, keepdims=True) + epsilon) * gain[...]
            mixed[:, lanes] = (r * gate[:, lanes]).astype(bf16)


def read_out(arrived, past, floor, gain):
    count, heads, width, _ = past.shape
    inner, group = heads * width, 8
    rows = pltpu.VMEM((count, inner), f32)
    table = jax.ShapeDtypeStruct((count, inner), f32)
    whole = pl.BlockSpec((count, inner), lambda i: (0, 0))
    return pl.pallas_call(
        readout_body,
        grid=(count // group,),
        in_specs=[
            pl.BlockSpec(arrived.shape, lambda i: (0, 0, 0)),
            pl.BlockSpec((group, heads, width, width), lambda i: (i, 0, 0, 0)),
            pl.BlockSpec((1, inner), lambda i: (0, 0)),
            pl.BlockSpec((1, width), lambda i: (0, 0)),
        ],
        out_specs=[whole, whole, whole],
        out_shape=[jax.ShapeDtypeStruct((count, inner), bf16), table, table],
        scratch_shapes=[rows, rows, rows],
        compiler_params=pltpu.CompilerParams(vmem_limit_bytes=12 * 2**20),
        name="readout",
    )(arrived, in_hbm(past), floor.reshape(1, -1), gain.reshape(1, -1))


def state_body(forget, value, past, new, columns):
    step = pl.program_id(0)
    group, heads, width, _ = past.shape
    count = forget.shape[0]

    @pl.when(step == 0)
    def _():
        for h in range(heads):
            table = forget[:, width * h : width * (h + 1)]
            columns[h] = jnp.concatenate([table] * 4, axis=0).T

    here = pl.ds(pl.multiple_of(group * step, group), group)
    for h in range(heads):
        near = pltpu.roll(columns[h], lax.rem(4 * count - group * step, 4 * count), axis=1)
        values = value[here, width * h : width * (h + 1)]
        for j in range(group):
            keep = jnp.broadcast_to(near[:, j : j + 1], (width, width))
            added = values[j : j + 1, :]
            new[j, h] = added + keep * (past[j, h] - added)


def update_state(forget, value, past):
    count, heads, width, _ = past.shape
    group = 8
    block = pl.BlockSpec((group, heads, width, width), lambda i: (i, 0, 0, 0))
    whole = pl.BlockSpec(forget.shape, lambda i: (0, 0))
    return pl.pallas_call(
        state_body,
        grid=(count // group,),
        in_specs=[whole, whole, block],
        out_specs=block,
        out_shape=jax.ShapeDtypeStruct(past.shape, f32),
        scratch_shapes=[pltpu.VMEM((heads, width, 4 * count), f32)],
        compiler_params=pltpu.CompilerParams(vmem_limit_bytes=12 * 2**20),
        cost_estimate=pl.CostEstimate(
            flops=4 * 10**9, bytes_accessed=8 * 10**6, transcendentals=0
        ),
        name="state",
    )(forget, value, in_hbm(past))


def project_body(place, gain, *refs):
    pieces, weights, (out, block) = refs[:4], refs[4:-2], refs[-2:]
    width, rows = pieces[0].shape[0] // 2, pieces[0].shape[1]
    for k, piece in enumerate(pieces):
        first = lax.rem(place[0] + k, 4) * 2 * width
        for side in range(2):
            row = pl.multiple_of(first + lax.rem(place[1] + side, 2) * width, width)
            block[pl.ds(row, width), :] = piece[width * side : width * (side + 1), :]
    value = block[...].astype(f32)
    normed = (value * jnp.concatenate([gain[...]] * (rows // 128), axis=1)).astype(bf16)
    normed = normed.T
    count, own, _ = out.shape
    for i, w in enumerate(weights):
        part = jnp.dot(normed, w[...], preferred_element_type=f32).astype(bf16)
        out[:, :, 256 * i : 256 * (i + 1)] = part.reshape(count, own, 256)
    squares = jnp.sum(value * value, axis=0, keepdims=True)
    high = squares.astype(bf16).astype(f32)
    line = lax.broadcasted_iota(jnp.int32, (128, rows), 0)
    both = jnp.where(line < 64, high, squares - high).astype(bf16).T
    out[:, :, 1024:1152] = both.reshape(count, own, 128)


def in_smem():
    return pl.BlockSpec(memory_space=pltpu.SMEM)


def place_on_tp():
    return jnp.stack([lax.axis_index("x"), lax.axis_index("c")]).astype(jnp.int32)


def project(pieces, gain, weights, own_rows):
    rows, width = pieces[0].shape[1], gain.shape[0]
    operands = [jnp.broadcast_to(gain[:, None], (width, 128)), *pieces, *weights]
    return pl.pallas_call(
        project_body,
        in_specs=[in_smem()] + [pl.BlockSpec(v.shape, lambda: (0, 0)) for v in operands],
        out_shape=jax.ShapeDtypeStruct((rows // own_rows, own_rows, 4 * width + 128), bf16),
        scratch_shapes=[pltpu.VMEM((width, rows), bf16)],
        compiler_params=pltpu.CompilerParams(vmem_limit_bytes=14 * 2**20),
        name="project",
    )(place_on_tp(), *operands)


def output_body(place, gathered, weight, mine, theirs, block):
    width = mine.shape[1]
    block[...] = lax.dot_general(
        weight[...].T, gathered[...], (((1,), (1,)), ((), ())), preferred_element_type=f32
    )
    for k in range(4):
        first = lax.rem(place[0] + k, 4) * 2 * width
        for side, out in enumerate((mine, theirs)):
            row = pl.multiple_of(first + lax.rem(place[1] + side, 2) * width, width)
            out[k] = block[pl.ds(row, width), :].astype(bf16)


def project_out(gathered, weight):
    rows, width = gathered.shape[0], weight.shape[1]
    shape = jax.ShapeDtypeStruct((4, width // 8, rows), bf16)
    return pl.pallas_call(
        output_body,
        in_specs=[in_smem()] + [pl.BlockSpec(v.shape, lambda: (0, 0)) for v in (gathered, weight)],
        out_shape=[shape, shape],
        scratch_shapes=[pltpu.VMEM((width, rows), f32)],
        compiler_params=pltpu.CompilerParams(vmem_limit_bytes=10 * 2**20),
        name="output",
    )(place_on_tp(), gathered, weight)


def half_step(own, near_w, far_w, gains, near):
    width, rows = own.shape
    half = near.shape[0] // 2
    top, low = slice(0, half), slice(half, 2 * half)
    left_top = shift(near[top], 1)
    right_low = shift(near[low], -1)
    left_low = shift(near[low], 1)
    right_top = shift(near[top], -1)
    left_top, right_low, far_w = lax.optimization_barrier((left_top, right_low, far_w))
    far_top = shift(left_top, 1)
    far_low = shift(right_low, -1)
    early = [
        (near, 0, 0),
        (left_top, 3, 0),
        (right_low, 1, half),
        (left_low, 3, half),
        (right_top, 1, 0),
    ]
    (acc,) = products(early, [0, 3, 1], near_w, far_w, gains)
    late = [(far_top, 2, 0), (far_low, 2, half)]
    acc, away = products(late, [2], near_w, far_w, gains, acc)
    got = other_core(away).astype(f32)
    squares = acc[4 * PAD] + got[4 * PAD] + got[4 * PAD + 8]
    scale = lax.rsqrt(squares / D + epsilon)[None, :]
    own_acc = acc[: 2 * PAD] + got[2 * PAD : 4 * PAD]
    far_acc = acc[2 * PAD : 4 * PAD] + got[: 2 * PAD]
    hidden = jnp.concatenate(
        [
            (jax.nn.silu(scale * a[:PAD]) * (scale * a[PAD:])).astype(bf16)
            for a in (own_acc, far_acc)
        ],
        axis=0,
    )
    deep = jnp.concatenate([near_w[:, 2], far_w[:, 2]], axis=1)

    sums, arrived = {}, []
    for k in (2, 1, 3, 0):
        sums[k] = lax.dot_general(
            deep[k], hidden, (((0,), (0,)), ((), ())), preferred_element_type=f32
        ).astype(bf16)
        if k:
            arrived.append(shift(sums[k], k))
    total = sums[0].astype(f32)
    for piece in arrived:
        total = total + piece.astype(f32)
    total = total.astype(bf16)
    total = plane_exchange(total.reshape(16, width, rows)).astype(f32).sum(axis=0)
    return lax.optimization_barrier((own.astype(f32) + 0.5 * total).astype(bf16))


def plane_gather(own):
    return plane_exchange(jnp.broadcast_to(own, (16, *own.shape))).reshape(-1, own.shape[1])


def per_device(
    tokens,
    past_state,
    pre_gain,
    pre_gate,
    pre_up,
    pre_down,
    mix_gain,
    query_weight,
    forget_weight,
    value_weight,
    output_gate_weight,
    forget_floor,
    head_gain,
    proj_out,
    post_gain,
    post_gate,
    post_up,
    post_down,
):
    tokens = tokens.T
    near = plane_gather(tokens)
    near_w, far_w, gains = order_weights(pre_gain, pre_gate.T, pre_up.T, pre_down)
    near, near_w, far_w = lax.optimization_barrier((near, near_w, far_w))
    first = half_step(tokens, near_w, other_core(far_w), gains, near)

    width = mix_gain.shape[0] // lax.axis_size(KV)
    own_rows, _, _, _ = past_state.shape
    gains = lax.dynamic_slice_in_dim(mix_gain, lax.axis_index(KV) * width, width, 0)
    pair = jnp.concatenate([first, other_core(first)], axis=0)
    pieces = [pair] + [shift_x(pair, -k) for k in (1, 2, 3)]
    weight_list = (query_weight, forget_weight, value_weight, output_gate_weight)
    sent = project(pieces, gains, weight_list, own_rows)
    sent, post_gate, post_up, post_down = lax.optimization_barrier(
        (sent, post_gate, post_up, post_down)
    )
    near_w, far_w, gains = order_weights(post_gain, post_gate.T, post_up.T, post_down)
    arrived = exchange(sent, KV)
    arrived, near_w = lax.optimization_barrier((arrived, near_w))
    mixed_in, forget, value = read_out(arrived, past_state, forget_floor, head_gain)
    new_state = update_state(forget, value, past_state)
    gathered = copy_for_each(mixed_in, KV).reshape(-1, mixed_in.shape[1])
    gathered, new_state = lax.optimization_barrier((gathered, new_state))
    mine, theirs = project_out(gathered, proj_out)
    mixed = (mine.astype(f32) + other_core(theirs).astype(f32)).astype(bf16)
    mixed_sum = mixed[0].astype(f32)
    for piece in [shift_x(mixed[k], k) for k in (2, 1, 3)]:
        mixed_sum = mixed_sum + piece.astype(f32)
    second = lax.optimization_barrier((first.astype(f32) + mixed_sum).astype(bf16))
    near = plane_gather(second)
    near, far_w = lax.optimization_barrier((near, far_w))
    far_w = other_core(far_w)
    result = half_step(second, near_w, far_w, gains, near)
    return (result.T, new_state)


def solution(mesh):
    torus = Mesh(mesh.devices.reshape(4, 4, 4, 2), ALL)
    return jax.shard_map(
        per_device,
        mesh=torus,
        in_specs=(
            P(None, ALL),
            P(KV, TP, None, None),
            P(),
            P(None, ALL),
            P(None, ALL),
            P(ALL, None),
            P(),
            P(KV, TP),
            P(KV, TP),
            P(KV, TP),
            P(KV, TP),
            P(TP),
            P(),
            P(TP, KV),
            P(),
            P(None, ALL),
            P(None, ALL),
            P(ALL, None),
        ),
        out_specs=(P(None, ALL), P(KV, TP, None, None)),
        check_vma=False,
    )
```

profile of v0, /device:TPU:0, one launch (start us, length us, event | category | flops | bytes accessed | tf_op | source)
XLA Modules:
  0.0 199.9 jit_solution(15211693628161406451)
XLA Ops:
  2.3 8.2 %all-to-all-start = ((bf16[16,32,512]{2,1,0:T(8,128)(2,1)}), bf16[16,32,512]{2,1,0:T(8,128)(2,1)S(1)}, u32[]{:S(2)}, u32[]{:S(2)}) async-start(bf16[16,32,512]{2,1,0:T(8,128)(2,1)} %broadcast_in_dim.8), calls=%async_computation | async-start | bytes 1048576 | tf_op jit(solution)/shard_map/all_to_all | solution.py:58
  10.5 5.4 %order.2 = (bf16[4,3,96,512]{3,2,1,0:T(8,128)(2,1)S(1)}, bf16[4,3,96,512]{3,2,1,0:T(8,128)(2,1)S(1)}, f32[4,512,128]{2,1,0:T(8,128)S(1)}) custom-call(s32[1,512]{1,0:T(1,128)S(1)} %get-tuple-element.85.mine, s32[1,512]{1,0:T(1,128)S(1)} %get-tuple-element.86.theirs, f32[4,1,1024]{2,1,0:T(1,128)S(1)} %bitcast.74, bf16[88,4096]{1,0:T(8,128)(2,1)} %bitcast.82, ...), custom_call_target="tpu_custom_call" | custom-call | flops 5000000000 | bytes 6000000 | tf_op jit(solution)/shard_map/order/pallas_call | solution.py:119
  16.9 3.6 %all-to-all-done = bf16[16,32,512]{2,1,0:T(8,128)(2,1)S(1)} async-done(((bf16[16,32,512]{2,1,0:T(8,128)(2,1)}), bf16[16,32,512]{2,1,0:T(8,128)(2,1)S(1)}, u32[]{:S(2)}, u32[]{:S(2)}) %all-to-all-start) | async-done | bytes 524320 | tf_op jit(solution)/shard_map/all_to_all | solution.py:58
  24.2 3.0 %collective-permute-start.6 = (bf16[256,512]{1,0:T(8,128)(2,1)S(1)}, bf16[256,512]{1,0:T(8,128)(2,1)S(1)}, u32[]{:S(2)}, u32[]{:S(2)}) collective-permute-start(bf16[256,512]{1,0:T(8,128)(2,1)S(1)} %get-tuple-element.77), channel_id=1, source_target_pairs={{0,6},{1,25},{2,0},{3,27},{4,2},{5,29},{6,4},{7,31},{8,14},{9,1},{... | collective-permute-start | bytes 786440 | tf_op jit(solution)/shard_map/ppermute | solution.py:49
  32.6 3.5 %collective-permute-done.3.refs_0_ = bf16[256,512]{1,0:T(8,128)(2,1)S(1)} collective-permute-done((bf16[256,512]{1,0:T(8,128)(2,1)S(1)}, bf16[256,512]{1,0:T(8,128)(2,1)S(1)}, u32[]{:S(2)}, u32[]{:S(2)}) %collective-permute-start.3) | collective-permute-done | bytes 262176 | tf_op jit(solution)/shard_map/ppermute | solution.py:49
  40.1 3.0 %collective-permute-start.8 = (bf16[512,512]{1,0:T(8,128)(2,1)S(1)}, bf16[512,512]{1,0:T(8,128)(2,1)S(1)}, u32[]{:S(2)}, u32[]{:S(2)}) collective-permute-start(bf16[512,512]{1,0:T(8,128)(2,1)S(1)} %convolution_convert_fusion.6), channel_id=1, source_target_pairs={{0,4},{1,17},{2,6},{3,19},{4,0},{5,21},{6,2},{7,23},{8,12},{9,25},... | collective-permute-start | bytes 1572872 | tf_op jit(solution)/shard_map/ppermute | solution.py:49
  46.3 4.6 %collective-permute-done.8 = bf16[512,512]{1,0:T(8,128)(2,1)S(1)} collective-permute-done((bf16[512,512]{1,0:T(8,128)(2,1)S(1)}, bf16[512,512]{1,0:T(8,128)(2,1)S(1)}, u32[]{:S(2)}, u32[]{:S(2)}) %collective-permute-start.8) | collective-permute-done | bytes 524320 | tf_op jit(solution)/shard_map/ppermute | solution.py:49
  50.9 5.5 %collective-permute-done.9 = bf16[512,512]{1,0:T(8,128)(2,1)S(1)} collective-permute-done((bf16[512,512]{1,0:T(8,128)(2,1)S(1)}, bf16[512,512]{1,0:T(8,128)(2,1)S(1)}, u32[]{:S(2)}, u32[]{:S(2)}) %collective-permute-start.9) | collective-permute-done | bytes 524320 | tf_op jit(solution)/shard_map/ppermute | solution.py:49
  57.3 15.0 %all_to_all.30 = bf16[16,32,512]{2,1,0:T(8,128)(2,1)S(1)} all-to-all(bf16[16,32,512]{2,1,0:T(8,128)(2,1)S(1)} %bitcast.76), channel_id=1, replica_groups={{0,8,16,24,32,40,48,56,64,72,80,88,96,104,112,120},{2,10,18,26,34,42,50..., dimensions={0} | all-to-all | bytes 1048576 | tf_op jit(solution)/shard_map/all_to_all | solution.py:58
  79.4 3.0 %collective-permute-done.13.refs_2_ = bf16[64,512]{1,0:T(8,128)(2,1)S(1)} collective-permute-done((bf16[64,512]{1,0:T(8,128)(2,1)S(1)}, bf16[64,512]{1,0:T(8,128)(2,1)S(1)}, u32[]{:S(2)}, u32[]{:S(2)}) %collective-permute-start.13) | collective-permute-done | bytes 65568 | tf_op jit(solution)/shard_map/ppermute | solution.py:54
  85.2 4.0 %all-to-all-start.2 = ((bf16[16,32,1152]{2,1,0:T(8,128)(2,1)}), bf16[16,32,1152]{2,1,0:T(8,128)(2,1)S(1)}, u32[]{:S(2)}, u32[]{:S(2)}) async-start(bf16[16,32,1152]{2,1,0:T(8,128)(2,1)} %project.1), calls=%async_computation.2 | async-start | bytes 2359296 | tf_op jit(solution)/shard_map/all_to_all | solution.py:27
  89.3 5.4 %order.3 = (bf16[4,3,96,512]{3,2,1,0:T(8,128)(2,1)S(1)}, bf16[4,3,96,512]{3,2,1,0:T(8,128)(2,1)S(1)}, f32[4,512,128]{2,1,0:T(8,128)S(1)}) custom-call(s32[1,512]{1,0:T(1,128)S(1)} %get-tuple-element.85.mine, s32[1,512]{1,0:T(1,128)S(1)} %get-tuple-element.86.theirs, f32[4,1,1024]{2,1,0:T(1,128)S(1)} %bitcast.75, bf16[88,4096]{1,0:T(8,128)(2,1)} %bitcast.84, ...), custom_call_target="tpu_custom_call" | custom-call | flops 5000000000 | bytes 6000000 | tf_op jit(solution)/shard_map/order/pallas_call | solution.py:119
  95.8 12.5 %all-to-all-done.2.arrived = bf16[16,32,1152]{2,1,0:T(8,128)(2,1)S(1)} async-done(((bf16[16,32,1152]{2,1,0:T(8,128)(2,1)}), bf16[16,32,1152]{2,1,0:T(8,128)(2,1)S(1)}, u32[]{:S(2)}, u32[]{:S(2)}) %all-to-all-start.2) | async-done | bytes 1179680 | tf_op jit(solution)/shard_map/all_to_all | solution.py:27
  108.3 4.1 %readout.1 = (bf16[32,256]{1,0:T(8,128)(2,1)S(1)}, f32[32,256]{1,0:T(8,128)S(1)}, f32[32,256]{1,0:T(8,128)S(1)}) custom-call(bf16[16,32,1152]{2,1,0:T(8,128)(2,1)S(1)} %all-to-all-done.2.arrived, f32[32,2,128,128]{3,2,1,0:T(8,128)} %past.3, f32[1,256]{1,0:T(1,128)S(1)} %bitcast.72, f32[1,128]{1,0:T(1,128)S(1)} %bitcast.73), custom_call_target="tpu_custom_call" | custom-call | tf_op jit(solution)/shard_map/readout/pallas_call | solution.py:253
  113.2 3.5 %all-to-all-start.3 = ((bf16[16,32,256]{2,1,0:T(8,128)(2,1)}), bf16[16,32,256]{2,1,0:T(8,128)(2,1)S(1)}, u32[]{:S(2)}, u32[]{:S(2)}) async-start(bf16[16,32,256]{2,1,0:T(8,128)(2,1)} %broadcast_in_dim.19), calls=%async_computation.3 | async-start | bytes 524288 | tf_op jit(solution)/shard_map/all_to_all | solution.py:23
  116.7 5.9 %state.1 = f32[32,2,128,128]{3,2,1,0:T(8,128)} custom-call(f32[32,256]{1,0:T(8,128)S(1)} %get-tuple-element.54.forget, f32[32,256]{1,0:T(8,128)S(1)} %get-tuple-element.55.value, f32[32,2,128,128]{3,2,1,0:T(8,128)} %past.3), custom_call_target="tpu_custom_call" | custom-call | flops 4000000000 | bytes 8000000 | tf_op jit(solution)/shard_map/state/pallas_call | solution.py:296
  128.6 3.2 %collective-permute-start.18 = (bf16[32,512]{1,0:T(8,128)(2,1)S(1)}, bf16[32,512]{1,0:T(8,128)(2,1)S(1)}, u32[]{:S(2)}, u32[]{:S(2)}) collective-permute-start(bf16[32,512]{1,0:T(8,128)(2,1)S(1)} %get-tuple-element.79), channel_id=1, source_target_pairs={{0,6},{1,7},{2,0},{3,1},{4,2},{5,3},{6,4},{7,5},{8,14},{9,15},{10,... | collective-permute-start | bytes 98312 | tf_op jit(solution)/shard_map/ppermute | solution.py:54
  133.8 14.4 %all_to_all.31 = bf16[16,32,512]{2,1,0:T(8,128)(2,1)S(1)} all-to-all(bf16[16,32,512]{2,1,0:T(8,128)(2,1)S(1)} %broadcast_in_dim.20), channel_id=1, replica_groups={{0,8,16,24,32,40,48,56,64,72,80,88,96,104,112,120},{2,10,18,26,34,42,50..., dimensions={0} | all-to-all | bytes 1048576 | tf_op jit(solution)/shard_map/all_to_all | solution.py:58
  151.8 3.1 %collective-permute-start.25 = (bf16[256,512]{1,0:T(8,128)(2,1)S(1)}, bf16[256,512]{1,0:T(8,128)(2,1)S(1)}, u32[]{:S(2)}, u32[]{:S(2)}) collective-permute-start(bf16[256,512]{1,0:T(8,128)(2,1)S(1)} %get-tuple-element.75), channel_id=1, source_target_pairs={{0,6},{1,25},{2,0},{3,27},{4,2},{5,29},{6,4},{7,31},{8,14},{9,1},{... | collective-permute-start | bytes 786440 | tf_op jit(solution)/shard_map/ppermute | solution.py:49
  160.2 3.5 %collective-permute-done.22.refs_0_ = bf16[256,512]{1,0:T(8,128)(2,1)S(1)} collective-permute-done((bf16[256,512]{1,0:T(8,128)(2,1)S(1)}, bf16[256,512]{1,0:T(8,128)(2,1)S(1)}, u32[]{:S(2)}, u32[]{:S(2)}) %collective-permute-start.22) | collective-permute-done | bytes 262176 | tf_op jit(solution)/shard_map/ppermute | solution.py:49
  167.4 3.4 %collective-permute-start.27 = (bf16[512,512]{1,0:T(8,128)(2,1)S(1)}, bf16[512,512]{1,0:T(8,128)(2,1)S(1)}, u32[]{:S(2)}, u32[]{:S(2)}) collective-permute-start(bf16[512,512]{1,0:T(8,128)(2,1)S(1)} %convolution_convert_fusion.2), channel_id=1, source_target_pairs={{0,4},{1,17},{2,6},{3,19},{4,0},{5,21},{6,2},{7,23},{8,12},{9,25},... | collective-permute-start | bytes 1572872 | tf_op jit(solution)/shard_map/ppermute | solution.py:49
  174.0 4.2 %collective-permute-done.27 = bf16[512,512]{1,0:T(8,128)(2,1)S(1)} collective-permute-done((bf16[512,512]{1,0:T(8,128)(2,1)S(1)}, bf16[512,512]{1,0:T(8,128)(2,1)S(1)}, u32[]{:S(2)}, u32[]{:S(2)}) %collective-permute-start.27) | collective-permute-done | bytes 524320 | tf_op jit(solution)/shard_map/ppermute | solution.py:49
  178.2 5.5 %collective-permute-done.28 = bf16[512,512]{1,0:T(8,128)(2,1)S(1)} collective-permute-done((bf16[512,512]{1,0:T(8,128)(2,1)S(1)}, bf16[512,512]{1,0:T(8,128)(2,1)S(1)}, u32[]{:S(2)}, u32[]{:S(2)}) %collective-permute-start.28) | collective-permute-done | bytes 524320 | tf_op jit(solution)/shard_map/ppermute | solution.py:49
  184.8 14.5 %all_to_all.32 = bf16[16,32,512]{2,1,0:T(8,128)(2,1)S(1)} all-to-all(bf16[16,32,512]{2,1,0:T(8,128)(2,1)S(1)} %bitcast.77), channel_id=1, replica_groups={{0,8,16,24,32,40,48,56,64,72,80,88,96,104,112,120},{2,10,18,26,34,42,50..., dimensions={0} | all-to-all | bytes 1048576 | tf_op jit(solution)/shard_map/all_to_all | solution.py:58
  (118 shorter events, 56.7 us)
Async XLA Ops:
  2.3 18.3 %all-to-all-start = ((bf16[16,32,512]{2,1,0:T(8,128)(2,1)}), bf16[16,32,512]{2,1,0:T(8,128)(2,1)S(1)}, u32[]{:S(2)}, u32[]{:S(2)}) async-start(bf16[16,32,512]{2,1,0:T(8,128)(2,1)} %broadcast_in_dim.8), calls=%async_computation | async-start | bytes 1048576 | tf_op jit(solution)/shard_map/all_to_all | solution.py:58
  20.6 8.0 %collective-permute-start.2 = (bf16[4,3,96,512]{3,2,1,0:T(8,128)(2,1)}, bf16[4,3,96,512]{3,2,1,0:T(8,128)(2,1)S(1)}, u32[]{:S(2)}, u32[]{:S(2)}) collective-permute-start(bf16[4,3,96,512]{3,2,1,0:T(8,128)(2,1)} %copy-done.9), channel_id=1, source_target_pairs={{0,1},{1,0},{2,3},{3,2},{4,5},{5,4},{6,7},{7,6},{8,9},{9,8},{10,11... | collective-permute-start | bytes 3538952 | tf_op jit(solution)/shard_map/ppermute | solution.py:31
  20.6 7.7 %collective-permute-start = (bf16[256,512]{1,0:T(8,128)(2,1)S(1)}, bf16[256,512]{1,0:T(8,128)(2,1)S(1)}, u32[]{:S(2)}, u32[]{:S(2)}) collective-permute-start(bf16[256,512]{1,0:T(8,128)(2,1)S(1)} %get-tuple-element.77), channel_id=1, source_target_pairs={{0,2},{1,9},{2,4},{3,11},{4,6},{5,13},{6,0},{7,15},{8,10},{9,17},{... | collective-permute-start | bytes 786440 | tf_op jit(solution)/shard_map/ppermute | solution.py:49
  22.2 6.4 %collective-permute-start.1 = (bf16[256,512]{1,0:T(8,128)(2,1)S(1)}, bf16[256,512]{1,0:T(8,128)(2,1)S(1)}, u32[]{:S(2)}, u32[]{:S(2)}) collective-permute-start(bf16[256,512]{1,0:T(8,128)(2,1)S(1)} %get-tuple-element.76), channel_id=1, source_target_pairs={{0,6},{1,25},{2,0},{3,27},{4,2},{5,29},{6,4},{7,31},{8,14},{9,1},{... | collective-permute-start | bytes 786440 | tf_op jit(solution)/shard_map/ppermute | solution.py:49
  23.9 7.9 %collective-permute-start.5 = (bf16[256,512]{1,0:T(8,128)(2,1)S(1)}, bf16[256,512]{1,0:T(8,128)(2,1)S(1)}, u32[]{:S(2)}, u32[]{:S(2)}) collective-permute-start(bf16[256,512]{1,0:T(8,128)(2,1)S(1)} %get-tuple-element.76), channel_id=1, source_target_pairs={{0,2},{1,9},{2,4},{3,11},{4,6},{5,13},{6,0},{7,15},{8,10},{9,17},{... | collective-permute-start | bytes 786440 | tf_op jit(solution)/shard_map/ppermute | solution.py:49
  24.2 7.6 %collective-permute-start.6 = (bf16[256,512]{1,0:T(8,128)(2,1)S(1)}, bf16[256,512]{1,0:T(8,128)(2,1)S(1)}, u32[]{:S(2)}, u32[]{:S(2)}) collective-permute-start(bf16[256,512]{1,0:T(8,128)(2,1)S(1)} %get-tuple-element.77), channel_id=1, source_target_pairs={{0,6},{1,25},{2,0},{3,27},{4,2},{5,29},{6,4},{7,31},{8,14},{9,1},{... | collective-permute-start | bytes 786440 | tf_op jit(solution)/shard_map/ppermute | solution.py:49
  28.5 7.6 %collective-permute-start.3 = (bf16[256,512]{1,0:T(8,128)(2,1)S(1)}, bf16[256,512]{1,0:T(8,128)(2,1)S(1)}, u32[]{:S(2)}, u32[]{:S(2)}) collective-permute-start(bf16[256,512]{1,0:T(8,128)(2,1)S(1)} %collective-permute-done.refs_1_), channel_id=1, source_target_pairs={{0,2},{1,9},{2,4},{3,11},{4,6},{5,13},{6,0},{7,15},{8,10},{9,17},{... | collective-permute-start | bytes 786440 | tf_op jit(solution)/shard_map/ppermute | solution.py:49
  30.0 6.4 %collective-permute-start.4 = (bf16[256,512]{1,0:T(8,128)(2,1)S(1)}, bf16[256,512]{1,0:T(8,128)(2,1)S(1)}, u32[]{:S(2)}, u32[]{:S(2)}) collective-permute-start(bf16[256,512]{1,0:T(8,128)(2,1)S(1)} %collective-permute-done.1.refs_2_), channel_id=1, source_target_pairs={{0,6},{1,25},{2,0},{3,27},{4,2},{5,29},{6,4},{7,31},{8,14},{9,1},{... | collective-permute-start | bytes 786440 | tf_op jit(solution)/shard_map/ppermute | solution.py:49
  40.1 10.9 %collective-permute-start.8 = (bf16[512,512]{1,0:T(8,128)(2,1)S(1)}, bf16[512,512]{1,0:T(8,128)(2,1)S(1)}, u32[]{:S(2)}, u32[]{:S(2)}) collective-permute-start(bf16[512,512]{1,0:T(8,128)(2,1)S(1)} %convolution_convert_fusion.6), channel_id=1, source_target_pairs={{0,4},{1,17},{2,6},{3,19},{4,0},{5,21},{6,2},{7,23},{8,12},{9,25},... | collective-permute-start | bytes 1572872 | tf_op jit(solution)/shard_map/ppermute | solution.py:49
  43.1 13.4 %collective-permute-start.9 = (bf16[512,512]{1,0:T(8,128)(2,1)S(1)}, bf16[512,512]{1,0:T(8,128)(2,1)S(1)}, u32[]{:S(2)}, u32[]{:S(2)}) collective-permute-start(bf16[512,512]{1,0:T(8,128)(2,1)S(1)} %convolution_convert_fusion.5), channel_id=1, source_target_pairs={{0,2},{1,9},{2,4},{3,11},{4,6},{5,13},{6,0},{7,15},{8,10},{9,17},{... | collective-permute-start | bytes 1572872 | tf_op jit(solution)/shard_map/ppermute | solution.py:49
  44.0 12.8 %collective-permute-start.10 = (bf16[512,512]{1,0:T(8,128)(2,1)S(1)}, bf16[512,512]{1,0:T(8,128)(2,1)S(1)}, u32[]{:S(2)}, u32[]{:S(2)}) collective-permute-start(bf16[512,512]{1,0:T(8,128)(2,1)S(1)} %convolution_convert_fusion.4), channel_id=1, source_target_pairs={{0,6},{1,25},{2,0},{3,27},{4,2},{5,29},{6,4},{7,31},{8,14},{9,1},{... | collective-permute-start | bytes 1572872 | tf_op jit(solution)/shard_map/ppermute | solution.py:49
  76.8 6.2 %collective-permute-start.14 = (bf16[64,512]{1,0:T(8,128)(2,1)S(1)}, bf16[64,512]{1,0:T(8,128)(2,1)S(1)}, u32[]{:S(2)}, u32[]{:S(2)}) collective-permute-start(bf16[64,512]{1,0:T(8,128)(2,1)S(1)} %pad_maximum_fusion.4.refs_0_), channel_id=1, source_target_pairs={{0,2},{1,3},{2,4},{3,5},{4,6},{5,7},{6,0},{7,1},{8,10},{9,11},{10,... | collective-permute-start | bytes 196616 | tf_op jit(solution)/shard_map/ppermute | solution.py:54
  85.2 23.1 %all-to-all-start.2 = ((bf16[16,32,1152]{2,1,0:T(8,128)(2,1)}), bf16[16,32,1152]{2,1,0:T(8,128)(2,1)S(1)}, u32[]{:S(2)}, u32[]{:S(2)}) async-start(bf16[16,32,1152]{2,1,0:T(8,128)(2,1)} %project.1), calls=%async_computation.2 | async-start | bytes 2359296 | tf_op jit(solution)/shard_map/all_to_all | solution.py:27
  113.2 12.2 %all-to-all-start.3 = ((bf16[16,32,256]{2,1,0:T(8,128)(2,1)}), bf16[16,32,256]{2,1,0:T(8,128)(2,1)S(1)}, u32[]{:S(2)}, u32[]{:S(2)}) async-start(bf16[16,32,256]{2,1,0:T(8,128)(2,1)} %broadcast_in_dim.19), calls=%async_computation.3 | async-start | bytes 524288 | tf_op jit(solution)/shard_map/all_to_all | solution.py:23
  148.2 7.9 %collective-permute-start.21 = (bf16[4,3,96,512]{3,2,1,0:T(8,128)(2,1)S(1)}, bf16[4,3,96,512]{3,2,1,0:T(8,128)(2,1)S(1)}, u32[]{:S(2)}, u32[]{:S(2)}) collective-permute-start(bf16[4,3,96,512]{3,2,1,0:T(8,128)(2,1)S(1)} %copy-done.8), channel_id=1, source_target_pairs={{0,1},{1,0},{2,3},{3,2},{4,5},{5,4},{6,7},{7,6},{8,9},{9,8},{10,11... | collective-permute-start | bytes 3538952 | tf_op jit(solution)/shard_map/ppermute | solution.py:31
  148.3 7.7 %collective-permute-start.19 = (bf16[256,512]{1,0:T(8,128)(2,1)S(1)}, bf16[256,512]{1,0:T(8,128)(2,1)S(1)}, u32[]{:S(2)}, u32[]{:S(2)}) collective-permute-start(bf16[256,512]{1,0:T(8,128)(2,1)S(1)} %get-tuple-element.75), channel_id=1, source_target_pairs={{0,2},{1,9},{2,4},{3,11},{4,6},{5,13},{6,0},{7,15},{8,10},{9,17},{... | collective-permute-start | bytes 786440 | tf_op jit(solution)/shard_map/ppermute | solution.py:49
  149.7 6.4 %collective-permute-start.20 = (bf16[256,512]{1,0:T(8,128)(2,1)S(1)}, bf16[256,512]{1,0:T(8,128)(2,1)S(1)}, u32[]{:S(2)}, u32[]{:S(2)}) collective-permute-start(bf16[256,512]{1,0:T(8,128)(2,1)S(1)} %get-tuple-element.74), channel_id=1, source_target_pairs={{0,6},{1,25},{2,0},{3,27},{4,2},{5,29},{6,4},{7,31},{8,14},{9,1},{... | collective-permute-start | bytes 786440 | tf_op jit(solution)/shard_map/ppermute | solution.py:49
  151.6 7.7 %collective-permute-start.24 = (bf16[256,512]{1,0:T(8,128)(2,1)S(1)}, bf16[256,512]{1,0:T(8,128)(2,1)S(1)}, u32[]{:S(2)}, u32[]{:S(2)}) collective-permute-start(bf16[256,512]{1,0:T(8,128)(2,1)S(1)} %get-tuple-element.74), channel_id=1, source_target_pairs={{0,2},{1,9},{2,4},{3,11},{4,6},{5,13},{6,0},{7,15},{8,10},{9,17},{... | collective-permute-start | bytes 786440 | tf_op jit(solution)/shard_map/ppermute | solution.py:49
  151.8 7.6 %collective-permute-start.25 = (bf16[256,512]{1,0:T(8,128)(2,1)S(1)}, bf16[256,512]{1,0:T(8,128)(2,1)S(1)}, u32[]{:S(2)}, u32[]{:S(2)}) collective-permute-start(bf16[256,512]{1,0:T(8,128)(2,1)S(1)} %get-tuple-element.75), channel_id=1, source_target_pairs={{0,6},{1,25},{2,0},{3,27},{4,2},{5,29},{6,4},{7,31},{8,14},{9,1},{... | collective-permute-start | bytes 786440 | tf_op jit(solution)/shard_map/ppermute | solution.py:49
  156.1 7.6 %collective-permute-start.22 = (bf16[256,512]{1,0:T(8,128)(2,1)S(1)}, bf16[256,512]{1,0:T(8,128)(2,1)S(1)}, u32[]{:S(2)}, u32[]{:S(2)}) collective-permute-start(bf16[256,512]{1,0:T(8,128)(2,1)S(1)} %collective-permute-done.19.refs_1_), channel_id=1, source_target_pairs={{0,2},{1,9},{2,4},{3,11},{4,6},{5,13},{6,0},{7,15},{8,10},{9,17},{... | collective-permute-start | bytes 786440 | tf_op jit(solution)/shard_map/ppermute | solution.py:49
  157.3 6.4 %collective-permute-start.23 = (bf16[256,512]{1,0:T(8,128)(2,1)S(1)}, bf16[256,512]{1,0:T(8,128)(2,1)S(1)}, u32[]{:S(2)}, u32[]{:S(2)}) collective-permute-start(bf16[256,512]{1,0:T(8,128)(2,1)S(1)} %collective-permute-done.20.refs_2_), channel_id=1, source_target_pairs={{0,6},{1,25},{2,0},{3,27},{4,2},{5,29},{6,4},{7,31},{8,14},{9,1},{... | collective-permute-start | bytes 786440 | tf_op jit(solution)/shard_map/ppermute | solution.py:49
  167.4 10.9 %collective-permute-start.27 = (bf16[512,512]{1,0:T(8,128)(2,1)S(1)}, bf16[512,512]{1,0:T(8,128)(2,1)S(1)}, u32[]{:S(2)}, u32[]{:S(2)}) collective-permute-start(bf16[512,512]{1,0:T(8,128)(2,1)S(1)} %convolution_convert_fusion.2), channel_id=1, source_target_pairs={{0,4},{1,17},{2,6},{3,19},{4,0},{5,21},{6,2},{7,23},{8,12},{9,25},... | collective-permute-start | bytes 1572872 | tf_op jit(solution)/shard_map/ppermute | solution.py:49
  170.8 12.9 %collective-permute-start.28 = (bf16[512,512]{1,0:T(8,128)(2,1)S(1)}, bf16[512,512]{1,0:T(8,128)(2,1)S(1)}, u32[]{:S(2)}, u32[]{:S(2)}) collective-permute-start(bf16[512,512]{1,0:T(8,128)(2,1)S(1)} %convolution_convert_fusion.1), channel_id=1, source_target_pairs={{0,2},{1,9},{2,4},{3,11},{4,6},{5,13},{6,0},{7,15},{8,10},{9,17},{... | collective-permute-start | bytes 1572872 | tf_op jit(solution)/shard_map/ppermute | solution.py:49
  171.5 12.8 %collective-permute-start.29 = (bf16[512,512]{1,0:T(8,128)(2,1)S(1)}, bf16[512,512]{1,0:T(8,128)(2,1)S(1)}, u32[]{:S(2)}, u32[]{:S(2)}) collective-permute-start(bf16[512,512]{1,0:T(8,128)(2,1)S(1)} %convolution_convert_fusion), channel_id=1, source_target_pairs={{0,6},{1,25},{2,0},{3,27},{4,2},{5,29},{6,4},{7,31},{8,14},{9,1},{... | collective-permute-start | bytes 1572872 | tf_op jit(solution)/shard_map/ppermute | solution.py:49
  (22 other events, 236.0 us)
where the time goes:
time: 201 us; the launch traced here: 200 us
  waiting for transfers between devices  62.3 us (31%)
  starting transfers between devices  56.4 us (28%)
  blocking collectives  43.8 us (22%)
  Pallas kernels  26.2 us (13%)
  local copies, waits for them, and re-layouts  5.59 us (3%)
  matrix products  2.79 us (1%)
    all_to_all x3, blocking collectives, plane_exchange(): lax.all_to_all(pieces, ALL, split_axis=0, concat_axis=0, axis_index_group...  43.8 us
    ppermute x18, starting transfers between devices, shift(): return lax.ppermute(value, ALL, pairs)  32.6 us
    ppermute x18, waiting for transfers between devices, shift(): return lax.ppermute(value, ALL, pairs)  30.7 us
    all_to_all x1, waiting for transfers between devices, exchange(): return lax.all_to_all(pieces, axes, split_axis=0, concat_axis=0, tiled=True)  12.5 us
    pallas_call x2, Pallas kernels, order_weights(): pl.pallas_call(order_body, grid=(4,), in_specs=[whole, whole, pl.BlockSpe...  10.9 us
    all_to_all x1, starting transfers between devices, plane_exchange(): lax.all_to_all(pieces, ALL, split_axis=0, concat_axis=0, axis_index_group...  8.16 us
    ppermute x6, starting transfers between devices, shift_x(): return lax.ppermute(value, ALL, pairs)  7.76 us
    ppermute x6, waiting for transfers between devices, shift_x(): return lax.ppermute(value, ALL, pairs)  7.66 us
  transfers between devices with their start and end apart: 33, of which 25 were waited for; matrix products, arithmetic and copies ran while one was open for 1% of the time, Pallas kernels for 9%

commit v1 on v0

--- a/solution.py
+++ b/solution.py
@@ -198,108 +198,118 @@
     )(*operands)
 
 
-def readout_body(arrived, past, floor, gain, mixed, forget, value, query, gate, readout):
-    step = pl.program_id(0)
-    group, heads, width, _ = past.shape
-
-    @pl.when(step == 0)
-    def _():
-        total = arrived[0].astype(f32)
-        for i in range(1, arrived.shape[0]):
-            total = total + arrived[i].astype(f32)
-        inner = heads * width
-        squares = total[:, 4 * inner : 4 * inner + 1] + total[:, 4 * inner + 64 : 4 * inner + 65]
-        total = total[:, : 4 * inner] * lax.rsqrt(squares / D + epsilon)
-        query[...] = jax.nn.silu(total[:, :inner])
-        value[...] = total[:, 2 * inner : 3 * inner]
-        gate[...] = jax.nn.silu(total[:, 3 * inner :])
-        bound = floor[...]
-        forget[...] = bound + (1.0 - bound) * jax.nn.sigmoid(total[:, inner : 2 * inner])
-
-    here = pl.ds(pl.multiple_of(group * step, group), group)
-    for h in range(heads):
-        lanes = slice(width * h, width * (h + 1))
-        keep, ask = forget[here, lanes], query[here, lanes]
-        both = keep * ask
-        high = both.astype(bf16).astype(f32)
-        both = jnp.concatenate([high, both - high], axis=0).astype(bf16)
-        sums = []
-        for j in range(group):
-            state = past[j, h]
-            top = state.astype(bf16)
-            low = (state - top.astype(f32)).astype(bf16)
-            dots = jnp.dot(both, top, preferred_element_type=f32) + jnp.dot(
-                both, low, preferred_element_type=f32
-            )
-            sums.append(dots[j : j + 1] + dots[group + j : group + j + 1])
-        share = jnp.sum((1.0 - keep) * ask, axis=1, keepdims=True)
-        readout[here, lanes] = jnp.concatenate(sums, axis=0) + share * value[here, lanes]
-
-    @pl.when(step == pl.num_programs(0) - 1)
-    def _():
+def chunk_copies(source, target, sems, outward=False):
+    copies = []
+    for i in range(target.shape[0] // 8):
+        rows = pl.ds(8 * i, 8)
+        ends = (target.at[rows], source.at[rows]) if outward else (source.at[rows], target.at[rows])
+        copies.append(pltpu.make_async_copy(*ends, sems.at[i]))
+    return copies
+
+
+def readout_body(arrived, past, floor, gain, mixed, forget, value, query, gate, states, sems):
+    copies = chunk_copies(past, states, sems)
+    for copy in copies:
+        copy.start()
+    heads, width = past.shape[1:3]
+    inner = heads * width
+    total = arrived[0].astype(f32)
+    for i in range(1, arrived.shape[0]):
+        total = total + arrived[i].astype(f32)
+    squares = total[:, 4 * inner : 4 * inner + 1] + total[:, 4 * inner + 64 : 4 * inner + 65]
+    total = total[:, : 4 * inner] * lax.rsqrt(squares / D + epsilon)
+    query[...] = jax.nn.silu(total[:, :inner])
+    value[...] = total[:, 2 * inner : 3 * inner]
+    gate[...] = jax.nn.silu(total[:, 3 * inner :])
+    bound = floor[...]
+    forget[...] = bound + (1.0 - bound) * jax.nn.sigmoid(total[:, inner : 2 * inner])
+    for i, copy in enumerate(copies):
+        copy.wait()
+        here = slice(8 * i, 8 * (i + 1))
         for h in range(heads):
             lanes = slice(width * h, width * (h + 1))
-            r = readout[:, lanes]
+            keep, ask = forget[here, lanes], query[here, lanes]
+            both = keep * ask
+            high = both.astype(bf16).astype(f32)
+            both = jnp.concatenate([high, both - high], axis=0).astype(bf16)
+            sums = []
+            for j in range(8):
+                state = states[8 * i + j, h]
+                top = state.astype(bf16)
+                low = (state - top.astype(f32)).astype(bf16)
+                dots = jnp.dot(both, top, preferred_element_type=f32) + jnp.dot(
+                    both, low, preferred_element_type=f32
+                )
+                sums.append(dots[j : j + 1] + dots[8 + j : 8 + j + 1])
+            share = jnp.sum((1.0 - keep) * ask, axis=1, keepdims=True)
+            r = jnp.concatenate(sums, axis=0) + share * value[here, lanes]
             r = r * lax.rsqrt(jnp.mean(r * r, axis=1, keepdims=True) + epsilon) * gain[...]
-            mixed[:, lanes] = (r * gate[:, lanes]).astype(bf16)
+            query[here, lanes] = r * gate[here, lanes]
+    mixed[...] = query[...].astype(bf16)
 
 
 def read_out(arrived, past, floor, gain):
     count, heads, width, _ = past.shape
-    inner, group = heads * width, 8
+    inner = heads * width
     rows = pltpu.VMEM((count, inner), f32)
     table = jax.ShapeDtypeStruct((count, inner), f32)
-    whole = pl.BlockSpec((count, inner), lambda i: (0, 0))
     return pl.pallas_call(
         readout_body,
-        grid=(count // group,),
         in_specs=[
-            pl.BlockSpec(arrived.shape, lambda i: (0, 0, 0)),
-            pl.BlockSpec((group, heads, width, width), lambda i: (i, 0, 0, 0)),
-            pl.BlockSpec((1, inner), lambda i: (0, 0)),
-            pl.BlockSpec((1, width), lambda i: (0, 0)),
+            pl.BlockSpec(arrived.shape, lambda: (0, 0, 0)),
+            pl.BlockSpec(memory_space=pl.ANY),
+            pl.BlockSpec((1, inner), lambda: (0, 0)),
+            pl.BlockSpec((1, width), lambda: (0, 0)),
         ],
-        out_specs=[whole, whole, whole],
         out_shape=[jax.ShapeDtypeStruct((count, inner), bf16), table, table],
-        scratch_shapes=[rows, rows, rows],
-        compiler_params=pltpu.CompilerParams(vmem_limit_bytes=12 * 2**20),
+        scratch_shapes=[
+            rows,
+            rows,
+            pltpu.VMEM(past.shape, f32),
+            pltpu.SemaphoreType.DMA((count // 8,)),
+        ],
+        compiler_params=pltpu.CompilerParams(vmem_limit_bytes=14 * 2**20),
         name="readout",
     )(arrived, in_hbm(past), floor.reshape(1, -1), gain.reshape(1, -1))
 
 
-def state_body(forget, value, past, new, columns):
-    step = pl.program_id(0)
-    group, heads, width, _ = past.shape
-    count = forget.shape[0]
-
-    @pl.when(step == 0)
-    def _():
+def state_body(forget, value, past, new, columns, states, arrivals, departures):
+    copies = chunk_copies(past, states, arrivals)
+    for copy in copies:
+        copy.start()
+    count, heads, width, _ = past.shape
+    for h in range(heads):
+        table = forget[:, width * h : width * (h + 1)]
+        columns[h] = jnp.concatenate([table] * (width // count), axis=0).T
+    leaving = chunk_copies(new, states, departures, outward=True)
+    for i, copy in enumerate(copies):
+        copy.wait()
         for h in range(heads):
-            table = forget[:, width * h : width * (h + 1)]
-            columns[h] = jnp.concatenate([table] * 4, axis=0).T
-
-    here = pl.ds(pl.multiple_of(group * step, group), group)
-    for h in range(heads):
-        near = pltpu.roll(columns[h], lax.rem(4 * count - group * step, 4 * count), axis=1)
-        values = value[here, width * h : width * (h + 1)]
-        for j in range(group):
-            keep = jnp.broadcast_to(near[:, j : j + 1], (width, width))
-            added = values[j : j + 1, :]
-            new[j, h] = added + keep * (past[j, h] - added)
+            near = columns[h]
+            for j in range(8 * i, 8 * (i + 1)):
+                keep = jnp.broadcast_to(near[:, j : j + 1], (width, width))
+                added = value[j : j + 1, width * h : width * (h + 1)]
+                states[j, h] = added + keep * (states[j, h] - added)
+        leaving[i].start()
+    for copy in leaving:
+        copy.wait()
 
 
 def update_state(forget, value, past):
     count, heads, width, _ = past.shape
-    group = 8
-    block = pl.BlockSpec((group, heads, width, width), lambda i: (i, 0, 0, 0))
-    whole = pl.BlockSpec(forget.shape, lambda i: (0, 0))
+    whole = pl.BlockSpec(forget.shape, lambda: (0, 0))
+    sems = pltpu.SemaphoreType.DMA((count // 8,))
     return pl.pallas_call(
         state_body,
-        grid=(count // group,),
-        in_specs=[whole, whole, block],
-        out_specs=block,
+        in_specs=[whole, whole, pl.BlockSpec(memory_space=pl.ANY)],
+        out_specs=pl.BlockSpec(memory_space=pl.ANY),
         out_shape=jax.ShapeDtypeStruct(past.shape, f32),
-        scratch_shapes=[pltpu.VMEM((heads, width, 4 * count), f32)],
+        scratch_shapes=[
+            pltpu.VMEM((heads, width, width), f32),
+            pltpu.VMEM(past.shape, f32),
+            sems,
+            sems,
+        ],
         compiler_params=pltpu.CompilerParams(vmem_limit_bytes=12 * 2**20),
         cost_estimate=pl.CostEstimate(
             flops=4 * 10**9, bytes_accessed=8 * 10**6, transcendentals=0
@@ -308,7 +318,8 @@
     )(forget, value, in_hbm(past))
 
 
-def project_body(place, gain, *refs):
+def project_body(gain, *refs):
+    place = lax.axis_index("x"), lax.axis_index("c")
     pieces, weights, (out, block) = refs[:4], refs[4:-2], refs[-2:]
     width, rows = pieces[0].shape[0] // 2, pieces[0].shape[1]
     for k, piece in enumerate(pieces):
@@ -330,28 +341,21 @@
     out[:, :, 1024:1152] = both.reshape(count, own, 128)
 
 
-def in_smem():
-    return pl.BlockSpec(memory_space=pltpu.SMEM)
-
-
-def place_on_tp():
-    return jnp.stack([lax.axis_index("x"), lax.axis_index("c")]).astype(jnp.int32)
-
-
 def project(pieces, gain, weights, own_rows):
     rows, width = pieces[0].shape[1], gain.shape[0]
     operands = [jnp.broadcast_to(gain[:, None], (width, 128)), *pieces, *weights]
     return pl.pallas_call(
         project_body,
-        in_specs=[in_smem()] + [pl.BlockSpec(v.shape, lambda: (0, 0)) for v in operands],
+        in_specs=[pl.BlockSpec(v.shape, lambda: (0, 0)) for v in operands],
         out_shape=jax.ShapeDtypeStruct((rows // own_rows, own_rows, 4 * width + 128), bf16),
         scratch_shapes=[pltpu.VMEM((width, rows), bf16)],
         compiler_params=pltpu.CompilerParams(vmem_limit_bytes=14 * 2**20),
         name="project",
-    )(place_on_tp(), *operands)
-
-
-def output_body(place, gathered, weight, mine, theirs, block):
+    )(*operands)
+
+
+def output_body(gathered, weight, mine, theirs, block):
+    place = lax.axis_index("x"), lax.axis_index("c")
     width = mine.shape[1]
     block[...] = lax.dot_general(
         weight[...].T, gathered[...], (((1,), (1,)), ((), ())), preferred_element_type=f32
@@ -368,12 +372,12 @@
     shape = jax.ShapeDtypeStruct((4, width // 8, rows), bf16)
     return pl.pallas_call(
         output_body,
-        in_specs=[in_smem()] + [pl.BlockSpec(v.shape, lambda: (0, 0)) for v in (gathered, weight)],
+        in_specs=[pl.BlockSpec(v.shape, lambda: (0, 0)) for v in (gathered, weight)],
         out_shape=[shape, shape],
         scratch_shapes=[pltpu.VMEM((width, rows), f32)],
         compiler_params=pltpu.CompilerParams(vmem_limit_bytes=10 * 2**20),
         name="output",
-    )(place_on_tp(), gathered, weight)
+    )(gathered, weight)
 
 
 def half_step(own, near_w, far_w, gains, near):

time: 201 us -> 198 us (0.985)
  Pallas kernels: 26.2 us -> 22.1 us
    pallas_call x4, Pallas kernels: 12.9 us -> 8.75 us  [the longest x1 3.75 us: update_state(): pl.pallas_call(state_body, in_specs=[whole, whole, pl.BlockSpec(memory_sp...]
    all_to_all x1, waiting for transfers between devices: 2.71 us -> 4.88 us  [copy_for_each(): return lax.all_to_all(copies, axes, split_axis=0, concat_axis=0, tiled=True)]
  transfers between devices with their start and end apart: 33 -> 33, of which waited for: 25 -> 24; matrix products, arithmetic and copies ran while one was open for 1% -> 0% of each run, Pallas kernels for 9% -> 8%
where the time goes in v1:
time: 198 us; the launch traced here: 197 us
  waiting for transfers between devices  64.3 us (32%)
  starting transfers between devices  56.4 us (28%)
  blocking collectives  42.8 us (22%)
  Pallas kernels  22.1 us (11%)
  local copies, waits for them, and re-layouts  5.58 us (3%)
  matrix products  2.79 us (1%)
    all_to_all x3, blocking collectives, plane_exchange(): lax.all_to_all(pieces, ALL, split_axis=0, concat_axis=0, axis_index_group...  42.8 us
    ppermute x18, starting transfers between devices, shift(): return lax.ppermute(value, ALL, pairs)  32.6 us
    ppermute x18, waiting for transfers between devices, shift(): return lax.ppermute(value, ALL, pairs)  30.5 us
    all_to_all x1, waiting for transfers between devices, exchange(): return lax.all_to_all(pieces, axes, split_axis=0, concat_axis=0, tiled=True)  12.5 us
    pallas_call x2, Pallas kernels, order_weights(): pl.pallas_call(order_body, grid=(4,), in_specs=[whole, whole, pl.BlockSpe...  10.9 us
    all_to_all x1, starting transfers between devices, plane_exchange(): lax.all_to_all(pieces, ALL, split_axis=0, concat_axis=0, axis_index_group...  8.16 us
    ppermute x6, starting transfers between devices, shift_x(): return lax.ppermute(value, ALL, pairs)  7.76 us
    ppermute x6, waiting for transfers between devices, shift_x(): return lax.ppermute(value, ALL, pairs)  6.97 us
  transfers between devices with their start and end apart: 33, of which 24 were waited for; matrix products, arithmetic and copies ran while one was open for 0% of the time, Pallas kernels for 8%

profile of v1, /device:TPU:0, one launch (start us, length us, event | category | flops | bytes accessed | tf_op | source)
XLA Modules:
  0.0 196.8 jit_solution(3280119366224872200)
XLA Ops:
  2.3 8.2 %all-to-all-start = ((bf16[16,32,512]{2,1,0:T(8,128)(2,1)}), bf16[16,32,512]{2,1,0:T(8,128)(2,1)S(1)}, u32[]{:S(2)}, u32[]{:S(2)}) async-start(bf16[16,32,512]{2,1,0:T(8,128)(2,1)} %broadcast_in_dim.8), calls=%async_computation | async-start | bytes 1048576 | tf_op jit(solution)/shard_map/all_to_all | solution.py:58
  10.5 5.4 %order.2 = (bf16[4,3,96,512]{3,2,1,0:T(8,128)(2,1)S(1)}, bf16[4,3,96,512]{3,2,1,0:T(8,128)(2,1)S(1)}, f32[4,512,128]{2,1,0:T(8,128)S(1)}) custom-call(s32[1,512]{1,0:T(1,128)S(1)} %get-tuple-element.85.mine, s32[1,512]{1,0:T(1,128)S(1)} %get-tuple-element.86.theirs, f32[4,1,1024]{2,1,0:T(1,128)S(1)} %bitcast.72, bf16[88,4096]{1,0:T(8,128)(2,1)} %bitcast.80, ...), custom_call_target="tpu_custom_call" | custom-call | flops 5000000000 | bytes 6000000 | tf_op jit(solution)/shard_map/order/pallas_call | solution.py:119
  17.0 3.6 %all-to-all-done = bf16[16,32,512]{2,1,0:T(8,128)(2,1)S(1)} async-done(((bf16[16,32,512]{2,1,0:T(8,128)(2,1)}), bf16[16,32,512]{2,1,0:T(8,128)(2,1)S(1)}, u32[]{:S(2)}, u32[]{:S(2)}) %all-to-all-start) | async-done | bytes 524320 | tf_op jit(solution)/shard_map/all_to_all | solution.py:58
  32.6 3.5 %collective-permute-done.3.refs_0_ = bf16[256,512]{1,0:T(8,128)(2,1)S(1)} collective-permute-done((bf16[256,512]{1,0:T(8,128)(2,1)S(1)}, bf16[256,512]{1,0:T(8,128)(2,1)S(1)}, u32[]{:S(2)}, u32[]{:S(2)}) %collective-permute-start.3) | collective-permute-done | bytes 262176 | tf_op jit(solution)/shard_map/ppermute | solution.py:49
  40.1 3.0 %collective-permute-start.8 = (bf16[512,512]{1,0:T(8,128)(2,1)S(1)}, bf16[512,512]{1,0:T(8,128)(2,1)S(1)}, u32[]{:S(2)}, u32[]{:S(2)}) collective-permute-start(bf16[512,512]{1,0:T(8,128)(2,1)S(1)} %convolution_convert_fusion.6), channel_id=1, source_target_pairs={{0,4},{1,17},{2,6},{3,19},{4,0},{5,21},{6,2},{7,23},{8,12},{9,25},... | collective-permute-start | bytes 1572872 | tf_op jit(solution)/shard_map/ppermute | solution.py:49
  46.3 4.6 %collective-permute-done.8 = bf16[512,512]{1,0:T(8,128)(2,1)S(1)} collective-permute-done((bf16[512,512]{1,0:T(8,128)(2,1)S(1)}, bf16[512,512]{1,0:T(8,128)(2,1)S(1)}, u32[]{:S(2)}, u32[]{:S(2)}) %collective-permute-start.8) | collective-permute-done | bytes 524320 | tf_op jit(solution)/shard_map/ppermute | solution.py:49
  50.9 5.5 %collective-permute-done.9 = bf16[512,512]{1,0:T(8,128)(2,1)S(1)} collective-permute-done((bf16[512,512]{1,0:T(8,128)(2,1)S(1)}, bf16[512,512]{1,0:T(8,128)(2,1)S(1)}, u32[]{:S(2)}, u32[]{:S(2)}) %collective-permute-start.9) | collective-permute-done | bytes 524320 | tf_op jit(solution)/shard_map/ppermute | solution.py:49
  57.3 15.0 %all_to_all.30 = bf16[16,32,512]{2,1,0:T(8,128)(2,1)S(1)} all-to-all(bf16[16,32,512]{2,1,0:T(8,128)(2,1)S(1)} %bitcast.74), channel_id=1, replica_groups={{0,8,16,24,32,40,48,56,64,72,80,88,96,104,112,120},{2,10,18,26,34,42,50..., dimensions={0} | all-to-all | bytes 1048576 | tf_op jit(solution)/shard_map/all_to_all | solution.py:58
  79.4 3.0 %collective-permute-done.13.refs_2_ = bf16[64,512]{1,0:T(8,128)(2,1)S(1)} collective-permute-done((bf16[64,512]{1,0:T(8,128)(2,1)S(1)}, bf16[64,512]{1,0:T(8,128)(2,1)S(1)}, u32[]{:S(2)}, u32[]{:S(2)}) %collective-permute-start.13) | collective-permute-done | bytes 65568 | tf_op jit(solution)/shard_map/ppermute | solution.py:54
  84.7 4.0 %all-to-all-start.2 = ((bf16[16,32,1152]{2,1,0:T(8,128)(2,1)}), bf16[16,32,1152]{2,1,0:T(8,128)(2,1)S(1)}, u32[]{:S(2)}, u32[]{:S(2)}) async-start(bf16[16,32,1152]{2,1,0:T(8,128)(2,1)} %project.1), calls=%async_computation.2 | async-start | bytes 2359296 | tf_op jit(solution)/shard_map/all_to_all | solution.py:27
  88.8 5.4 %order.3 = (bf16[4,3,96,512]{3,2,1,0:T(8,128)(2,1)S(1)}, bf16[4,3,96,512]{3,2,1,0:T(8,128)(2,1)S(1)}, f32[4,512,128]{2,1,0:T(8,128)S(1)}) custom-call(s32[1,512]{1,0:T(1,128)S(1)} %get-tuple-element.85.mine, s32[1,512]{1,0:T(1,128)S(1)} %get-tuple-element.86.theirs, f32[4,1,1024]{2,1,0:T(1,128)S(1)} %bitcast.73, bf16[88,4096]{1,0:T(8,128)(2,1)} %bitcast.82, ...), custom_call_target="tpu_custom_call" | custom-call | flops 5000000000 | bytes 6000000 | tf_op jit(solution)/shard_map/order/pallas_call | solution.py:119
  95.3 12.5 %all-to-all-done.2.arrived = bf16[16,32,1152]{2,1,0:T(8,128)(2,1)S(1)} async-done(((bf16[16,32,1152]{2,1,0:T(8,128)(2,1)}), bf16[16,32,1152]{2,1,0:T(8,128)(2,1)S(1)}, u32[]{:S(2)}, u32[]{:S(2)}) %all-to-all-start.2) | async-done | bytes 1179680 | tf_op jit(solution)/shard_map/all_to_all | solution.py:27
  107.8 3.2 %readout.1 = (bf16[32,256]{1,0:T(8,128)(2,1)S(1)}, f32[32,256]{1,0:T(8,128)S(1)}, f32[32,256]{1,0:T(8,128)S(1)}) custom-call(bf16[16,32,1152]{2,1,0:T(8,128)(2,1)S(1)} %all-to-all-done.2.arrived, f32[32,2,128,128]{3,2,1,0:T(8,128)} %past.3, f32[1,256]{1,0:T(1,128)S(1)} %bitcast.70, f32[1,128]{1,0:T(1,128)S(1)} %bitcast.71), custom_call_target="tpu_custom_call" | custom-call | tf_op jit(solution)/shard_map/readout/pallas_call | solution.py:256
  111.7 3.5 %all-to-all-start.3 = ((bf16[16,32,256]{2,1,0:T(8,128)(2,1)}), bf16[16,32,256]{2,1,0:T(8,128)(2,1)S(1)}, u32[]{:S(2)}, u32[]{:S(2)}) async-start(bf16[16,32,256]{2,1,0:T(8,128)(2,1)} %broadcast_in_dim.19), calls=%async_computation.3 | async-start | bytes 524288 | tf_op jit(solution)/shard_map/all_to_all | solution.py:23
  115.3 3.8 %state.1 = f32[32,2,128,128]{3,2,1,0:T(8,128)} custom-call(f32[32,256]{1,0:T(8,128)S(1)} %get-tuple-element.54.forget, f32[32,256]{1,0:T(8,128)S(1)} %get-tuple-element.55.value, f32[32,2,128,128]{3,2,1,0:T(8,128)} %past.3), custom_call_target="tpu_custom_call" | custom-call | flops 4000000000 | bytes 8000000 | tf_op jit(solution)/shard_map/state/pallas_call | solution.py:302
  119.0 4.9 %all-to-all-done.3 = bf16[16,32,256]{2,1,0:T(8,128)(2,1)S(1)} async-done(((bf16[16,32,256]{2,1,0:T(8,128)(2,1)}), bf16[16,32,256]{2,1,0:T(8,128)(2,1)S(1)}, u32[]{:S(2)}, u32[]{:S(2)}) %all-to-all-start.3) | async-done | bytes 262176 | tf_op jit(solution)/shard_map/all_to_all | solution.py:23
  126.7 3.2 %collective-permute-start.18 = (bf16[32,512]{1,0:T(8,128)(2,1)S(1)}, bf16[32,512]{1,0:T(8,128)(2,1)S(1)}, u32[]{:S(2)}, u32[]{:S(2)}) collective-permute-start(bf16[32,512]{1,0:T(8,128)(2,1)S(1)} %get-tuple-element.79), channel_id=1, source_target_pairs={{0,6},{1,7},{2,0},{3,1},{4,2},{5,3},{6,4},{7,5},{8,14},{9,15},{10,... | collective-permute-start | bytes 98312 | tf_op jit(solution)/shard_map/ppermute | solution.py:54
  131.9 13.3 %all_to_all.31 = bf16[16,32,512]{2,1,0:T(8,128)(2,1)S(1)} all-to-all(bf16[16,32,512]{2,1,0:T(8,128)(2,1)S(1)} %broadcast_in_dim.20), channel_id=1, replica_groups={{0,8,16,24,32,40,48,56,64,72,80,88,96,104,112,120},{2,10,18,26,34,42,50..., dimensions={0} | all-to-all | bytes 1048576 | tf_op jit(solution)/shard_map/all_to_all | solution.py:58
  148.5 3.2 %collective-permute-start.25 = (bf16[256,512]{1,0:T(8,128)(2,1)S(1)}, bf16[256,512]{1,0:T(8,128)(2,1)S(1)}, u32[]{:S(2)}, u32[]{:S(2)}) collective-permute-start(bf16[256,512]{1,0:T(8,128)(2,1)S(1)} %get-tuple-element.75), channel_id=1, source_target_pairs={{0,6},{1,25},{2,0},{3,27},{4,2},{5,29},{6,4},{7,31},{8,14},{9,1},{... | collective-permute-start | bytes 786440 | tf_op jit(solution)/shard_map/ppermute | solution.py:49
  156.9 3.5 %collective-permute-done.22.refs_0_ = bf16[256,512]{1,0:T(8,128)(2,1)S(1)} collective-permute-done((bf16[256,512]{1,0:T(8,128)(2,1)S(1)}, bf16[256,512]{1,0:T(8,128)(2,1)S(1)}, u32[]{:S(2)}, u32[]{:S(2)}) %collective-permute-start.22) | collective-permute-done | bytes 262176 | tf_op jit(solution)/shard_map/ppermute | solution.py:49
  164.1 3.6 %collective-permute-start.27 = (bf16[512,512]{1,0:T(8,128)(2,1)S(1)}, bf16[512,512]{1,0:T(8,128)(2,1)S(1)}, u32[]{:S(2)}, u32[]{:S(2)}) collective-permute-start(bf16[512,512]{1,0:T(8,128)(2,1)S(1)} %convolution_convert_fusion.2), channel_id=1, source_target_pairs={{0,4},{1,17},{2,6},{3,19},{4,0},{5,21},{6,2},{7,23},{8,12},{9,25},... | collective-permute-start | bytes 1572872 | tf_op jit(solution)/shard_map/ppermute | solution.py:49
  170.9 4.1 %collective-permute-done.27 = bf16[512,512]{1,0:T(8,128)(2,1)S(1)} collective-permute-done((bf16[512,512]{1,0:T(8,128)(2,1)S(1)}, bf16[512,512]{1,0:T(8,128)(2,1)S(1)}, u32[]{:S(2)}, u32[]{:S(2)}) %collective-permute-start.27) | collective-permute-done | bytes 524320 | tf_op jit(solution)/shard_map/ppermute | solution.py:49
  174.9 5.5 %collective-permute-done.28 = bf16[512,512]{1,0:T(8,128)(2,1)S(1)} collective-permute-done((bf16[512,512]{1,0:T(8,128)(2,1)S(1)}, bf16[512,512]{1,0:T(8,128)(2,1)S(1)}, u32[]{:S(2)}, u32[]{:S(2)}) %collective-permute-start.28) | collective-permute-done | bytes 524320 | tf_op jit(solution)/shard_map/ppermute | solution.py:49
  181.5 14.6 %all_to_all.32 = bf16[16,32,512]{2,1,0:T(8,128)(2,1)S(1)} all-to-all(bf16[16,32,512]{2,1,0:T(8,128)(2,1)S(1)} %bitcast.75), channel_id=1, replica_groups={{0,8,16,24,32,40,48,56,64,72,80,88,96,104,112,120},{2,10,18,26,34,42,50..., dimensions={0} | all-to-all | bytes 1048576 | tf_op jit(solution)/shard_map/all_to_all | solution.py:58
  (117 shorter events, 55.5 us)
Async XLA Ops:
  2.3 18.3 %all-to-all-start = ((bf16[16,32,512]{2,1,0:T(8,128)(2,1)}), bf16[16,32,512]{2,1,0:T(8,128)(2,1)S(1)}, u32[]{:S(2)}, u32[]{:S(2)}) async-start(bf16[16,32,512]{2,1,0:T(8,128)(2,1)} %broadcast_in_dim.8), calls=%async_computation | async-start | bytes 1048576 | tf_op jit(solution)/shard_map/all_to_all | solution.py:58
  20.6 8.0 %collective-permute-start.2 = (bf16[4,3,96,512]{3,2,1,0:T(8,128)(2,1)}, bf16[4,3,96,512]{3,2,1,0:T(8,128)(2,1)S(1)}, u32[]{:S(2)}, u32[]{:S(2)}) collective-permute-start(bf16[4,3,96,512]{3,2,1,0:T(8,128)(2,1)} %copy-done.9), channel_id=1, source_target_pairs={{0,1},{1,0},{2,3},{3,2},{4,5},{5,4},{6,7},{7,6},{8,9},{9,8},{10,11... | collective-permute-start | bytes 3538952 | tf_op jit(solution)/shard_map/ppermute | solution.py:31
  20.6 7.7 %collective-permute-start = (bf16[256,512]{1,0:T(8,128)(2,1)S(1)}, bf16[256,512]{1,0:T(8,128)(2,1)S(1)}, u32[]{:S(2)}, u32[]{:S(2)}) collective-permute-start(bf16[256,512]{1,0:T(8,128)(2,1)S(1)} %get-tuple-element.77), channel_id=1, source_target_pairs={{0,2},{1,9},{2,4},{3,11},{4,6},{5,13},{6,0},{7,15},{8,10},{9,17},{... | collective-permute-start | bytes 786440 | tf_op jit(solution)/shard_map/ppermute | solution.py:49
  22.2 6.4 %collective-permute-start.1 = (bf16[256,512]{1,0:T(8,128)(2,1)S(1)}, bf16[256,512]{1,0:T(8,128)(2,1)S(1)}, u32[]{:S(2)}, u32[]{:S(2)}) collective-permute-start(bf16[256,512]{1,0:T(8,128)(2,1)S(1)} %get-tuple-element.76), channel_id=1, source_target_pairs={{0,6},{1,25},{2,0},{3,27},{4,2},{5,29},{6,4},{7,31},{8,14},{9,1},{... | collective-permute-start | bytes 786440 | tf_op jit(solution)/shard_map/ppermute | solution.py:49
  23.9 7.9 %collective-permute-start.5 = (bf16[256,512]{1,0:T(8,128)(2,1)S(1)}, bf16[256,512]{1,0:T(8,128)(2,1)S(1)}, u32[]{:S(2)}, u32[]{:S(2)}) collective-permute-start(bf16[256,512]{1,0:T(8,128)(2,1)S(1)} %get-tuple-element.76), channel_id=1, source_target_pairs={{0,2},{1,9},{2,4},{3,11},{4,6},{5,13},{6,0},{7,15},{8,10},{9,17},{... | collective-permute-start | bytes 786440 | tf_op jit(solution)/shard_map/ppermute | solution.py:49
  24.2 7.6 %collective-permute-start.6 = (bf16[256,512]{1,0:T(8,128)(2,1)S(1)}, bf16[256,512]{1,0:T(8,128)(2,1)S(1)}, u32[]{:S(2)}, u32[]{:S(2)}) collective-permute-start(bf16[256,512]{1,0:T(8,128)(2,1)S(1)} %get-tuple-element.77), channel_id=1, source_target_pairs={{0,6},{1,25},{2,0},{3,27},{4,2},{5,29},{6,4},{7,31},{8,14},{9,1},{... | collective-permute-start | bytes 786440 | tf_op jit(solution)/shard_map/ppermute | solution.py:49
  28.5 7.6 %collective-permute-start.3 = (bf16[256,512]{1,0:T(8,128)(2,1)S(1)}, bf16[256,512]{1,0:T(8,128)(2,1)S(1)}, u32[]{:S(2)}, u32[]{:S(2)}) collective-permute-start(bf16[256,512]{1,0:T(8,128)(2,1)S(1)} %collective-permute-done.refs_1_), channel_id=1, source_target_pairs={{0,2},{1,9},{2,4},{3,11},{4,6},{5,13},{6,0},{7,15},{8,10},{9,17},{... | collective-permute-start | bytes 786440 | tf_op jit(solution)/shard_map/ppermute | solution.py:49
  30.0 6.4 %collective-permute-start.4 = (bf16[256,512]{1,0:T(8,128)(2,1)S(1)}, bf16[256,512]{1,0:T(8,128)(2,1)S(1)}, u32[]{:S(2)}, u32[]{:S(2)}) collective-permute-start(bf16[256,512]{1,0:T(8,128)(2,1)S(1)} %collective-permute-done.1.refs_2_), channel_id=1, source_target_pairs={{0,6},{1,25},{2,0},{3,27},{4,2},{5,29},{6,4},{7,31},{8,14},{9,1},{... | collective-permute-start | bytes 786440 | tf_op jit(solution)/shard_map/ppermute | solution.py:49
  40.1 10.9 %collective-permute-start.8 = (bf16[512,512]{1,0:T(8,128)(2,1)S(1)}, bf16[512,512]{1,0:T(8,128)(2,1)S(1)}, u32[]{:S(2)}, u32[]{:S(2)}) collective-permute-start(bf16[512,512]{1,0:T(8,128)(2,1)S(1)} %convolution_convert_fusion.6), channel_id=1, source_target_pairs={{0,4},{1,17},{2,6},{3,19},{4,0},{5,21},{6,2},{7,23},{8,12},{9,25},... | collective-permute-start | bytes 1572872 | tf_op jit(solution)/shard_map/ppermute | solution.py:49
  43.1 13.4 %collective-permute-start.9 = (bf16[512,512]{1,0:T(8,128)(2,1)S(1)}, bf16[512,512]{1,0:T(8,128)(2,1)S(1)}, u32[]{:S(2)}, u32[]{:S(2)}) collective-permute-start(bf16[512,512]{1,0:T(8,128)(2,1)S(1)} %convolution_convert_fusion.5), channel_id=1, source_target_pairs={{0,2},{1,9},{2,4},{3,11},{4,6},{5,13},{6,0},{7,15},{8,10},{9,17},{... | collective-permute-start | bytes 1572872 | tf_op jit(solution)/shard_map/ppermute | solution.py:49
  44.0 12.8 %collective-permute-start.10 = (bf16[512,512]{1,0:T(8,128)(2,1)S(1)}, bf16[512,512]{1,0:T(8,128)(2,1)S(1)}, u32[]{:S(2)}, u32[]{:S(2)}) collective-permute-start(bf16[512,512]{1,0:T(8,128)(2,1)S(1)} %convolution_convert_fusion.4), channel_id=1, source_target_pairs={{0,6},{1,25},{2,0},{3,27},{4,2},{5,29},{6,4},{7,31},{8,14},{9,1},{... | collective-permute-start | bytes 1572872 | tf_op jit(solution)/shard_map/ppermute | solution.py:49
  76.8 6.2 %collective-permute-start.14 = (bf16[64,512]{1,0:T(8,128)(2,1)S(1)}, bf16[64,512]{1,0:T(8,128)(2,1)S(1)}, u32[]{:S(2)}, u32[]{:S(2)}) collective-permute-start(bf16[64,512]{1,0:T(8,128)(2,1)S(1)} %pad_maximum_fusion.4.refs_0_), channel_id=1, source_target_pairs={{0,2},{1,3},{2,4},{3,5},{4,6},{5,7},{6,0},{7,1},{8,10},{9,11},{10,... | collective-permute-start | bytes 196616 | tf_op jit(solution)/shard_map/ppermute | solution.py:54
  84.7 23.1 %all-to-all-start.2 = ((bf16[16,32,1152]{2,1,0:T(8,128)(2,1)}), bf16[16,32,1152]{2,1,0:T(8,128)(2,1)S(1)}, u32[]{:S(2)}, u32[]{:S(2)}) async-start(bf16[16,32,1152]{2,1,0:T(8,128)(2,1)} %project.1), calls=%async_computation.2 | async-start | bytes 2359296 | tf_op jit(solution)/shard_map/all_to_all | solution.py:27
  111.7 12.2 %all-to-all-start.3 = ((bf16[16,32,256]{2,1,0:T(8,128)(2,1)}), bf16[16,32,256]{2,1,0:T(8,128)(2,1)S(1)}, u32[]{:S(2)}, u32[]{:S(2)}) async-start(bf16[16,32,256]{2,1,0:T(8,128)(2,1)} %broadcast_in_dim.19), calls=%async_computation.3 | async-start | bytes 524288 | tf_op jit(solution)/shard_map/all_to_all | solution.py:23
  145.1 7.7 %collective-permute-start.21 = (bf16[4,3,96,512]{3,2,1,0:T(8,128)(2,1)S(1)}, bf16[4,3,96,512]{3,2,1,0:T(8,128)(2,1)S(1)}, u32[]{:S(2)}, u32[]{:S(2)}) collective-permute-start(bf16[4,3,96,512]{3,2,1,0:T(8,128)(2,1)S(1)} %copy-done.8), channel_id=1, source_target_pairs={{0,1},{1,0},{2,3},{3,2},{4,5},{5,4},{6,7},{7,6},{8,9},{9,8},{10,11... | collective-permute-start | bytes 3538952 | tf_op jit(solution)/shard_map/ppermute | solution.py:31
  145.2 7.7 %collective-permute-start.19 = (bf16[256,512]{1,0:T(8,128)(2,1)S(1)}, bf16[256,512]{1,0:T(8,128)(2,1)S(1)}, u32[]{:S(2)}, u32[]{:S(2)}) collective-permute-start(bf16[256,512]{1,0:T(8,128)(2,1)S(1)} %get-tuple-element.75), channel_id=1, source_target_pairs={{0,2},{1,9},{2,4},{3,11},{4,6},{5,13},{6,0},{7,15},{8,10},{9,17},{... | collective-permute-start | bytes 786440 | tf_op jit(solution)/shard_map/ppermute | solution.py:49
  146.4 6.4 %collective-permute-start.20 = (bf16[256,512]{1,0:T(8,128)(2,1)S(1)}, bf16[256,512]{1,0:T(8,128)(2,1)S(1)}, u32[]{:S(2)}, u32[]{:S(2)}) collective-permute-start(bf16[256,512]{1,0:T(8,128)(2,1)S(1)} %get-tuple-element.74), channel_id=1, source_target_pairs={{0,6},{1,25},{2,0},{3,27},{4,2},{5,29},{6,4},{7,31},{8,14},{9,1},{... | collective-permute-start | bytes 786440 | tf_op jit(solution)/shard_map/ppermute | solution.py:49
  148.5 7.6 %collective-permute-start.24 = (bf16[256,512]{1,0:T(8,128)(2,1)S(1)}, bf16[256,512]{1,0:T(8,128)(2,1)S(1)}, u32[]{:S(2)}, u32[]{:S(2)}) collective-permute-start(bf16[256,512]{1,0:T(8,128)(2,1)S(1)} %get-tuple-element.74), channel_id=1, source_target_pairs={{0,2},{1,9},{2,4},{3,11},{4,6},{5,13},{6,0},{7,15},{8,10},{9,17},{... | collective-permute-start | bytes 786440 | tf_op jit(solution)/shard_map/ppermute | solution.py:49
  148.5 7.6 %collective-permute-start.25 = (bf16[256,512]{1,0:T(8,128)(2,1)S(1)}, bf16[256,512]{1,0:T(8,128)(2,1)S(1)}, u32[]{:S(2)}, u32[]{:S(2)}) collective-permute-start(bf16[256,512]{1,0:T(8,128)(2,1)S(1)} %get-tuple-element.75), channel_id=1, source_target_pairs={{0,6},{1,25},{2,0},{3,27},{4,2},{5,29},{6,4},{7,31},{8,14},{9,1},{... | collective-permute-start | bytes 786440 | tf_op jit(solution)/shard_map/ppermute | solution.py:49
  152.8 7.6 %collective-permute-start.22 = (bf16[256,512]{1,0:T(8,128)(2,1)S(1)}, bf16[256,512]{1,0:T(8,128)(2,1)S(1)}, u32[]{:S(2)}, u32[]{:S(2)}) collective-permute-start(bf16[256,512]{1,0:T(8,128)(2,1)S(1)} %collective-permute-done.19.refs_1_), channel_id=1, source_target_pairs={{0,2},{1,9},{2,4},{3,11},{4,6},{5,13},{6,0},{7,15},{8,10},{9,17},{... | collective-permute-start | bytes 786440 | tf_op jit(solution)/shard_map/ppermute | solution.py:49
  154.0 6.4 %collective-permute-start.23 = (bf16[256,512]{1,0:T(8,128)(2,1)S(1)}, bf16[256,512]{1,0:T(8,128)(2,1)S(1)}, u32[]{:S(2)}, u32[]{:S(2)}) collective-permute-start(bf16[256,512]{1,0:T(8,128)(2,1)S(1)} %collective-permute-done.20.refs_2_), channel_id=1, source_target_pairs={{0,6},{1,25},{2,0},{3,27},{4,2},{5,29},{6,4},{7,31},{8,14},{9,1},{... | collective-permute-start | bytes 786440 | tf_op jit(solution)/shard_map/ppermute | solution.py:49
  164.1 10.9 %collective-permute-start.27 = (bf16[512,512]{1,0:T(8,128)(2,1)S(1)}, bf16[512,512]{1,0:T(8,128)(2,1)S(1)}, u32[]{:S(2)}, u32[]{:S(2)}) collective-permute-start(bf16[512,512]{1,0:T(8,128)(2,1)S(1)} %convolution_convert_fusion.2), channel_id=1, source_target_pairs={{0,4},{1,17},{2,6},{3,19},{4,0},{5,21},{6,2},{7,23},{8,12},{9,25},... | collective-permute-start | bytes 1572872 | tf_op jit(solution)/shard_map/ppermute | solution.py:49
  167.6 12.8 %collective-permute-start.28 = (bf16[512,512]{1,0:T(8,128)(2,1)S(1)}, bf16[512,512]{1,0:T(8,128)(2,1)S(1)}, u32[]{:S(2)}, u32[]{:S(2)}) collective-permute-start(bf16[512,512]{1,0:T(8,128)(2,1)S(1)} %convolution_convert_fusion.1), channel_id=1, source_target_pairs={{0,2},{1,9},{2,4},{3,11},{4,6},{5,13},{6,0},{7,15},{8,10},{9,17},{... | collective-permute-start | bytes 1572872 | tf_op jit(solution)/shard_map/ppermute | solution.py:49
  168.2 12.8 %collective-permute-start.29 = (bf16[512,512]{1,0:T(8,128)(2,1)S(1)}, bf16[512,512]{1,0:T(8,128)(2,1)S(1)}, u32[]{:S(2)}, u32[]{:S(2)}) collective-permute-start(bf16[512,512]{1,0:T(8,128)(2,1)S(1)} %convolution_convert_fusion), channel_id=1, source_target_pairs={{0,6},{1,25},{2,0},{3,27},{4,2},{5,29},{6,4},{7,31},{8,14},{9,1},{... | collective-permute-start | bytes 1572872 | tf_op jit(solution)/shard_map/ppermute | solution.py:49
  (22 other events, 234.9 us)

commit v2 on v1

--- a/solution.py
+++ b/solution.py
@@ -7,7 +7,6 @@
 from jax.experimental.pallas import tpu as pltpu
 from jax.sharding import Mesh
 from jax.sharding import PartitionSpec as P
-
 
 D = 4096
 ALL = ("z", "y", "x", "c")
@@ -128,7 +127,7 @@
             piece,
         ],
         out_specs=[side, side, pl.BlockSpec((4, 128, 128), lambda z: (0, z, 0))],
-        out_shape=[shape, shape, jax.ShapeDtypeStruct((4, 512, 128), f32)],
+        out_shape=[shape, pltpu.HBM(shape.shape, bf16), jax.ShapeDtypeStruct((4, 512, 128), f32)],
         scratch_shapes=[pltpu.VMEM((3 * PAD + 16, 1024), bf16), pltpu.VMEM((2, 1024, 512), bf16)],
         cost_estimate=pl.CostEstimate(flops=5 * 10**9, bytes_accessed=6 * 10**6, transcendentals=0),
         compiler_params=pltpu.CompilerParams(vmem_limit_bytes=20 * 2**20),
@@ -415,17 +414,26 @@
     )
     deep = jnp.concatenate([near_w[:, 2], far_w[:, 2]], axis=1)
 
-    sums, arrived = {}, []
-    for k in (2, 1, 3, 0):
-        sums[k] = lax.dot_general(
-            deep[k], hidden, (((0,), (0,)), ((), ())), preferred_element_type=f32
-        ).astype(bf16)
-        if k:
-            arrived.append(shift(sums[k], k))
-    total = sums[0].astype(f32)
-    for piece in arrived:
-        total = total + piece.astype(f32)
-    total = total.astype(bf16)
+    def sums(weights):
+        return lax.dot_general(
+            weights, hidden, (((0,), (0,)), ((), ())), preferred_element_type=f32
+        )
+
+    to_right = jnp.concatenate([deep[2][:, top], deep[1][:, low]], axis=1)
+    to_left = jnp.concatenate([deep[2][:, low], deep[3][:, top]], axis=1)
+    from_left = shift(sums(to_right).astype(bf16), 1)
+    from_right = shift(sums(to_left).astype(bf16), -1)
+    next_top, next_low = sums(deep[1][:, top]), sums(deep[3][:, low])
+    own_sums = sums(deep[0])
+    next_top = shift((next_top + from_left[top].astype(f32)).astype(bf16), 1)
+    next_low = shift((next_low + from_right[top].astype(f32)).astype(bf16), -1)
+    total = jnp.concatenate(
+        [
+            own_sums[top] + from_right[low].astype(f32) + next_top.astype(f32),
+            own_sums[low] + from_left[low].astype(f32) + next_low.astype(f32),
+        ],
+        axis=0,
+    ).astype(bf16)
     total = plane_exchange(total.reshape(16, width, rows)).astype(f32).sum(axis=0)
     return lax.optimization_barrier((own.astype(f32) + 0.5 * total).astype(bf16))
 

time: 198 us -> 202 us (1.020)
  waiting for transfers between devices: 64.3 us -> 69.7 us
  local copies, waits for them, and re-layouts: 5.58 us -> 3.55 us
    ppermute x18 -> x20, waiting for transfers between devices: 30.5 us -> 34.7 us  [shift(): return lax.ppermute(value, ALL, pairs)]
    unnamed x26 -> x22, local copies, waits for them, and re-layouts: 2.13 us -> 0.06 us
    ppermute x18 -> x20, starting transfers between devices: 32.6 us -> 31.5 us  [shift(): return lax.ppermute(value, ALL, pairs)]
  transfers between devices with their start and end apart: 33 -> 35, of which waited for: 24 -> 22; matrix products, arithmetic and copies ran while one was open for 0% -> 2% of each run, Pallas kernels for 8% -> 9%
where the time goes in v2:
time: 202 us; the launch traced here: 201 us
  waiting for transfers between devices  69.7 us (35%)
  starting transfers between devices  56.6 us (28%)
  blocking collectives  41.2 us (20%)
  Pallas kernels  23.4 us (12%)
  local copies, waits for them, and re-layouts  3.55 us (2%)
  matrix products  3 us (1%)
  other arithmetic  2.23 us (1%)
    all_to_all x3, blocking collectives, plane_exchange(): lax.all_to_all(pieces, ALL, split_axis=0, concat_axis=0, axis_index_group...  41.2 us
    ppermute x20, waiting for transfers between devices, shift(): return lax.ppermute(value, ALL, pairs)  34.7 us
    ppermute x20, starting transfers between devices, shift(): return lax.ppermute(value, ALL, pairs)  31.5 us
    pallas_call x2, Pallas kernels, order_weights(): pl.pallas_call(order_body, grid=(4,), in_specs=[whole, whole, pl.BlockSpe...  12.2 us
    all_to_all x1, waiting for transfers between devices, exchange(): return lax.all_to_all(pieces, axes, split_axis=0, concat_axis=0, tiled=True)  11.9 us
    ppermute x6, starting transfers between devices, shift_x(): return lax.ppermute(value, ALL, pairs)  9.05 us
    ppermute x6, waiting for transfers between devices, shift_x(): return lax.ppermute(value, ALL, pairs)  8.44 us
    all_to_all x1, starting transfers between devices, plane_exchange(): lax.all_to_all(pieces, ALL, split_axis=0, concat_axis=0, axis_index_group...  8.16 us
  transfers between devices with their start and end apart: 35, of which 22 were waited for; matrix products, arithmetic and copies ran while one was open for 2% of the time, Pallas kernels for 9%

profile of v2, /device:TPU:0, one launch (start us, length us, event | category | flops | bytes accessed | tf_op | source)
XLA Modules:
  0.0 201.0 jit_solution(1841489086753127729)
XLA Ops:
  2.3 8.2 %all-to-all-start = ((bf16[16,32,512]{2,1,0:T(8,128)(2,1)}), bf16[16,32,512]{2,1,0:T(8,128)(2,1)S(1)}, u32[]{:S(2)}, u32[]{:S(2)}) async-start(bf16[16,32,512]{2,1,0:T(8,128)(2,1)} %broadcast_in_dim.8), calls=%async_computation | async-start | bytes 1048576 | tf_op jit(solution)/shard_map/all_to_all | solution.py:57
  10.5 6.0 %order.2 = (bf16[4,3,96,512]{3,2,1,0:T(8,128)(2,1)S(1)}, bf16[4,3,96,512]{3,2,1,0:T(8,128)(2,1)}, f32[4,512,128]{2,1,0:T(8,128)S(1)}) custom-call(s32[1,512]{1,0:T(1,128)S(1)} %get-tuple-element.99.mine, s32[1,512]{1,0:T(1,128)S(1)} %get-tuple-element.100.theirs, f32[4,1,1024]{2,1,0:T(1,128)S(1)} %bitcast.62, bf16[88,4096]{1,0:T(8,128)(2,1)} %bitcast.70, ...), custom_call_target="tpu_custom_call" | custom-call | flops 5000000000 | bytes 6000000 | tf_op jit(solution)/shard_map/order/pallas_call | solution.py:118
  16.5 4.0 %all-to-all-done = bf16[16,32,512]{2,1,0:T(8,128)(2,1)S(1)} async-done(((bf16[16,32,512]{2,1,0:T(8,128)(2,1)}), bf16[16,32,512]{2,1,0:T(8,128)(2,1)S(1)}, u32[]{:S(2)}, u32[]{:S(2)}) %all-to-all-start) | async-done | bytes 524320 | tf_op jit(solution)/shard_map/all_to_all | solution.py:57
  27.3 3.7 %collective-permute-done.refs_1_ = bf16[256,512]{1,0:T(8,128)(2,1)S(1)} collective-permute-done((bf16[256,512]{1,0:T(8,128)(2,1)S(1)}, bf16[256,512]{1,0:T(8,128)(2,1)S(1)}, u32[]{:S(2)}, u32[]{:S(2)}) %collective-permute-start) | collective-permute-done | bytes 262176 | tf_op jit(solution)/shard_map/ppermute | solution.py:48
  35.2 3.5 %collective-permute-done.3.refs_0_ = bf16[256,512]{1,0:T(8,128)(2,1)S(1)} collective-permute-done((bf16[256,512]{1,0:T(8,128)(2,1)S(1)}, bf16[256,512]{1,0:T(8,128)(2,1)S(1)}, u32[]{:S(2)}, u32[]{:S(2)}) %collective-permute-start.3) | collective-permute-done | bytes 262176 | tf_op jit(solution)/shard_map/ppermute | solution.py:48
  42.0 3.3 %collective-permute-start.8 = (bf16[512,512]{1,0:T(8,128)(2,1)S(1)}, bf16[512,512]{1,0:T(8,128)(2,1)S(1)}, u32[]{:S(2)}, u32[]{:S(2)}) collective-permute-start(bf16[512,512]{1,0:T(8,128)(2,1)S(1)} %convolution_convert_fusion.3), channel_id=1, source_target_pairs={{0,6},{1,25},{2,0},{3,27},{4,2},{5,29},{6,4},{7,31},{8,14},{9,1},{... | collective-permute-start | bytes 1572872 | tf_op jit(solution)/shard_map/ppermute | solution.py:48
  45.3 6.7 %collective-permute-done.9 = bf16[512,512]{1,0:T(8,128)(2,1)S(1)} collective-permute-done((bf16[512,512]{1,0:T(8,128)(2,1)S(1)}, bf16[512,512]{1,0:T(8,128)(2,1)S(1)}, u32[]{:S(2)}, u32[]{:S(2)}) %collective-permute-start.9) | collective-permute-done | bytes 524320 | tf_op jit(solution)/shard_map/ppermute | solution.py:48
  52.7 3.4 %collective-permute-start.11 = (bf16[256,512]{1,0:T(8,128)(2,1)S(1)}, bf16[256,512]{1,0:T(8,128)(2,1)S(1)}, u32[]{:S(2)}, u32[]{:S(2)}) collective-permute-start(bf16[256,512]{1,0:T(8,128)(2,1)S(1)} %add_convert_fusion.2), channel_id=1, source_target_pairs={{0,6},{1,25},{2,0},{3,27},{4,2},{5,29},{6,4},{7,31},{8,14},{9,1},{... | collective-permute-start | bytes 786440 | tf_op jit(solution)/shard_map/ppermute | solution.py:48
  56.4 3.6 %collective-permute-done.10 = bf16[256,512]{1,0:T(8,128)(2,1)S(1)} collective-permute-done((bf16[256,512]{1,0:T(8,128)(2,1)S(1)}, bf16[256,512]{1,0:T(8,128)(2,1)S(1)}, u32[]{:S(2)}, u32[]{:S(2)}) %collective-permute-start.10) | collective-permute-done | bytes 262176 | tf_op jit(solution)/shard_map/ppermute | solution.py:48
  60.3 14.6 %all_to_all.30 = bf16[16,32,512]{2,1,0:T(8,128)(2,1)S(1)} all-to-all(bf16[16,32,512]{2,1,0:T(8,128)(2,1)S(1)} %bitcast.64), channel_id=1, replica_groups={{0,8,16,24,32,40,48,56,64,72,80,88,96,104,112,120},{2,10,18,26,34,42,50..., dimensions={0} | all-to-all | bytes 1048576 | tf_op jit(solution)/shard_map/all_to_all | solution.py:57
  76.9 4.5 %collective-permute-start.14 = (bf16[64,512]{1,0:T(8,128)(2,1)S(1)}, bf16[64,512]{1,0:T(8,128)(2,1)S(1)}, u32[]{:S(2)}, u32[]{:S(2)}) collective-permute-start(bf16[64,512]{1,0:T(8,128)(2,1)S(1)} %pad_maximum_fusion.6.refs_0_), channel_id=1, source_target_pairs={{0,4},{1,5},{2,6},{3,7},{4,0},{5,1},{6,2},{7,3},{8,12},{9,13},{10,... | collective-permute-start | bytes 196616 | tf_op jit(solution)/shard_map/ppermute | solution.py:53
  87.3 4.0 %all-to-all-start.2 = ((bf16[16,32,1152]{2,1,0:T(8,128)(2,1)}), bf16[16,32,1152]{2,1,0:T(8,128)(2,1)S(1)}, u32[]{:S(2)}, u32[]{:S(2)}) async-start(bf16[16,32,1152]{2,1,0:T(8,128)(2,1)} %project.1), calls=%async_computation.2 | async-start | bytes 2359296 | tf_op jit(solution)/shard_map/all_to_all | solution.py:26
  91.4 6.1 %order.3 = (bf16[4,3,96,512]{3,2,1,0:T(8,128)(2,1)S(1)}, bf16[4,3,96,512]{3,2,1,0:T(8,128)(2,1)}, f32[4,512,128]{2,1,0:T(8,128)S(1)}) custom-call(s32[1,512]{1,0:T(1,128)S(1)} %get-tuple-element.99.mine, s32[1,512]{1,0:T(1,128)S(1)} %get-tuple-element.100.theirs, f32[4,1,1024]{2,1,0:T(1,128)S(1)} %bitcast.63, bf16[88,4096]{1,0:T(8,128)(2,1)} %bitcast.72, ...), custom_call_target="tpu_custom_call" | custom-call | flops 5000000000 | bytes 6000000 | tf_op jit(solution)/shard_map/order/pallas_call | solution.py:118
  97.5 11.9 %all-to-all-done.2.arrived = bf16[16,32,1152]{2,1,0:T(8,128)(2,1)S(1)} async-done(((bf16[16,32,1152]{2,1,0:T(8,128)(2,1)}), bf16[16,32,1152]{2,1,0:T(8,128)(2,1)S(1)}, u32[]{:S(2)}, u32[]{:S(2)}) %all-to-all-start.2) | async-done | bytes 1179680 | tf_op jit(solution)/shard_map/all_to_all | solution.py:26
  113.3 3.5 %all-to-all-start.3 = ((bf16[16,32,256]{2,1,0:T(8,128)(2,1)}), bf16[16,32,256]{2,1,0:T(8,128)(2,1)S(1)}, u32[]{:S(2)}, u32[]{:S(2)}) async-start(bf16[16,32,256]{2,1,0:T(8,128)(2,1)} %broadcast_in_dim.19), calls=%async_computation.3 | async-start | bytes 524288 | tf_op jit(solution)/shard_map/all_to_all | solution.py:22
  116.9 3.8 %state.1 = f32[32,2,128,128]{3,2,1,0:T(8,128)} custom-call(f32[32,256]{1,0:T(8,128)S(1)} %get-tuple-element.54.forget, f32[32,256]{1,0:T(8,128)S(1)} %get-tuple-element.55.value, f32[32,2,128,128]{3,2,1,0:T(8,128)} %past.3), custom_call_target="tpu_custom_call" | custom-call | flops 4000000000 | bytes 8000000 | tf_op jit(solution)/shard_map/state/pallas_call | solution.py:301
  120.6 4.9 %all-to-all-done.3 = bf16[16,32,256]{2,1,0:T(8,128)(2,1)S(1)} async-done(((bf16[16,32,256]{2,1,0:T(8,128)(2,1)}), bf16[16,32,256]{2,1,0:T(8,128)(2,1)S(1)}, u32[]{:S(2)}, u32[]{:S(2)}) %all-to-all-start.3) | async-done | bytes 262176 | tf_op jit(solution)/shard_map/all_to_all | solution.py:22
  136.2 13.0 %all_to_all.31 = bf16[16,32,512]{2,1,0:T(8,128)(2,1)S(1)} all-to-all(bf16[16,32,512]{2,1,0:T(8,128)(2,1)S(1)} %broadcast_in_dim.20), channel_id=1, replica_groups={{0,8,16,24,32,40,48,56,64,72,80,88,96,104,112,120},{2,10,18,26,34,42,50..., dimensions={0} | all-to-all | bytes 1048576 | tf_op jit(solution)/shard_map/all_to_all | solution.py:57
  161.6 3.5 %collective-permute-done.23.refs_0_ = bf16[256,512]{1,0:T(8,128)(2,1)S(1)} collective-permute-done((bf16[256,512]{1,0:T(8,128)(2,1)S(1)}, bf16[256,512]{1,0:T(8,128)(2,1)S(1)}, u32[]{:S(2)}, u32[]{:S(2)}) %collective-permute-start.23) | collective-permute-done | bytes 262176 | tf_op jit(solution)/shard_map/ppermute | solution.py:48
  168.5 3.3 %collective-permute-start.28 = (bf16[512,512]{1,0:T(8,128)(2,1)S(1)}, bf16[512,512]{1,0:T(8,128)(2,1)S(1)}, u32[]{:S(2)}, u32[]{:S(2)}) collective-permute-start(bf16[512,512]{1,0:T(8,128)(2,1)S(1)} %convolution_convert_fusion.1), channel_id=1, source_target_pairs={{0,6},{1,25},{2,0},{3,27},{4,2},{5,29},{6,4},{7,31},{8,14},{9,1},{... | collective-permute-start | bytes 1572872 | tf_op jit(solution)/shard_map/ppermute | solution.py:48
  171.8 6.7 %collective-permute-done.29 = bf16[512,512]{1,0:T(8,128)(2,1)S(1)} collective-permute-done((bf16[512,512]{1,0:T(8,128)(2,1)S(1)}, bf16[512,512]{1,0:T(8,128)(2,1)S(1)}, u32[]{:S(2)}, u32[]{:S(2)}) %collective-permute-start.29) | collective-permute-done | bytes 524320 | tf_op jit(solution)/shard_map/ppermute | solution.py:48
  179.1 3.4 %collective-permute-start.31 = (bf16[256,512]{1,0:T(8,128)(2,1)S(1)}, bf16[256,512]{1,0:T(8,128)(2,1)S(1)}, u32[]{:S(2)}, u32[]{:S(2)}) collective-permute-start(bf16[256,512]{1,0:T(8,128)(2,1)S(1)} %add_convert_fusion), channel_id=1, source_target_pairs={{0,6},{1,25},{2,0},{3,27},{4,2},{5,29},{6,4},{7,31},{8,14},{9,1},{... | collective-permute-start | bytes 786440 | tf_op jit(solution)/shard_map/ppermute | solution.py:48
  182.8 3.6 %collective-permute-done.30 = bf16[256,512]{1,0:T(8,128)(2,1)S(1)} collective-permute-done((bf16[256,512]{1,0:T(8,128)(2,1)S(1)}, bf16[256,512]{1,0:T(8,128)(2,1)S(1)}, u32[]{:S(2)}, u32[]{:S(2)}) %collective-permute-start.30) | collective-permute-done | bytes 262176 | tf_op jit(solution)/shard_map/ppermute | solution.py:48
  186.7 13.6 %all_to_all.32 = bf16[16,32,512]{2,1,0:T(8,128)(2,1)S(1)} all-to-all(bf16[16,32,512]{2,1,0:T(8,128)(2,1)S(1)} %bitcast.65), channel_id=1, replica_groups={{0,8,16,24,32,40,48,56,64,72,80,88,96,104,112,120},{2,10,18,26,34,42,50..., dimensions={0} | all-to-all | bytes 1048576 | tf_op jit(solution)/shard_map/all_to_all | solution.py:57
  (131 shorter events, 57.0 us)
Async XLA Ops:
  2.3 18.3 %all-to-all-start = ((bf16[16,32,512]{2,1,0:T(8,128)(2,1)}), bf16[16,32,512]{2,1,0:T(8,128)(2,1)S(1)}, u32[]{:S(2)}, u32[]{:S(2)}) async-start(bf16[16,32,512]{2,1,0:T(8,128)(2,1)} %broadcast_in_dim.8), calls=%async_computation | async-start | bytes 1048576 | tf_op jit(solution)/shard_map/all_to_all | solution.py:57
  20.6 10.5 %collective-permute-start.2 = (bf16[4,3,96,512]{3,2,1,0:T(8,128)(2,1)}, bf16[4,3,96,512]{3,2,1,0:T(8,128)(2,1)S(1)}, u32[]{:S(2)}, u32[]{:S(2)}) collective-permute-start(bf16[4,3,96,512]{3,2,1,0:T(8,128)(2,1)} %get-tuple-element.40), channel_id=1, source_target_pairs={{0,1},{1,0},{2,3},{3,2},{4,5},{5,4},{6,7},{7,6},{8,9},{9,8},{10,11... | collective-permute-start | bytes 3538952 | tf_op jit(solution)/shard_map/ppermute | solution.py:30
  23.4 7.6 %collective-permute-start = (bf16[256,512]{1,0:T(8,128)(2,1)S(1)}, bf16[256,512]{1,0:T(8,128)(2,1)S(1)}, u32[]{:S(2)}, u32[]{:S(2)}) collective-permute-start(bf16[256,512]{1,0:T(8,128)(2,1)S(1)} %get-tuple-element.87), channel_id=1, source_target_pairs={{0,2},{1,9},{2,4},{3,11},{4,6},{5,13},{6,0},{7,15},{8,10},{9,17},{... | collective-permute-start | bytes 786440 | tf_op jit(solution)/shard_map/ppermute | solution.py:48
  23.5 10.9 %collective-permute-start.5 = (bf16[256,512]{1,0:T(8,128)(2,1)S(1)}, bf16[256,512]{1,0:T(8,128)(2,1)S(1)}, u32[]{:S(2)}, u32[]{:S(2)}) collective-permute-start(bf16[256,512]{1,0:T(8,128)(2,1)S(1)} %get-tuple-element.86), channel_id=1, source_target_pairs={{0,2},{1,9},{2,4},{3,11},{4,6},{5,13},{6,0},{7,15},{8,10},{9,17},{... | collective-permute-start | bytes 786440 | tf_op jit(solution)/shard_map/ppermute | solution.py:48
  24.2 10.1 %collective-permute-start.6 = (bf16[256,512]{1,0:T(8,128)(2,1)S(1)}, bf16[256,512]{1,0:T(8,128)(2,1)S(1)}, u32[]{:S(2)}, u32[]{:S(2)}) collective-permute-start(bf16[256,512]{1,0:T(8,128)(2,1)S(1)} %get-tuple-element.87), channel_id=1, source_target_pairs={{0,6},{1,25},{2,0},{3,27},{4,2},{5,29},{6,4},{7,31},{8,14},{9,1},{... | collective-permute-start | bytes 786440 | tf_op jit(solution)/shard_map/ppermute | solution.py:48
  31.0 7.6 %collective-permute-start.3 = (bf16[256,512]{1,0:T(8,128)(2,1)S(1)}, bf16[256,512]{1,0:T(8,128)(2,1)S(1)}, u32[]{:S(2)}, u32[]{:S(2)}) collective-permute-start(bf16[256,512]{1,0:T(8,128)(2,1)S(1)} %collective-permute-done.refs_1_), channel_id=1, source_target_pairs={{0,2},{1,9},{2,4},{3,11},{4,6},{5,13},{6,0},{7,15},{8,10},{9,17},{... | collective-permute-start | bytes 786440 | tf_op jit(solution)/shard_map/ppermute | solution.py:48
  31.0 7.6 %collective-permute-start.4 = (bf16[256,512]{1,0:T(8,128)(2,1)S(1)}, bf16[256,512]{1,0:T(8,128)(2,1)S(1)}, u32[]{:S(2)}, u32[]{:S(2)}) collective-permute-start(bf16[256,512]{1,0:T(8,128)(2,1)S(1)} %collective-permute-done.1.refs_2_), channel_id=1, source_target_pairs={{0,6},{1,25},{2,0},{3,27},{4,2},{5,29},{6,4},{7,31},{8,14},{9,1},{... | collective-permute-start | bytes 786440 | tf_op jit(solution)/shard_map/ppermute | solution.py:48
  41.6 10.5 %collective-permute-start.9 = (bf16[512,512]{1,0:T(8,128)(2,1)S(1)}, bf16[512,512]{1,0:T(8,128)(2,1)S(1)}, u32[]{:S(2)}, u32[]{:S(2)}) collective-permute-start(bf16[512,512]{1,0:T(8,128)(2,1)S(1)} %convolution_convert_fusion.2), channel_id=1, source_target_pairs={{0,2},{1,9},{2,4},{3,11},{4,6},{5,13},{6,0},{7,15},{8,10},{9,17},{... | collective-permute-start | bytes 1572872 | tf_op jit(solution)/shard_map/ppermute | solution.py:48
  42.0 10.4 %collective-permute-start.8 = (bf16[512,512]{1,0:T(8,128)(2,1)S(1)}, bf16[512,512]{1,0:T(8,128)(2,1)S(1)}, u32[]{:S(2)}, u32[]{:S(2)}) collective-permute-start(bf16[512,512]{1,0:T(8,128)(2,1)S(1)} %convolution_convert_fusion.3), channel_id=1, source_target_pairs={{0,6},{1,25},{2,0},{3,27},{4,2},{5,29},{6,4},{7,31},{8,14},{9,1},{... | collective-permute-start | bytes 1572872 | tf_op jit(solution)/shard_map/ppermute | solution.py:48
  52.3 7.7 %collective-permute-start.10 = (bf16[256,512]{1,0:T(8,128)(2,1)S(1)}, bf16[256,512]{1,0:T(8,128)(2,1)S(1)}, u32[]{:S(2)}, u32[]{:S(2)}) collective-permute-start(bf16[256,512]{1,0:T(8,128)(2,1)S(1)} %add_convert_fusion.3), channel_id=1, source_target_pairs={{0,2},{1,9},{2,4},{3,11},{4,6},{5,13},{6,0},{7,15},{8,10},{9,17},{... | collective-permute-start | bytes 786440 | tf_op jit(solution)/shard_map/ppermute | solution.py:48
  52.7 7.3 %collective-permute-start.11 = (bf16[256,512]{1,0:T(8,128)(2,1)S(1)}, bf16[256,512]{1,0:T(8,128)(2,1)S(1)}, u32[]{:S(2)}, u32[]{:S(2)}) collective-permute-start(bf16[256,512]{1,0:T(8,128)(2,1)S(1)} %add_convert_fusion.2), channel_id=1, source_target_pairs={{0,6},{1,25},{2,0},{3,27},{4,2},{5,29},{6,4},{7,31},{8,14},{9,1},{... | collective-permute-start | bytes 786440 | tf_op jit(solution)/shard_map/ppermute | solution.py:48
  76.9 8.0 %collective-permute-start.14 = (bf16[64,512]{1,0:T(8,128)(2,1)S(1)}, bf16[64,512]{1,0:T(8,128)(2,1)S(1)}, u32[]{:S(2)}, u32[]{:S(2)}) collective-permute-start(bf16[64,512]{1,0:T(8,128)(2,1)S(1)} %pad_maximum_fusion.6.refs_0_), channel_id=1, source_target_pairs={{0,4},{1,5},{2,6},{3,7},{4,0},{5,1},{6,2},{7,3},{8,12},{9,13},{10,... | collective-permute-start | bytes 196616 | tf_op jit(solution)/shard_map/ppermute | solution.py:53
  87.3 22.0 %all-to-all-start.2 = ((bf16[16,32,1152]{2,1,0:T(8,128)(2,1)}), bf16[16,32,1152]{2,1,0:T(8,128)(2,1)S(1)}, u32[]{:S(2)}, u32[]{:S(2)}) async-start(bf16[16,32,1152]{2,1,0:T(8,128)(2,1)} %project.1), calls=%async_computation.2 | async-start | bytes 2359296 | tf_op jit(solution)/shard_map/all_to_all | solution.py:26
  113.3 12.2 %all-to-all-start.3 = ((bf16[16,32,256]{2,1,0:T(8,128)(2,1)}), bf16[16,32,256]{2,1,0:T(8,128)(2,1)S(1)}, u32[]{:S(2)}, u32[]{:S(2)}) async-start(bf16[16,32,256]{2,1,0:T(8,128)(2,1)} %broadcast_in_dim.19), calls=%async_computation.3 | async-start | bytes 524288 | tf_op jit(solution)/shard_map/all_to_all | solution.py:22
  149.3 8.2 %collective-permute-start.22 = (bf16[4,3,96,512]{3,2,1,0:T(8,128)(2,1)S(1)}, bf16[4,3,96,512]{3,2,1,0:T(8,128)(2,1)S(1)}, u32[]{:S(2)}, u32[]{:S(2)}) collective-permute-start(bf16[4,3,96,512]{3,2,1,0:T(8,128)(2,1)S(1)} %copy-done.10), channel_id=1, source_target_pairs={{0,1},{1,0},{2,3},{3,2},{4,5},{5,4},{6,7},{7,6},{8,9},{9,8},{10,11... | collective-permute-start | bytes 3538952 | tf_op jit(solution)/shard_map/ppermute | solution.py:30
  149.9 7.6 %collective-permute-start.20 = (bf16[256,512]{1,0:T(8,128)(2,1)S(1)}, bf16[256,512]{1,0:T(8,128)(2,1)S(1)}, u32[]{:S(2)}, u32[]{:S(2)}) collective-permute-start(bf16[256,512]{1,0:T(8,128)(2,1)S(1)} %get-tuple-element.85), channel_id=1, source_target_pairs={{0,2},{1,9},{2,4},{3,11},{4,6},{5,13},{6,0},{7,15},{8,10},{9,17},{... | collective-permute-start | bytes 786440 | tf_op jit(solution)/shard_map/ppermute | solution.py:48
  151.4 9.3 %collective-permute-start.25 = (bf16[256,512]{1,0:T(8,128)(2,1)S(1)}, bf16[256,512]{1,0:T(8,128)(2,1)S(1)}, u32[]{:S(2)}, u32[]{:S(2)}) collective-permute-start(bf16[256,512]{1,0:T(8,128)(2,1)S(1)} %get-tuple-element.84), channel_id=1, source_target_pairs={{0,2},{1,9},{2,4},{3,11},{4,6},{5,13},{6,0},{7,15},{8,10},{9,17},{... | collective-permute-start | bytes 786440 | tf_op jit(solution)/shard_map/ppermute | solution.py:48
  151.4 9.3 %collective-permute-start.26 = (bf16[256,512]{1,0:T(8,128)(2,1)S(1)}, bf16[256,512]{1,0:T(8,128)(2,1)S(1)}, u32[]{:S(2)}, u32[]{:S(2)}) collective-permute-start(bf16[256,512]{1,0:T(8,128)(2,1)S(1)} %get-tuple-element.85), channel_id=1, source_target_pairs={{0,6},{1,25},{2,0},{3,27},{4,2},{5,29},{6,4},{7,31},{8,14},{9,1},{... | collective-permute-start | bytes 786440 | tf_op jit(solution)/shard_map/ppermute | solution.py:48
  157.5 7.6 %collective-permute-start.23 = (bf16[256,512]{1,0:T(8,128)(2,1)S(1)}, bf16[256,512]{1,0:T(8,128)(2,1)S(1)}, u32[]{:S(2)}, u32[]{:S(2)}) collective-permute-start(bf16[256,512]{1,0:T(8,128)(2,1)S(1)} %collective-permute-done.20.refs_1_), channel_id=1, source_target_pairs={{0,2},{1,9},{2,4},{3,11},{4,6},{5,13},{6,0},{7,15},{8,10},{9,17},{... | collective-permute-start | bytes 786440 | tf_op jit(solution)/shard_map/ppermute | solution.py:48
  157.8 7.3 %collective-permute-start.24 = (bf16[256,512]{1,0:T(8,128)(2,1)S(1)}, bf16[256,512]{1,0:T(8,128)(2,1)S(1)}, u32[]{:S(2)}, u32[]{:S(2)}) collective-permute-start(bf16[256,512]{1,0:T(8,128)(2,1)S(1)} %collective-permute-done.21.refs_2_), channel_id=1, source_target_pairs={{0,6},{1,25},{2,0},{3,27},{4,2},{5,29},{6,4},{7,31},{8,14},{9,1},{... | collective-permute-start | bytes 786440 | tf_op jit(solution)/shard_map/ppermute | solution.py:48
  168.0 10.5 %collective-permute-start.29 = (bf16[512,512]{1,0:T(8,128)(2,1)S(1)}, bf16[512,512]{1,0:T(8,128)(2,1)S(1)}, u32[]{:S(2)}, u32[]{:S(2)}) collective-permute-start(bf16[512,512]{1,0:T(8,128)(2,1)S(1)} %convolution_convert_fusion), channel_id=1, source_target_pairs={{0,2},{1,9},{2,4},{3,11},{4,6},{5,13},{6,0},{7,15},{8,10},{9,17},{... | collective-permute-start | bytes 1572872 | tf_op jit(solution)/shard_map/ppermute | solution.py:48
  168.5 10.4 %collective-permute-start.28 = (bf16[512,512]{1,0:T(8,128)(2,1)S(1)}, bf16[512,512]{1,0:T(8,128)(2,1)S(1)}, u32[]{:S(2)}, u32[]{:S(2)}) collective-permute-start(bf16[512,512]{1,0:T(8,128)(2,1)S(1)} %convolution_convert_fusion.1), channel_id=1, source_target_pairs={{0,6},{1,25},{2,0},{3,27},{4,2},{5,29},{6,4},{7,31},{8,14},{9,1},{... | collective-permute-start | bytes 1572872 | tf_op jit(solution)/shard_map/ppermute | solution.py:48
  178.8 7.7 %collective-permute-start.30 = (bf16[256,512]{1,0:T(8,128)(2,1)S(1)}, bf16[256,512]{1,0:T(8,128)(2,1)S(1)}, u32[]{:S(2)}, u32[]{:S(2)}) collective-permute-start(bf16[256,512]{1,0:T(8,128)(2,1)S(1)} %add_convert_fusion.1), channel_id=1, source_target_pairs={{0,2},{1,9},{2,4},{3,11},{4,6},{5,13},{6,0},{7,15},{8,10},{9,17},{... | collective-permute-start | bytes 786440 | tf_op jit(solution)/shard_map/ppermute | solution.py:48
  179.1 7.3 %collective-permute-start.31 = (bf16[256,512]{1,0:T(8,128)(2,1)S(1)}, bf16[256,512]{1,0:T(8,128)(2,1)S(1)}, u32[]{:S(2)}, u32[]{:S(2)}) collective-permute-start(bf16[256,512]{1,0:T(8,128)(2,1)S(1)} %add_convert_fusion), channel_id=1, source_target_pairs={{0,6},{1,25},{2,0},{3,27},{4,2},{5,29},{6,4},{7,31},{8,14},{9,1},{... | collective-permute-start | bytes 786440 | tf_op jit(solution)/shard_map/ppermute | solution.py:48
  (22 other events, 242.1 us)

commit v3 on v1

--- a/solution.py
+++ b/solution.py
@@ -23,10 +23,6 @@
     return lax.all_to_all(copies, axes, split_axis=0, concat_axis=0, tiled=True)
 
 
-def exchange(pieces, axes):
-    return lax.all_to_all(pieces, axes, split_axis=0, concat_axis=0, tiled=True)
-
-
 def other_core(value):
     return lax.ppermute(value, "c", [(0, 1), (1, 0)])
 
@@ -44,6 +40,17 @@
 def shift(value, steps):
     pairs = [
         (device(z, y, x, c), device(z, y, x + steps, c) if c == 0 else device(z, y + steps, x, c))
+        for z, y, x, c in PLACES
+    ]
+    return lax.ppermute(value, ALL, pairs)
+
+
+def shift_kv(value, steps, stage):
+    pairs = [
+        (
+            device(z, y, x, c),
+            device(z + steps, y, x, c) if c == stage else device(z, y + steps, x, c),
+        )
         for z, y, x, c in PLACES
     ]
     return lax.ppermute(value, ALL, pairs)
@@ -207,15 +214,17 @@
     return copies
 
 
-def readout_body(arrived, past, floor, gain, mixed, forget, value, query, gate, states, sems):
+def readout_body(*refs):
+    arrived, refs = refs[:4], refs[4:]
+    past, floor, gain, mixed, forget, value, query, gate, states, sems = refs
     copies = chunk_copies(past, states, sems)
     for copy in copies:
         copy.start()
     heads, width = past.shape[1:3]
     inner = heads * width
-    total = arrived[0].astype(f32)
-    for i in range(1, arrived.shape[0]):
-        total = total + arrived[i].astype(f32)
+    total = arrived[0][...].astype(f32)
+    for piece in arrived[1:]:
+        total = total + piece[...].astype(f32)
     squares = total[:, 4 * inner : 4 * inner + 1] + total[:, 4 * inner + 64 : 4 * inner + 65]
     total = total[:, : 4 * inner] * lax.rsqrt(squares / D + epsilon)
     query[...] = jax.nn.silu(total[:, :inner])
@@ -256,7 +265,7 @@
     return pl.pallas_call(
         readout_body,
         in_specs=[
-            pl.BlockSpec(arrived.shape, lambda: (0, 0, 0)),
+            *[pl.BlockSpec(piece.shape, lambda: (0, 0)) for piece in arrived],
             pl.BlockSpec(memory_space=pl.ANY),
             pl.BlockSpec((1, inner), lambda: (0, 0)),
             pl.BlockSpec((1, width), lambda: (0, 0)),
@@ -270,7 +279,7 @@
         ],
         compiler_params=pltpu.CompilerParams(vmem_limit_bytes=14 * 2**20),
         name="readout",
-    )(arrived, in_hbm(past), floor.reshape(1, -1), gain.reshape(1, -1))
+    )(*arrived, in_hbm(past), floor.reshape(1, -1), gain.reshape(1, -1))
 
 
 def state_body(forget, value, past, new, columns, states, arrivals, departures):
@@ -319,26 +328,39 @@
 
 
 def project_body(gain, *refs):
-    place = lax.axis_index("x"), lax.axis_index("c")
-    pieces, weights, (out, block) = refs[:4], refs[4:-2], refs[-2:]
+    pieces, weights, outs = refs[:4], refs[4:8], refs[8:12]
+    block, rows_scratch, sums_scratch = refs[12:]
+    x, core = lax.axis_index("x"), lax.axis_index("c")
     width, rows = pieces[0].shape[0] // 2, pieces[0].shape[1]
     for k, piece in enumerate(pieces):
-        first = lax.rem(place[0] + k, 4) * 2 * width
+        first = lax.rem(x + k, 4) * 2 * width
         for side in range(2):
-            row = pl.multiple_of(first + lax.rem(place[1] + side, 2) * width, width)
+            row = pl.multiple_of(first + lax.rem(core + side, 2) * width, width)
             block[pl.ds(row, width), :] = piece[width * side : width * (side + 1), :]
     value = block[...].astype(f32)
     normed = (value * jnp.concatenate([gain[...]] * (rows // 128), axis=1)).astype(bf16)
-    normed = normed.T
-    count, own, _ = out.shape
-    for i, w in enumerate(weights):
-        part = jnp.dot(normed, w[...], preferred_element_type=f32).astype(bf16)
-        out[:, :, 256 * i : 256 * (i + 1)] = part.reshape(count, own, 256)
+    rows_scratch[...] = normed.T
     squares = jnp.sum(value * value, axis=0, keepdims=True)
     high = squares.astype(bf16).astype(f32)
     line = lax.broadcasted_iota(jnp.int32, (128, rows), 0)
-    both = jnp.where(line < 64, high, squares - high).astype(bf16).T
-    out[:, :, 1024:1152] = both.reshape(count, own, 128)
+    sums_scratch[...] = jnp.where(line < 64, high, squares - high).astype(bf16).T
+    own = outs[0].shape[1]
+    z, y = lax.axis_index("z"), lax.axis_index("y")
+    starts = []
+    for k in range(4):
+        for m in range(4):
+            ahead = jnp.where(core == 0, k, m), jnp.where(core == 0, m, k)
+            owner = lax.rem(z + ahead[0], 4) * 4 + lax.rem(y + ahead[1], 4)
+            starts.append(pl.multiple_of(owner * own, own))
+    normed = jnp.concatenate([rows_scratch[pl.ds(row, own), :] for row in starts], axis=0)
+    for i, w in enumerate(weights):
+        part = jnp.dot(normed, w[...], preferred_element_type=f32).astype(bf16)
+        for k, out in enumerate(outs):
+            here = part[4 * own * k : 4 * own * (k + 1)]
+            out[:, :, 256 * i : 256 * (i + 1)] = here.reshape(4, own, 256)
+    for k, out in enumerate(outs):
+        for m in range(4):
+            out[m, :, 1024:1152] = sums_scratch[pl.ds(starts[4 * k + m], own), :]
 
 
 def project(pieces, gain, weights, own_rows):
@@ -347,8 +369,12 @@
     return pl.pallas_call(
         project_body,
         in_specs=[pl.BlockSpec(v.shape, lambda: (0, 0)) for v in operands],
-        out_shape=jax.ShapeDtypeStruct((rows // own_rows, own_rows, 4 * width + 128), bf16),
-        scratch_shapes=[pltpu.VMEM((width, rows), bf16)],
+        out_shape=[jax.ShapeDtypeStruct((4, own_rows, 4 * width + 128), bf16)] * 4,
+        scratch_shapes=[
+            pltpu.VMEM((width, rows), bf16),
+            pltpu.VMEM((rows, width), bf16),
+            pltpu.VMEM((rows, 128), bf16),
+        ],
         compiler_params=pltpu.CompilerParams(vmem_limit_bytes=14 * 2**20),
         name="project",
     )(*operands)
@@ -467,12 +493,18 @@
     pieces = [pair] + [shift_x(pair, -k) for k in (1, 2, 3)]
     weight_list = (query_weight, forget_weight, value_weight, output_gate_weight)
     sent = project(pieces, gains, weight_list, own_rows)
-    sent, post_gate, post_up, post_down = lax.optimization_barrier(
-        (sent, post_gate, post_up, post_down)
+    blocks = list(sent)
+    blocks[0], post_gate, post_up, post_down = lax.optimization_barrier(
+        (blocks[0], post_gate, post_up, post_down)
     )
     near_w, far_w, gains = order_weights(post_gain, post_gate.T, post_up.T, post_down)
-    arrived = exchange(sent, KV)
-    arrived, near_w = lax.optimization_barrier((arrived, near_w))
+    summed = blocks[0].astype(f32)
+    passed = [shift_kv(blocks[k], k, 0) for k in (2, 1, 3)]
+    passed, near_w = lax.optimization_barrier((passed, near_w))
+    for piece in passed:
+        summed = summed + piece.astype(f32)
+    summed = summed.astype(bf16)
+    arrived = [summed[0]] + [shift_kv(summed[m], m, 1) for m in (2, 1, 3)]
     mixed_in, forget, value = read_out(arrived, past_state, forget_floor, head_gain)
     new_state = update_state(forget, value, past_state)
     gathered = copy_for_each(mixed_in, KV).reshape(-1, mixed_in.shape[1])

time: 198 us -> 194 us (0.980)
  waiting for transfers between devices: 64.3 us -> 56.2 us
  starting transfers between devices: 56.4 us -> 62.9 us
    all_to_all x1 -> x0, waiting for transfers between devices: 12.5 us -> none  [exchange(): return lax.all_to_all(pieces, axes, split_axis=0, concat_axis=0, tiled=True)]
    ppermute x0 -> x6, starting transfers between devices: none -> 8.31 us  [shift_kv(): return lax.ppermute(value, ALL, pairs)]
    ppermute x0 -> x6, waiting for transfers between devices: none -> 4.42 us  [shift_kv(): return lax.ppermute(value, ALL, pairs)]
    all_to_all x1 -> x0, starting transfers between devices: 4.01 us -> none  [exchange(): return lax.all_to_all(pieces, axes, split_axis=0, concat_axis=0, tiled=True)]
  transfers between devices with their start and end apart: 33 -> 38, of which waited for: 24 -> 26; matrix products, arithmetic and copies ran while one was open for 0% -> 1% of each run, Pallas kernels for 8% -> 8%
where the time goes in v3:
time: 194 us; the launch traced here: 193 us
  starting transfers between devices  62.9 us (32%)
  waiting for transfers between devices  56.2 us (29%)
  blocking collectives  42.8 us (22%)
  Pallas kernels  21.1 us (11%)
  local copies, waits for them, and re-layouts  4.53 us (2%)
  matrix products  2.79 us (1%)
    all_to_all x3, blocking collectives, plane_exchange(): lax.all_to_all(pieces, ALL, split_axis=0, concat_axis=0, axis_index_group...  42.8 us
    ppermute x18, starting transfers between devices, shift(): return lax.ppermute(value, ALL, pairs)  32.6 us
    ppermute x18, waiting for transfers between devices, shift(): return lax.ppermute(value, ALL, pairs)  30.5 us
    pallas_call x2, Pallas kernels, order_weights(): pl.pallas_call(order_body, grid=(4,), in_specs=[whole, whole, pl.BlockSpe...  10.9 us
    ppermute x6, starting transfers between devices, shift_kv(): return lax.ppermute(value, ALL, pairs)  8.31 us
    all_to_all x1, starting transfers between devices, plane_exchange(): lax.all_to_all(pieces, ALL, split_axis=0, concat_axis=0, axis_index_group...  8.16 us
    ppermute x6, starting transfers between devices, shift_x(): return lax.ppermute(value, ALL, pairs)  7.93 us
    ppermute x6, waiting for transfers between devices, shift_x(): return lax.ppermute(value, ALL, pairs)  6.97 us
  transfers between devices with their start and end apart: 38, of which 26 were waited for; matrix products, arithmetic and copies ran while one was open for 1% of the time, Pallas kernels for 8%

profile of v3, /device:TPU:0, one launch (start us, length us, event | category | flops | bytes accessed | tf_op | source)
XLA Modules:
  0.0 193.4 jit_solution(8381520372666845642)
XLA Ops:
  2.3 8.2 %all-to-all-start = ((bf16[16,32,512]{2,1,0:T(8,128)(2,1)}), bf16[16,32,512]{2,1,0:T(8,128)(2,1)S(1)}, u32[]{:S(2)}, u32[]{:S(2)}) async-start(bf16[16,32,512]{2,1,0:T(8,128)(2,1)} %broadcast_in_dim.8), calls=%async_computation | async-start | bytes 1048576 | tf_op jit(solution)/shard_map/all_to_all | solution.py:65
  10.5 5.4 %order.2 = (bf16[4,3,96,512]{3,2,1,0:T(8,128)(2,1)S(1)}, bf16[4,3,96,512]{3,2,1,0:T(8,128)(2,1)S(1)}, f32[4,512,128]{2,1,0:T(8,128)S(1)}) custom-call(s32[1,512]{1,0:T(1,128)S(1)} %get-tuple-element.101.mine, s32[1,512]{1,0:T(1,128)S(1)} %get-tuple-element.102.theirs, f32[4,1,1024]{2,1,0:T(1,128)S(1)} %bitcast.80, bf16[88,4096]{1,0:T(8,128)(2,1)} %bitcast.88, ...), custom_call_target="tpu_custom_call" | custom-call | flops 5000000000 | bytes 6000000 | tf_op jit(solution)/shard_map/order/pallas_call | solution.py:126
  17.0 3.6 %all-to-all-done = bf16[16,32,512]{2,1,0:T(8,128)(2,1)S(1)} async-done(((bf16[16,32,512]{2,1,0:T(8,128)(2,1)}), bf16[16,32,512]{2,1,0:T(8,128)(2,1)S(1)}, u32[]{:S(2)}, u32[]{:S(2)}) %all-to-all-start) | async-done | bytes 524320 | tf_op jit(solution)/shard_map/all_to_all | solution.py:65
  24.2 3.0 %collective-permute-start.6 = (bf16[256,512]{1,0:T(8,128)(2,1)S(1)}, bf16[256,512]{1,0:T(8,128)(2,1)S(1)}, u32[]{:S(2)}, u32[]{:S(2)}) collective-permute-start(bf16[256,512]{1,0:T(8,128)(2,1)S(1)} %get-tuple-element.89), channel_id=1, source_target_pairs={{0,6},{1,25},{2,0},{3,27},{4,2},{5,29},{6,4},{7,31},{8,14},{9,1},{... | collective-permute-start | bytes 786440 | tf_op jit(solution)/shard_map/ppermute | solution.py:45
  32.6 3.5 %collective-permute-done.3.refs_0_ = bf16[256,512]{1,0:T(8,128)(2,1)S(1)} collective-permute-done((bf16[256,512]{1,0:T(8,128)(2,1)S(1)}, bf16[256,512]{1,0:T(8,128)(2,1)S(1)}, u32[]{:S(2)}, u32[]{:S(2)}) %collective-permute-start.3) | collective-permute-done | bytes 262176 | tf_op jit(solution)/shard_map/ppermute | solution.py:45
  40.1 3.0 %collective-permute-start.8 = (bf16[512,512]{1,0:T(8,128)(2,1)S(1)}, bf16[512,512]{1,0:T(8,128)(2,1)S(1)}, u32[]{:S(2)}, u32[]{:S(2)}) collective-permute-start(bf16[512,512]{1,0:T(8,128)(2,1)S(1)} %convolution_convert_fusion.6), channel_id=1, source_target_pairs={{0,4},{1,17},{2,6},{3,19},{4,0},{5,21},{6,2},{7,23},{8,12},{9,25},... | collective-permute-start | bytes 1572872 | tf_op jit(solution)/shard_map/ppermute | solution.py:45
  46.3 4.6 %collective-permute-done.8 = bf16[512,512]{1,0:T(8,128)(2,1)S(1)} collective-permute-done((bf16[512,512]{1,0:T(8,128)(2,1)S(1)}, bf16[512,512]{1,0:T(8,128)(2,1)S(1)}, u32[]{:S(2)}, u32[]{:S(2)}) %collective-permute-start.8) | collective-permute-done | bytes 524320 | tf_op jit(solution)/shard_map/ppermute | solution.py:45
  50.9 5.5 %collective-permute-done.9 = bf16[512,512]{1,0:T(8,128)(2,1)S(1)} collective-permute-done((bf16[512,512]{1,0:T(8,128)(2,1)S(1)}, bf16[512,512]{1,0:T(8,128)(2,1)S(1)}, u32[]{:S(2)}, u32[]{:S(2)}) %collective-permute-start.9) | collective-permute-done | bytes 524320 | tf_op jit(solution)/shard_map/ppermute | solution.py:45
  57.3 15.0 %all_to_all.25 = bf16[16,32,512]{2,1,0:T(8,128)(2,1)S(1)} all-to-all(bf16[16,32,512]{2,1,0:T(8,128)(2,1)S(1)} %bitcast.82), channel_id=1, replica_groups={{0,8,16,24,32,40,48,56,64,72,80,88,96,104,112,120},{2,10,18,26,34,42,50..., dimensions={0} | all-to-all | bytes 1048576 | tf_op jit(solution)/shard_map/all_to_all | solution.py:65
  73.6 2.6 %collective-permute-start.12 = (bf16[64,512]{1,0:T(8,128)(2,1)S(1)}, bf16[64,512]{1,0:T(8,128)(2,1)S(1)}, u32[]{:S(2)}, u32[]{:S(2)}) collective-permute-start(bf16[64,512]{1,0:T(8,128)(2,1)S(1)} %pad_maximum_fusion.4.refs_0_), channel_id=1, source_target_pairs={{0,6},{1,7},{2,0},{3,1},{4,2},{5,3},{6,4},{7,5},{8,14},{9,15},{10,... | collective-permute-start | bytes 196616 | tf_op jit(solution)/shard_map/ppermute | solution.py:61
  79.4 3.0 %collective-permute-done.13.refs_2_ = bf16[64,512]{1,0:T(8,128)(2,1)S(1)} collective-permute-done((bf16[64,512]{1,0:T(8,128)(2,1)S(1)}, bf16[64,512]{1,0:T(8,128)(2,1)S(1)}, u32[]{:S(2)}, u32[]{:S(2)}) %collective-permute-start.13) | collective-permute-done | bytes 65568 | tf_op jit(solution)/shard_map/ppermute | solution.py:61
  88.0 5.4 %order.3 = (bf16[4,3,96,512]{3,2,1,0:T(8,128)(2,1)S(1)}, bf16[4,3,96,512]{3,2,1,0:T(8,128)(2,1)S(1)}, f32[4,512,128]{2,1,0:T(8,128)S(1)}) custom-call(s32[1,512]{1,0:T(1,128)S(1)} %get-tuple-element.101.mine, s32[1,512]{1,0:T(1,128)S(1)} %get-tuple-element.102.theirs, f32[4,1,1024]{2,1,0:T(1,128)S(1)} %bitcast.81, bf16[88,4096]{1,0:T(8,128)(2,1)} %bitcast.90, ...), custom_call_target="tpu_custom_call" | custom-call | flops 5000000000 | bytes 6000000 | tf_op jit(solution)/shard_map/order/pallas_call | solution.py:126
  102.2 3.2 %readout.1 = (bf16[32,256]{1,0:T(8,128)(2,1)S(1)}, f32[32,256]{1,0:T(8,128)S(1)}, f32[32,256]{1,0:T(8,128)S(1)}) custom-call(bf16[32,1152]{1,0:T(8,128)(2,1)S(1)} %get-tuple-element.93.refs_0_, bf16[32,1152]{1,0:T(8,128)(2,1)S(1)} %collective-permute-done.18.refs_1_, bf16[32,1152]{1,0:T(8,128)(2,1)S(1)} %collective-permute-done.19.refs_2_, ...), custom_call_target="tpu_custom_call" | custom-call | tf_op jit(solution)/shard_map/readout/pallas_call | solution.py:265
  106.1 5.3 %all-to-all-start.2 = ((bf16[16,32,256]{2,1,0:T(8,128)(2,1)}), bf16[16,32,256]{2,1,0:T(8,128)(2,1)S(1)}, u32[]{:S(2)}, u32[]{:S(2)}) async-start(bf16[16,32,256]{2,1,0:T(8,128)(2,1)} %broadcast_in_dim.19), calls=%async_computation.2 | async-start | bytes 524288 | tf_op jit(solution)/shard_map/all_to_all | solution.py:23
  111.4 3.8 %state.1 = f32[32,2,128,128]{3,2,1,0:T(8,128)} custom-call(f32[32,256]{1,0:T(8,128)S(1)} %get-tuple-element.66.forget, f32[32,256]{1,0:T(8,128)S(1)} %get-tuple-element.67.value, f32[32,2,128,128]{3,2,1,0:T(8,128)} %past.1), custom_call_target="tpu_custom_call" | custom-call | flops 4000000000 | bytes 8000000 | tf_op jit(solution)/shard_map/state/pallas_call | solution.py:311
  115.2 4.9 %all-to-all-done.2 = bf16[16,32,256]{2,1,0:T(8,128)(2,1)S(1)} async-done(((bf16[16,32,256]{2,1,0:T(8,128)(2,1)}), bf16[16,32,256]{2,1,0:T(8,128)(2,1)S(1)}, u32[]{:S(2)}, u32[]{:S(2)}) %all-to-all-start.2) | async-done | bytes 262176 | tf_op jit(solution)/shard_map/all_to_all | solution.py:23
  123.5 2.7 %collective-permute-start.24 = (bf16[32,512]{1,0:T(8,128)(2,1)S(1)}, bf16[32,512]{1,0:T(8,128)(2,1)S(1)}, u32[]{:S(2)}, u32[]{:S(2)}) collective-permute-start(bf16[32,512]{1,0:T(8,128)(2,1)S(1)} %get-tuple-element.95), channel_id=1, source_target_pairs={{0,6},{1,7},{2,0},{3,1},{4,2},{5,3},{6,4},{7,5},{8,14},{9,15},{10,... | collective-permute-start | bytes 98312 | tf_op jit(solution)/shard_map/ppermute | solution.py:61
  128.2 13.3 %all_to_all.26 = bf16[16,32,512]{2,1,0:T(8,128)(2,1)S(1)} all-to-all(bf16[16,32,512]{2,1,0:T(8,128)(2,1)S(1)} %broadcast_in_dim.20), channel_id=1, replica_groups={{0,8,16,24,32,40,48,56,64,72,80,88,96,104,112,120},{2,10,18,26,34,42,50..., dimensions={0} | all-to-all | bytes 1048576 | tf_op jit(solution)/shard_map/all_to_all | solution.py:65
  144.8 3.2 %collective-permute-start.31 = (bf16[256,512]{1,0:T(8,128)(2,1)S(1)}, bf16[256,512]{1,0:T(8,128)(2,1)S(1)}, u32[]{:S(2)}, u32[]{:S(2)}) collective-permute-start(bf16[256,512]{1,0:T(8,128)(2,1)S(1)} %get-tuple-element.87), channel_id=1, source_target_pairs={{0,6},{1,25},{2,0},{3,27},{4,2},{5,29},{6,4},{7,31},{8,14},{9,1},{... | collective-permute-start | bytes 786440 | tf_op jit(solution)/shard_map/ppermute | solution.py:45
  153.3 3.5 %collective-permute-done.28.refs_0_ = bf16[256,512]{1,0:T(8,128)(2,1)S(1)} collective-permute-done((bf16[256,512]{1,0:T(8,128)(2,1)S(1)}, bf16[256,512]{1,0:T(8,128)(2,1)S(1)}, u32[]{:S(2)}, u32[]{:S(2)}) %collective-permute-start.28) | collective-permute-done | bytes 262176 | tf_op jit(solution)/shard_map/ppermute | solution.py:45
  160.7 3.6 %collective-permute-start.33 = (bf16[512,512]{1,0:T(8,128)(2,1)S(1)}, bf16[512,512]{1,0:T(8,128)(2,1)S(1)}, u32[]{:S(2)}, u32[]{:S(2)}) collective-permute-start(bf16[512,512]{1,0:T(8,128)(2,1)S(1)} %convolution_convert_fusion.2), channel_id=1, source_target_pairs={{0,4},{1,17},{2,6},{3,19},{4,0},{5,21},{6,2},{7,23},{8,12},{9,25},... | collective-permute-start | bytes 1572872 | tf_op jit(solution)/shard_map/ppermute | solution.py:45
  167.5 4.1 %collective-permute-done.33 = bf16[512,512]{1,0:T(8,128)(2,1)S(1)} collective-permute-done((bf16[512,512]{1,0:T(8,128)(2,1)S(1)}, bf16[512,512]{1,0:T(8,128)(2,1)S(1)}, u32[]{:S(2)}, u32[]{:S(2)}) %collective-permute-start.33) | collective-permute-done | bytes 524320 | tf_op jit(solution)/shard_map/ppermute | solution.py:45
  171.5 5.5 %collective-permute-done.34 = bf16[512,512]{1,0:T(8,128)(2,1)S(1)} collective-permute-done((bf16[512,512]{1,0:T(8,128)(2,1)S(1)}, bf16[512,512]{1,0:T(8,128)(2,1)S(1)}, u32[]{:S(2)}, u32[]{:S(2)}) %collective-permute-start.34) | collective-permute-done | bytes 524320 | tf_op jit(solution)/shard_map/ppermute | solution.py:45
  178.1 14.6 %all_to_all.27 = bf16[16,32,512]{2,1,0:T(8,128)(2,1)S(1)} all-to-all(bf16[16,32,512]{2,1,0:T(8,128)(2,1)S(1)} %bitcast.83), channel_id=1, replica_groups={{0,8,16,24,32,40,48,56,64,72,80,88,96,104,112,120},{2,10,18,26,34,42,50..., dimensions={0} | all-to-all | bytes 1048576 | tf_op jit(solution)/shard_map/all_to_all | solution.py:65
  (129 shorter events, 61.7 us)
Async XLA Ops:
  2.3 18.3 %all-to-all-start = ((bf16[16,32,512]{2,1,0:T(8,128)(2,1)}), bf16[16,32,512]{2,1,0:T(8,128)(2,1)S(1)}, u32[]{:S(2)}, u32[]{:S(2)}) async-start(bf16[16,32,512]{2,1,0:T(8,128)(2,1)} %broadcast_in_dim.8), calls=%async_computation | async-start | bytes 1048576 | tf_op jit(solution)/shard_map/all_to_all | solution.py:65
  20.6 8.0 %collective-permute-start.2 = (bf16[4,3,96,512]{3,2,1,0:T(8,128)(2,1)}, bf16[4,3,96,512]{3,2,1,0:T(8,128)(2,1)S(1)}, u32[]{:S(2)}, u32[]{:S(2)}) collective-permute-start(bf16[4,3,96,512]{3,2,1,0:T(8,128)(2,1)} %copy-done.9), channel_id=1, source_target_pairs={{0,1},{1,0},{2,3},{3,2},{4,5},{5,4},{6,7},{7,6},{8,9},{9,8},{10,11... | collective-permute-start | bytes 3538952 | tf_op jit(solution)/shard_map/ppermute | solution.py:27
  20.6 7.7 %collective-permute-start = (bf16[256,512]{1,0:T(8,128)(2,1)S(1)}, bf16[256,512]{1,0:T(8,128)(2,1)S(1)}, u32[]{:S(2)}, u32[]{:S(2)}) collective-permute-start(bf16[256,512]{1,0:T(8,128)(2,1)S(1)} %get-tuple-element.89), channel_id=1, source_target_pairs={{0,2},{1,9},{2,4},{3,11},{4,6},{5,13},{6,0},{7,15},{8,10},{9,17},{... | collective-permute-start | bytes 786440 | tf_op jit(solution)/shard_map/ppermute | solution.py:45
  22.2 6.4 %collective-permute-start.1 = (bf16[256,512]{1,0:T(8,128)(2,1)S(1)}, bf16[256,512]{1,0:T(8,128)(2,1)S(1)}, u32[]{:S(2)}, u32[]{:S(2)}) collective-permute-start(bf16[256,512]{1,0:T(8,128)(2,1)S(1)} %get-tuple-element.88), channel_id=1, source_target_pairs={{0,6},{1,25},{2,0},{3,27},{4,2},{5,29},{6,4},{7,31},{8,14},{9,1},{... | collective-permute-start | bytes 786440 | tf_op jit(solution)/shard_map/ppermute | solution.py:45
  23.9 7.9 %collective-permute-start.5 = (bf16[256,512]{1,0:T(8,128)(2,1)S(1)}, bf16[256,512]{1,0:T(8,128)(2,1)S(1)}, u32[]{:S(2)}, u32[]{:S(2)}) collective-permute-start(bf16[256,512]{1,0:T(8,128)(2,1)S(1)} %get-tuple-element.88), channel_id=1, source_target_pairs={{0,2},{1,9},{2,4},{3,11},{4,6},{5,13},{6,0},{7,15},{8,10},{9,17},{... | collective-permute-start | bytes 786440 | tf_op jit(solution)/shard_map/ppermute | solution.py:45
  24.2 7.6 %collective-permute-start.6 = (bf16[256,512]{1,0:T(8,128)(2,1)S(1)}, bf16[256,512]{1,0:T(8,128)(2,1)S(1)}, u32[]{:S(2)}, u32[]{:S(2)}) collective-permute-start(bf16[256,512]{1,0:T(8,128)(2,1)S(1)} %get-tuple-element.89), channel_id=1, source_target_pairs={{0,6},{1,25},{2,0},{3,27},{4,2},{5,29},{6,4},{7,31},{8,14},{9,1},{... | collective-permute-start | bytes 786440 | tf_op jit(solution)/shard_map/ppermute | solution.py:45
  28.6 7.6 %collective-permute-start.3 = (bf16[256,512]{1,0:T(8,128)(2,1)S(1)}, bf16[256,512]{1,0:T(8,128)(2,1)S(1)}, u32[]{:S(2)}, u32[]{:S(2)}) collective-permute-start(bf16[256,512]{1,0:T(8,128)(2,1)S(1)} %collective-permute-done.refs_1_), channel_id=1, source_target_pairs={{0,2},{1,9},{2,4},{3,11},{4,6},{5,13},{6,0},{7,15},{8,10},{9,17},{... | collective-permute-start | bytes 786440 | tf_op jit(solution)/shard_map/ppermute | solution.py:45
  40.1 10.9 %collective-permute-start.8 = (bf16[512,512]{1,0:T(8,128)(2,1)S(1)}, bf16[512,512]{1,0:T(8,128)(2,1)S(1)}, u32[]{:S(2)}, u32[]{:S(2)}) collective-permute-start(bf16[512,512]{1,0:T(8,128)(2,1)S(1)} %convolution_convert_fusion.6), channel_id=1, source_target_pairs={{0,4},{1,17},{2,6},{3,19},{4,0},{5,21},{6,2},{7,23},{8,12},{9,25},... | collective-permute-start | bytes 1572872 | tf_op jit(solution)/shard_map/ppermute | solution.py:45
  43.1 13.4 %collective-permute-start.9 = (bf16[512,512]{1,0:T(8,128)(2,1)S(1)}, bf16[512,512]{1,0:T(8,128)(2,1)S(1)}, u32[]{:S(2)}, u32[]{:S(2)}) collective-permute-start(bf16[512,512]{1,0:T(8,128)(2,1)S(1)} %convolution_convert_fusion.5), channel_id=1, source_target_pairs={{0,2},{1,9},{2,4},{3,11},{4,6},{5,13},{6,0},{7,15},{8,10},{9,17},{... | collective-permute-start | bytes 1572872 | tf_op jit(solution)/shard_map/ppermute | solution.py:45
  44.0 12.8 %collective-permute-start.10 = (bf16[512,512]{1,0:T(8,128)(2,1)S(1)}, bf16[512,512]{1,0:T(8,128)(2,1)S(1)}, u32[]{:S(2)}, u32[]{:S(2)}) collective-permute-start(bf16[512,512]{1,0:T(8,128)(2,1)S(1)} %convolution_convert_fusion.4), channel_id=1, source_target_pairs={{0,6},{1,25},{2,0},{3,27},{4,2},{5,29},{6,4},{7,31},{8,14},{9,1},{... | collective-permute-start | bytes 1572872 | tf_op jit(solution)/shard_map/ppermute | solution.py:45
  83.8 9.6 %collective-permute-start.15 = (bf16[4,32,1152]{2,1,0:T(8,128)(2,1)S(1)}, bf16[4,32,1152]{2,1,0:T(8,128)(2,1)S(1)}, u32[]{:S(2)}, u32[]{:S(2)}) collective-permute-start(bf16[4,32,1152]{2,1,0:T(8,128)(2,1)S(1)} %get-tuple-element.55), channel_id=1, source_target_pairs={{0,64},{1,17},{2,66},{3,19},{4,68},{5,21},{6,70},{7,23},{8,72},{9,... | collective-permute-start | bytes 884744 | tf_op jit(solution)/shard_map/ppermute | solution.py:56
  84.7 10.5 %collective-permute-start.16 = (bf16[4,32,1152]{2,1,0:T(8,128)(2,1)S(1)}, bf16[4,32,1152]{2,1,0:T(8,128)(2,1)S(1)}, u32[]{:S(2)}, u32[]{:S(2)}) collective-permute-start(bf16[4,32,1152]{2,1,0:T(8,128)(2,1)S(1)} %get-tuple-element.56), channel_id=1, source_target_pairs={{0,32},{1,9},{2,34},{3,11},{4,36},{5,13},{6,38},{7,15},{8,40},{9,1... | collective-permute-start | bytes 884744 | tf_op jit(solution)/shard_map/ppermute | solution.py:56
  85.6 9.7 %collective-permute-start.17 = (bf16[4,32,1152]{2,1,0:T(8,128)(2,1)S(1)}, bf16[4,32,1152]{2,1,0:T(8,128)(2,1)S(1)}, u32[]{:S(2)}, u32[]{:S(2)}) collective-permute-start(bf16[4,32,1152]{2,1,0:T(8,128)(2,1)S(1)} %get-tuple-element.57), channel_id=1, source_target_pairs={{0,96},{1,25},{2,98},{3,27},{4,100},{5,29},{6,102},{7,31},{8,104},... | collective-permute-start | bytes 884744 | tf_op jit(solution)/shard_map/ppermute | solution.py:56
  106.1 14.0 %all-to-all-start.2 = ((bf16[16,32,256]{2,1,0:T(8,128)(2,1)}), bf16[16,32,256]{2,1,0:T(8,128)(2,1)S(1)}, u32[]{:S(2)}, u32[]{:S(2)}) async-start(bf16[16,32,256]{2,1,0:T(8,128)(2,1)} %broadcast_in_dim.19), calls=%async_computation.2 | async-start | bytes 524288 | tf_op jit(solution)/shard_map/all_to_all | solution.py:23
  141.5 7.7 %collective-permute-start.27 = (bf16[4,3,96,512]{3,2,1,0:T(8,128)(2,1)S(1)}, bf16[4,3,96,512]{3,2,1,0:T(8,128)(2,1)S(1)}, u32[]{:S(2)}, u32[]{:S(2)}) collective-permute-start(bf16[4,3,96,512]{3,2,1,0:T(8,128)(2,1)S(1)} %copy-done.8), channel_id=1, source_target_pairs={{0,1},{1,0},{2,3},{3,2},{4,5},{5,4},{6,7},{7,6},{8,9},{9,8},{10,11... | collective-permute-start | bytes 3538952 | tf_op jit(solution)/shard_map/ppermute | solution.py:27
  141.5 7.7 %collective-permute-start.25 = (bf16[256,512]{1,0:T(8,128)(2,1)S(1)}, bf16[256,512]{1,0:T(8,128)(2,1)S(1)}, u32[]{:S(2)}, u32[]{:S(2)}) collective-permute-start(bf16[256,512]{1,0:T(8,128)(2,1)S(1)} %get-tuple-element.87), channel_id=1, source_target_pairs={{0,2},{1,9},{2,4},{3,11},{4,6},{5,13},{6,0},{7,15},{8,10},{9,17},{... | collective-permute-start | bytes 786440 | tf_op jit(solution)/shard_map/ppermute | solution.py:45
  142.6 6.6 %collective-permute-start.26 = (bf16[256,512]{1,0:T(8,128)(2,1)S(1)}, bf16[256,512]{1,0:T(8,128)(2,1)S(1)}, u32[]{:S(2)}, u32[]{:S(2)}) collective-permute-start(bf16[256,512]{1,0:T(8,128)(2,1)S(1)} %get-tuple-element.86), channel_id=1, source_target_pairs={{0,6},{1,25},{2,0},{3,27},{4,2},{5,29},{6,4},{7,31},{8,14},{9,1},{... | collective-permute-start | bytes 786440 | tf_op jit(solution)/shard_map/ppermute | solution.py:45
  144.8 7.6 %collective-permute-start.30 = (bf16[256,512]{1,0:T(8,128)(2,1)S(1)}, bf16[256,512]{1,0:T(8,128)(2,1)S(1)}, u32[]{:S(2)}, u32[]{:S(2)}) collective-permute-start(bf16[256,512]{1,0:T(8,128)(2,1)S(1)} %get-tuple-element.86), channel_id=1, source_target_pairs={{0,2},{1,9},{2,4},{3,11},{4,6},{5,13},{6,0},{7,15},{8,10},{9,17},{... | collective-permute-start | bytes 786440 | tf_op jit(solution)/shard_map/ppermute | solution.py:45
  144.8 7.6 %collective-permute-start.31 = (bf16[256,512]{1,0:T(8,128)(2,1)S(1)}, bf16[256,512]{1,0:T(8,128)(2,1)S(1)}, u32[]{:S(2)}, u32[]{:S(2)}) collective-permute-start(bf16[256,512]{1,0:T(8,128)(2,1)S(1)} %get-tuple-element.87), channel_id=1, source_target_pairs={{0,6},{1,25},{2,0},{3,27},{4,2},{5,29},{6,4},{7,31},{8,14},{9,1},{... | collective-permute-start | bytes 786440 | tf_op jit(solution)/shard_map/ppermute | solution.py:45
  149.2 7.6 %collective-permute-start.28 = (bf16[256,512]{1,0:T(8,128)(2,1)S(1)}, bf16[256,512]{1,0:T(8,128)(2,1)S(1)}, u32[]{:S(2)}, u32[]{:S(2)}) collective-permute-start(bf16[256,512]{1,0:T(8,128)(2,1)S(1)} %collective-permute-done.25.refs_1_), channel_id=1, source_target_pairs={{0,2},{1,9},{2,4},{3,11},{4,6},{5,13},{6,0},{7,15},{8,10},{9,17},{... | collective-permute-start | bytes 786440 | tf_op jit(solution)/shard_map/ppermute | solution.py:45
  150.4 6.4 %collective-permute-start.29 = (bf16[256,512]{1,0:T(8,128)(2,1)S(1)}, bf16[256,512]{1,0:T(8,128)(2,1)S(1)}, u32[]{:S(2)}, u32[]{:S(2)}) collective-permute-start(bf16[256,512]{1,0:T(8,128)(2,1)S(1)} %collective-permute-done.26.refs_2_), channel_id=1, source_target_pairs={{0,6},{1,25},{2,0},{3,27},{4,2},{5,29},{6,4},{7,31},{8,14},{9,1},{... | collective-permute-start | bytes 786440 | tf_op jit(solution)/shard_map/ppermute | solution.py:45
  160.7 10.9 %collective-permute-start.33 = (bf16[512,512]{1,0:T(8,128)(2,1)S(1)}, bf16[512,512]{1,0:T(8,128)(2,1)S(1)}, u32[]{:S(2)}, u32[]{:S(2)}) collective-permute-start(bf16[512,512]{1,0:T(8,128)(2,1)S(1)} %convolution_convert_fusion.2), channel_id=1, source_target_pairs={{0,4},{1,17},{2,6},{3,19},{4,0},{5,21},{6,2},{7,23},{8,12},{9,25},... | collective-permute-start | bytes 1572872 | tf_op jit(solution)/shard_map/ppermute | solution.py:45
  164.2 12.8 %collective-permute-start.34 = (bf16[512,512]{1,0:T(8,128)(2,1)S(1)}, bf16[512,512]{1,0:T(8,128)(2,1)S(1)}, u32[]{:S(2)}, u32[]{:S(2)}) collective-permute-start(bf16[512,512]{1,0:T(8,128)(2,1)S(1)} %convolution_convert_fusion.1), channel_id=1, source_target_pairs={{0,2},{1,9},{2,4},{3,11},{4,6},{5,13},{6,0},{7,15},{8,10},{9,17},{... | collective-permute-start | bytes 1572872 | tf_op jit(solution)/shard_map/ppermute | solution.py:45
  164.8 12.8 %collective-permute-start.35 = (bf16[512,512]{1,0:T(8,128)(2,1)S(1)}, bf16[512,512]{1,0:T(8,128)(2,1)S(1)}, u32[]{:S(2)}, u32[]{:S(2)}) collective-permute-start(bf16[512,512]{1,0:T(8,128)(2,1)S(1)} %convolution_convert_fusion), channel_id=1, source_target_pairs={{0,6},{1,25},{2,0},{3,27},{4,2},{5,29},{6,4},{7,31},{8,14},{9,1},{... | collective-permute-start | bytes 1572872 | tf_op jit(solution)/shard_map/ppermute | solution.py:45
  (27 other events, 266.0 us)

commit v4 on v3

--- a/solution.py
+++ b/solution.py
@@ -16,11 +16,6 @@
 epsilon = 1e-06
 f32 = jnp.float32
 bf16 = jnp.bfloat16
-
-
-def copy_for_each(value, axes):
-    copies = jnp.broadcast_to(value, (lax.axis_size(axes), *value.shape))
-    return lax.all_to_all(copies, axes, split_axis=0, concat_axis=0, tiled=True)
 
 
 def other_core(value):
@@ -261,7 +256,7 @@
     count, heads, width, _ = past.shape
     inner = heads * width
     rows = pltpu.VMEM((count, inner), f32)
-    table = jax.ShapeDtypeStruct((count, inner), f32)
+    table = pltpu.HBM((count, inner), f32)
     return pl.pallas_call(
         readout_body,
         in_specs=[
@@ -324,7 +319,7 @@
             flops=4 * 10**9, bytes_accessed=8 * 10**6, transcendentals=0
         ),
         name="state",
-    )(forget, value, in_hbm(past))
+    )(in_hbm(forget), in_hbm(value), in_hbm(past))
 
 
 def project_body(gain, *refs):
@@ -380,30 +375,42 @@
     )(*operands)
 
 
-def output_body(gathered, weight, mine, theirs, block):
-    place = lax.axis_index("x"), lax.axis_index("c")
+def output_body(*refs):
+    pieces, (weight, mine, theirs, rows, block) = refs[:4], refs[4:]
+    x, core = lax.axis_index("x"), lax.axis_index("c")
+    z, y = lax.axis_index("z"), lax.axis_index("y")
+    own = pieces[0].shape[1]
+    for m, piece in enumerate(pieces):
+        for k in range(4):
+            ahead = jnp.where(core == 0, k, m), jnp.where(core == 0, m, k)
+            owner = lax.rem(z + ahead[0], 4) * 4 + lax.rem(y + ahead[1], 4)
+            rows[pl.ds(pl.multiple_of(owner * own, own), own), :] = piece[k]
     width = mine.shape[1]
     block[...] = lax.dot_general(
-        weight[...].T, gathered[...], (((1,), (1,)), ((), ())), preferred_element_type=f32
+        weight[...].T, rows[...], (((1,), (1,)), ((), ())), preferred_element_type=f32
     )
     for k in range(4):
-        first = lax.rem(place[0] + k, 4) * 2 * width
+        first = lax.rem(x + k, 4) * 2 * width
         for side, out in enumerate((mine, theirs)):
-            row = pl.multiple_of(first + lax.rem(place[1] + side, 2) * width, width)
+            row = pl.multiple_of(first + lax.rem(core + side, 2) * width, width)
             out[k] = block[pl.ds(row, width), :].astype(bf16)
 
 
-def project_out(gathered, weight):
-    rows, width = gathered.shape[0], weight.shape[1]
+def project_out(pieces, weight):
+    rows, width = 4 * pieces[0].shape[0] * pieces[0].shape[1], weight.shape[1]
     shape = jax.ShapeDtypeStruct((4, width // 8, rows), bf16)
     return pl.pallas_call(
         output_body,
-        in_specs=[pl.BlockSpec(v.shape, lambda: (0, 0)) for v in (gathered, weight)],
+        in_specs=[pl.BlockSpec(piece.shape, lambda: (0, 0, 0)) for piece in pieces]
+        + [pl.BlockSpec(weight.shape, lambda: (0, 0))],
         out_shape=[shape, shape],
-        scratch_shapes=[pltpu.VMEM((width, rows), f32)],
+        scratch_shapes=[
+            pltpu.VMEM((rows, weight.shape[0]), bf16),
+            pltpu.VMEM((width, rows), f32),
+        ],
         compiler_params=pltpu.CompilerParams(vmem_limit_bytes=10 * 2**20),
         name="output",
-    )(gathered, weight)
+    )(*pieces, weight)
 
 
 def half_step(own, near_w, far_w, gains, near):
@@ -506,10 +513,10 @@
     summed = summed.astype(bf16)
     arrived = [summed[0]] + [shift_kv(summed[m], m, 1) for m in (2, 1, 3)]
     mixed_in, forget, value = read_out(arrived, past_state, forget_floor, head_gain)
-    new_state = update_state(forget, value, past_state)
-    gathered = copy_for_each(mixed_in, KV).reshape(-1, mixed_in.shape[1])
-    gathered, new_state = lax.optimization_barrier((gathered, new_state))
-    mine, theirs = project_out(gathered, proj_out)
+    own_axis = {k: shift_kv(mixed_in, -k, 0) for k in (2, 1, 3)}
+    line = jnp.stack([mixed_in, own_axis[1], own_axis[2], own_axis[3]])
+    other_axis = {m: shift_kv(line, -m, 1) for m in (2, 1, 3)}
+    mine, theirs = project_out([line, other_axis[1], other_axis[2], other_axis[3]], proj_out)
     mixed = (mine.astype(f32) + other_core(theirs).astype(f32)).astype(bf16)
     mixed_sum = mixed[0].astype(f32)
     for piece in [shift_x(mixed[k], k) for k in (2, 1, 3)]:
@@ -518,6 +525,7 @@
     near = plane_gather(second)
     near, far_w = lax.optimization_barrier((near, far_w))
     far_w = other_core(far_w)
+    new_state = update_state(forget, value, past_state)
     result = half_step(second, near_w, far_w, gains, near)
     return (result.T, new_state)
 

time: 194 us -> 205 us (1.057)
  waiting for transfers between devices: 56.2 us -> 79.3 us
  blocking collectives: 42.8 us -> 30.3 us
    all_to_all x3 -> x2, blocking collectives: 42.8 us -> 30.3 us  [plane_exchange(): lax.all_to_all(pieces, ALL, split_axis=0, concat_axis=0, axis_index_group...]
    ppermute x18, waiting for transfers between devices: 30.5 us -> 42.7 us  [shift(): return lax.ppermute(value, ALL, pairs)]
    ppermute x6 -> x12, waiting for transfers between devices: 4.42 us -> 13.3 us  [shift_kv(): return lax.ppermute(value, ALL, pairs)]
    ppermute x6 -> x12, starting transfers between devices: 8.31 us -> 14.8 us  [shift_kv(): return lax.ppermute(value, ALL, pairs)]
    all_to_all x1 -> x2, waiting for transfers between devices: 3.61 us -> 9.21 us  [plane_exchange(): lax.all_to_all(pieces, ALL, split_axis=0, concat_axis=0, axis_index_group...]
    all_to_all x1 -> x0, starting transfers between devices: 5.3 us -> none  [copy_for_each(): return lax.all_to_all(copies, axes, split_axis=0, concat_axis=0, tiled=True)]
    ppermute x18, starting transfers between devices: 32.6 us -> 27.6 us  [shift(): return lax.ppermute(value, ALL, pairs)]
    all_to_all x1 -> x0, waiting for transfers between devices: 4.91 us -> none  [copy_for_each(): return lax.all_to_all(copies, axes, split_axis=0, concat_axis=0, tiled=True)]
  transfers between devices with their start and end apart: 38 -> 44, of which waited for: 26 -> 31; matrix products, arithmetic and copies ran while one was open for 1% -> 0% of each run, Pallas kernels for 8% -> 8%
where the time goes in v4:
time: 205 us; the launch traced here: 204 us
  waiting for transfers between devices  79.3 us (39%)
  starting transfers between devices  62.1 us (30%)
  blocking collectives  30.3 us (15%)
  Pallas kernels  22.1 us (11%)
  local copies, waits for them, and re-layouts  3.79 us (2%)
  matrix products  3.61 us (2%)
    ppermute x18, waiting for transfers between devices, shift(): return lax.ppermute(value, ALL, pairs)  42.7 us
    all_to_all x2, blocking collectives, plane_exchange(): lax.all_to_all(pieces, ALL, split_axis=0, concat_axis=0, axis_index_group...  30.3 us
    ppermute x18, starting transfers between devices, shift(): return lax.ppermute(value, ALL, pairs)  27.6 us
    ppermute x12, starting transfers between devices, shift_kv(): return lax.ppermute(value, ALL, pairs)  14.8 us
    ppermute x12, waiting for transfers between devices, shift_kv(): return lax.ppermute(value, ALL, pairs)  13.3 us
    all_to_all x2, starting transfers between devices, plane_exchange(): lax.all_to_all(pieces, ALL, split_axis=0, concat_axis=0, axis_index_group...  11.7 us
    pallas_call x2, Pallas kernels, order_weights(): pl.pallas_call(order_body, grid=(4,), in_specs=[whole, whole, pl.BlockSpe...  10.9 us
    all_to_all x2, waiting for transfers between devices, plane_exchange(): lax.all_to_all(pieces, ALL, split_axis=0, concat_axis=0, axis_index_group...  9.21 us
  transfers between devices with their start and end apart: 44, of which 31 were waited for; matrix products, arithmetic and copies ran while one was open for 0% of the time, Pallas kernels for 8%

profile of v4, /device:TPU:0, one launch (start us, length us, event | category | flops | bytes accessed | tf_op | source)
XLA Modules:
  0.0 204.2 jit_solution(6837666225185902640)
XLA Ops:
  2.3 8.2 %all-to-all-start = ((bf16[16,32,512]{2,1,0:T(8,128)(2,1)}), bf16[16,32,512]{2,1,0:T(8,128)(2,1)S(1)}, u32[]{:S(2)}, u32[]{:S(2)}) async-start(bf16[16,32,512]{2,1,0:T(8,128)(2,1)} %broadcast_in_dim.6), calls=%async_computation | async-start | bytes 1048576 | tf_op jit(solution)/shard_map/all_to_all | solution.py:60
  10.5 5.4 %order.2 = (bf16[4,3,96,512]{3,2,1,0:T(8,128)(2,1)S(1)}, bf16[4,3,96,512]{3,2,1,0:T(8,128)(2,1)S(1)}, f32[4,512,128]{2,1,0:T(8,128)S(1)}) custom-call(s32[1,512]{1,0:T(1,128)S(1)} %get-tuple-element.97.mine, s32[1,512]{1,0:T(1,128)S(1)} %get-tuple-element.98.theirs, f32[4,1,1024]{2,1,0:T(1,128)S(1)} %bitcast.83, bf16[88,4096]{1,0:T(8,128)(2,1)} %bitcast.93, ...), custom_call_target="tpu_custom_call" | custom-call | flops 5000000000 | bytes 6000000 | tf_op jit(solution)/shard_map/order/pallas_call | solution.py:121
  17.0 3.6 %all-to-all-done = bf16[16,32,512]{2,1,0:T(8,128)(2,1)S(1)} async-done(((bf16[16,32,512]{2,1,0:T(8,128)(2,1)}), bf16[16,32,512]{2,1,0:T(8,128)(2,1)S(1)}, u32[]{:S(2)}, u32[]{:S(2)}) %all-to-all-start) | async-done | bytes 524320 | tf_op jit(solution)/shard_map/all_to_all | solution.py:60
  27.3 3.7 %collective-permute-done.refs_1_ = bf16[256,512]{1,0:T(8,128)(2,1)S(1)} collective-permute-done((bf16[256,512]{1,0:T(8,128)(2,1)S(1)}, bf16[256,512]{1,0:T(8,128)(2,1)S(1)}, u32[]{:S(2)}, u32[]{:S(2)}) %collective-permute-start) | collective-permute-done | bytes 262176 | tf_op jit(solution)/shard_map/ppermute | solution.py:40
  31.0 3.2 %collective-permute-start.4 = (bf16[256,512]{1,0:T(8,128)(2,1)S(1)}, bf16[256,512]{1,0:T(8,128)(2,1)S(1)}, u32[]{:S(2)}, u32[]{:S(2)}) collective-permute-start(bf16[256,512]{1,0:T(8,128)(2,1)S(1)} %collective-permute-done.1.refs_2_), channel_id=1, source_target_pairs={{0,6},{1,25},{2,0},{3,27},{4,2},{5,29},{6,4},{7,31},{8,14},{9,1},{... | collective-permute-start | bytes 786440 | tf_op jit(solution)/shard_map/ppermute | solution.py:40
  35.1 3.5 %collective-permute-done.3.refs_0_ = bf16[256,512]{1,0:T(8,128)(2,1)S(1)} collective-permute-done((bf16[256,512]{1,0:T(8,128)(2,1)S(1)}, bf16[256,512]{1,0:T(8,128)(2,1)S(1)}, u32[]{:S(2)}, u32[]{:S(2)}) %collective-permute-start.3) | collective-permute-done | bytes 262176 | tf_op jit(solution)/shard_map/ppermute | solution.py:40
  42.3 3.3 %collective-permute-start.10 = (bf16[512,512]{1,0:T(8,128)(2,1)S(1)}, bf16[512,512]{1,0:T(8,128)(2,1)S(1)}, u32[]{:S(2)}, u32[]{:S(2)}) collective-permute-start(bf16[512,512]{1,0:T(8,128)(2,1)S(1)} %convolution_convert_fusion.4), channel_id=1, source_target_pairs={{0,6},{1,25},{2,0},{3,27},{4,2},{5,29},{6,4},{7,31},{8,14},{9,1},{... | collective-permute-start | bytes 1572872 | tf_op jit(solution)/shard_map/ppermute | solution.py:40
  47.1 10.8 %collective-permute-done.10 = bf16[512,512]{1,0:T(8,128)(2,1)S(1)} collective-permute-done((bf16[512,512]{1,0:T(8,128)(2,1)S(1)}, bf16[512,512]{1,0:T(8,128)(2,1)S(1)}, u32[]{:S(2)}, u32[]{:S(2)}) %collective-permute-start.10) | collective-permute-done | bytes 524320 | tf_op jit(solution)/shard_map/ppermute | solution.py:40
  57.9 3.7 %collective-permute-done.9 = bf16[512,512]{1,0:T(8,128)(2,1)S(1)} collective-permute-done((bf16[512,512]{1,0:T(8,128)(2,1)S(1)}, bf16[512,512]{1,0:T(8,128)(2,1)S(1)}, u32[]{:S(2)}, u32[]{:S(2)}) %collective-permute-start.9) | collective-permute-done | bytes 524320 | tf_op jit(solution)/shard_map/ppermute | solution.py:40
  62.1 14.6 %all_to_all.20 = bf16[16,32,512]{2,1,0:T(8,128)(2,1)S(1)} all-to-all(bf16[16,32,512]{2,1,0:T(8,128)(2,1)S(1)} %bitcast.85), channel_id=1, replica_groups={{0,8,16,24,32,40,48,56,64,72,80,88,96,104,112,120},{2,10,18,26,34,42,50..., dimensions={0} | all-to-all | bytes 1048576 | tf_op jit(solution)/shard_map/all_to_all | solution.py:60
  90.3 5.4 %order.3 = (bf16[4,3,96,512]{3,2,1,0:T(8,128)(2,1)S(1)}, bf16[4,3,96,512]{3,2,1,0:T(8,128)(2,1)S(1)}, f32[4,512,128]{2,1,0:T(8,128)S(1)}) custom-call(s32[1,512]{1,0:T(1,128)S(1)} %get-tuple-element.97.mine, s32[1,512]{1,0:T(1,128)S(1)} %get-tuple-element.98.theirs, f32[4,1,1024]{2,1,0:T(1,128)S(1)} %bitcast.84, bf16[88,4096]{1,0:T(8,128)(2,1)} %bitcast.95, ...), custom_call_target="tpu_custom_call" | custom-call | flops 5000000000 | bytes 6000000 | tf_op jit(solution)/shard_map/order/pallas_call | solution.py:121
  105.8 3.4 %readout.1 = (bf16[32,256]{1,0:T(8,128)(2,1)S(1)}, f32[32,256]{1,0:T(8,128)}, f32[32,256]{1,0:T(8,128)}) custom-call(bf16[32,1152]{1,0:T(8,128)(2,1)S(1)} %get-tuple-element.89.refs_0_, bf16[32,1152]{1,0:T(8,128)(2,1)S(1)} %collective-permute-done.18.refs_1_, bf16[32,1152]{1,0:T(8,128)(2,1)S(1)} %collective-permute-done.19.refs_2_, ...), custom_call_target="tpu_custom_call" | custom-call | tf_op jit(solution)/shard_map/readout/pallas_call | solution.py:260
  115.9 3.1 %collective-permute-start.25 = (bf16[4,32,256]{2,1,0:T(8,128)(2,1)S(1)}, bf16[4,32,256]{2,1,0:T(8,128)(2,1)S(1)}, u32[]{:S(2)}, u32[]{:S(2)}) collective-permute-start(bf16[4,32,256]{2,1,0:T(8,128)(2,1)S(1)} %pad_maximum_fusion.5.refs_0_), channel_id=1, source_target_pairs={{0,16},{1,65},{2,18},{3,67},{4,20},{5,69},{6,22},{7,71},{8,24},{9,... | collective-permute-start | bytes 196616 | tf_op jit(solution)/shard_map/ppermute | solution.py:51
  126.2 2.9 %collective-permute-start.30 = (bf16[32,512]{1,0:T(8,128)(2,1)S(1)}, bf16[32,512]{1,0:T(8,128)(2,1)S(1)}, u32[]{:S(2)}, u32[]{:S(2)}) collective-permute-start(bf16[32,512]{1,0:T(8,128)(2,1)S(1)} %get-tuple-element.91), channel_id=1, source_target_pairs={{0,6},{1,7},{2,0},{3,1},{4,2},{5,3},{6,4},{7,5},{8,14},{9,15},{10,... | collective-permute-start | bytes 98312 | tf_op jit(solution)/shard_map/ppermute | solution.py:56
  130.8 3.4 %collective-permute-done.29 = bf16[32,512]{1,0:T(8,128)(2,1)S(1)} collective-permute-done((bf16[32,512]{1,0:T(8,128)(2,1)S(1)}, bf16[32,512]{1,0:T(8,128)(2,1)S(1)}, u32[]{:S(2)}, u32[]{:S(2)}) %collective-permute-start.29) | collective-permute-done | bytes 32800 | tf_op jit(solution)/shard_map/ppermute | solution.py:56
  134.3 15.7 %all_to_all.21 = bf16[16,32,512]{2,1,0:T(8,128)(2,1)S(1)} all-to-all(bf16[16,32,512]{2,1,0:T(8,128)(2,1)S(1)} %broadcast_in_dim.16), channel_id=1, replica_groups={{0,8,16,24,32,40,48,56,64,72,80,88,96,104,112,120},{2,10,18,26,34,42,50..., dimensions={0} | all-to-all | bytes 1048576 | tf_op jit(solution)/shard_map/all_to_all | solution.py:60
  152.2 3.2 %collective-permute-start.37 = (bf16[256,512]{1,0:T(8,128)(2,1)S(1)}, bf16[256,512]{1,0:T(8,128)(2,1)S(1)}, u32[]{:S(2)}, u32[]{:S(2)}) collective-permute-start(bf16[256,512]{1,0:T(8,128)(2,1)S(1)} %get-tuple-element.83), channel_id=1, source_target_pairs={{0,6},{1,25},{2,0},{3,27},{4,2},{5,29},{6,4},{7,31},{8,14},{9,1},{... | collective-permute-start | bytes 786440 | tf_op jit(solution)/shard_map/ppermute | solution.py:40
  161.8 3.5 %collective-permute-done.34.refs_0_ = bf16[256,512]{1,0:T(8,128)(2,1)S(1)} collective-permute-done((bf16[256,512]{1,0:T(8,128)(2,1)S(1)}, bf16[256,512]{1,0:T(8,128)(2,1)S(1)}, u32[]{:S(2)}, u32[]{:S(2)}) %collective-permute-start.34) | collective-permute-done | bytes 262176 | tf_op jit(solution)/shard_map/ppermute | solution.py:40
  169.2 3.3 %collective-permute-start.41 = (bf16[512,512]{1,0:T(8,128)(2,1)S(1)}, bf16[512,512]{1,0:T(8,128)(2,1)S(1)}, u32[]{:S(2)}, u32[]{:S(2)}) collective-permute-start(bf16[512,512]{1,0:T(8,128)(2,1)S(1)} %convolution_convert_fusion), channel_id=1, source_target_pairs={{0,6},{1,25},{2,0},{3,27},{4,2},{5,29},{6,4},{7,31},{8,14},{9,1},{... | collective-permute-start | bytes 1572872 | tf_op jit(solution)/shard_map/ppermute | solution.py:40
  174.1 10.8 %collective-permute-done.41 = bf16[512,512]{1,0:T(8,128)(2,1)S(1)} collective-permute-done((bf16[512,512]{1,0:T(8,128)(2,1)S(1)}, bf16[512,512]{1,0:T(8,128)(2,1)S(1)}, u32[]{:S(2)}, u32[]{:S(2)}) %collective-permute-start.41) | collective-permute-done | bytes 524320 | tf_op jit(solution)/shard_map/ppermute | solution.py:40
  184.9 3.7 %collective-permute-done.40 = bf16[512,512]{1,0:T(8,128)(2,1)S(1)} collective-permute-done((bf16[512,512]{1,0:T(8,128)(2,1)S(1)}, bf16[512,512]{1,0:T(8,128)(2,1)S(1)}, u32[]{:S(2)}, u32[]{:S(2)}) %collective-permute-start.40) | collective-permute-done | bytes 524320 | tf_op jit(solution)/shard_map/ppermute | solution.py:40
  189.8 3.6 %all-to-all-start.3 = ((bf16[16,32,512]{2,1,0:T(8,128)(2,1)}), bf16[16,32,512]{2,1,0:T(8,128)(2,1)S(1)}, u32[]{:S(2)}, u32[]{:S(2)}) async-start(bf16[16,32,512]{2,1,0:T(8,128)(2,1)} %bitcast.38), calls=%async_computation.3 | async-start | bytes 1048576 | tf_op jit(solution)/shard_map/all_to_all | solution.py:60
  193.4 4.5 %state.1 = f32[32,2,128,128]{3,2,1,0:T(8,128)} custom-call(f32[32,256]{1,0:T(8,128)} %get-tuple-element.76.forget, f32[32,256]{1,0:T(8,128)} %get-tuple-element.77.value, f32[32,2,128,128]{3,2,1,0:T(8,128)} %past.1), custom_call_target="tpu_custom_call" | custom-call | flops 4000000000 | bytes 8000000 | tf_op jit(solution)/shard_map/state/pallas_call | solution.py:306
  197.9 5.6 %all-to-all-done.3 = bf16[16,32,512]{2,1,0:T(8,128)(2,1)S(1)} async-done(((bf16[16,32,512]{2,1,0:T(8,128)(2,1)}), bf16[16,32,512]{2,1,0:T(8,128)(2,1)S(1)}, u32[]{:S(2)}, u32[]{:S(2)}) %all-to-all-start.3) | async-done | bytes 524320 | tf_op jit(solution)/shard_map/all_to_all | solution.py:60
  (136 shorter events, 70.9 us)
Async XLA Ops:
  2.3 18.3 %all-to-all-start = ((bf16[16,32,512]{2,1,0:T(8,128)(2,1)}), bf16[16,32,512]{2,1,0:T(8,128)(2,1)S(1)}, u32[]{:S(2)}, u32[]{:S(2)}) async-start(bf16[16,32,512]{2,1,0:T(8,128)(2,1)} %broadcast_in_dim.6), calls=%async_computation | async-start | bytes 1048576 | tf_op jit(solution)/shard_map/all_to_all | solution.py:60
  20.6 10.5 %collective-permute-start.2 = (bf16[4,3,96,512]{3,2,1,0:T(8,128)(2,1)}, bf16[4,3,96,512]{3,2,1,0:T(8,128)(2,1)S(1)}, u32[]{:S(2)}, u32[]{:S(2)}) collective-permute-start(bf16[4,3,96,512]{3,2,1,0:T(8,128)(2,1)} %copy-done.7), channel_id=1, source_target_pairs={{0,1},{1,0},{2,3},{3,2},{4,5},{5,4},{6,7},{7,6},{8,9},{9,8},{10,11... | collective-permute-start | bytes 3538952 | tf_op jit(solution)/shard_map/ppermute | solution.py:22
  23.4 7.6 %collective-permute-start = (bf16[256,512]{1,0:T(8,128)(2,1)S(1)}, bf16[256,512]{1,0:T(8,128)(2,1)S(1)}, u32[]{:S(2)}, u32[]{:S(2)}) collective-permute-start(bf16[256,512]{1,0:T(8,128)(2,1)S(1)} %get-tuple-element.85), channel_id=1, source_target_pairs={{0,2},{1,9},{2,4},{3,11},{4,6},{5,13},{6,0},{7,15},{8,10},{9,17},{... | collective-permute-start | bytes 786440 | tf_op jit(solution)/shard_map/ppermute | solution.py:40
  23.4 10.8 %collective-permute-start.5 = (bf16[256,512]{1,0:T(8,128)(2,1)S(1)}, bf16[256,512]{1,0:T(8,128)(2,1)S(1)}, u32[]{:S(2)}, u32[]{:S(2)}) collective-permute-start(bf16[256,512]{1,0:T(8,128)(2,1)S(1)} %get-tuple-element.84), channel_id=1, source_target_pairs={{0,2},{1,9},{2,4},{3,11},{4,6},{5,13},{6,0},{7,15},{8,10},{9,17},{... | collective-permute-start | bytes 786440 | tf_op jit(solution)/shard_map/ppermute | solution.py:40
  24.2 10.1 %collective-permute-start.6 = (bf16[256,512]{1,0:T(8,128)(2,1)S(1)}, bf16[256,512]{1,0:T(8,128)(2,1)S(1)}, u32[]{:S(2)}, u32[]{:S(2)}) collective-permute-start(bf16[256,512]{1,0:T(8,128)(2,1)S(1)} %get-tuple-element.85), channel_id=1, source_target_pairs={{0,6},{1,25},{2,0},{3,27},{4,2},{5,29},{6,4},{7,31},{8,14},{9,1},{... | collective-permute-start | bytes 786440 | tf_op jit(solution)/shard_map/ppermute | solution.py:40
  31.0 7.6 %collective-permute-start.3 = (bf16[256,512]{1,0:T(8,128)(2,1)S(1)}, bf16[256,512]{1,0:T(8,128)(2,1)S(1)}, u32[]{:S(2)}, u32[]{:S(2)}) collective-permute-start(bf16[256,512]{1,0:T(8,128)(2,1)S(1)} %collective-permute-done.refs_1_), channel_id=1, source_target_pairs={{0,2},{1,9},{2,4},{3,11},{4,6},{5,13},{6,0},{7,15},{8,10},{9,17},{... | collective-permute-start | bytes 786440 | tf_op jit(solution)/shard_map/ppermute | solution.py:40
  31.0 7.6 %collective-permute-start.4 = (bf16[256,512]{1,0:T(8,128)(2,1)S(1)}, bf16[256,512]{1,0:T(8,128)(2,1)S(1)}, u32[]{:S(2)}, u32[]{:S(2)}) collective-permute-start(bf16[256,512]{1,0:T(8,128)(2,1)S(1)} %collective-permute-done.1.refs_2_), channel_id=1, source_target_pairs={{0,6},{1,25},{2,0},{3,27},{4,2},{5,29},{6,4},{7,31},{8,14},{9,1},{... | collective-permute-start | bytes 786440 | tf_op jit(solution)/shard_map/ppermute | solution.py:40
  42.3 15.6 %collective-permute-start.10 = (bf16[512,512]{1,0:T(8,128)(2,1)S(1)}, bf16[512,512]{1,0:T(8,128)(2,1)S(1)}, u32[]{:S(2)}, u32[]{:S(2)}) collective-permute-start(bf16[512,512]{1,0:T(8,128)(2,1)S(1)} %convolution_convert_fusion.4), channel_id=1, source_target_pairs={{0,6},{1,25},{2,0},{3,27},{4,2},{5,29},{6,4},{7,31},{8,14},{9,1},{... | collective-permute-start | bytes 1572872 | tf_op jit(solution)/shard_map/ppermute | solution.py:40
  45.6 16.0 %collective-permute-start.9 = (bf16[512,512]{1,0:T(8,128)(2,1)S(1)}, bf16[512,512]{1,0:T(8,128)(2,1)S(1)}, u32[]{:S(2)}, u32[]{:S(2)}) collective-permute-start(bf16[512,512]{1,0:T(8,128)(2,1)S(1)} %convolution_convert_fusion.5), channel_id=1, source_target_pairs={{0,2},{1,9},{2,4},{3,11},{4,6},{5,13},{6,0},{7,15},{8,10},{9,17},{... | collective-permute-start | bytes 1572872 | tf_op jit(solution)/shard_map/ppermute | solution.py:40
  45.6 16.0 %collective-permute-start.8 = (bf16[512,512]{1,0:T(8,128)(2,1)S(1)}, bf16[512,512]{1,0:T(8,128)(2,1)S(1)}, u32[]{:S(2)}, u32[]{:S(2)}) collective-permute-start(bf16[512,512]{1,0:T(8,128)(2,1)S(1)} %convolution_convert_fusion.6), channel_id=1, source_target_pairs={{0,4},{1,17},{2,6},{3,19},{4,0},{5,21},{6,2},{7,23},{8,12},{9,25},... | collective-permute-start | bytes 1572872 | tf_op jit(solution)/shard_map/ppermute | solution.py:40
  78.1 6.8 %collective-permute-start.14 = (bf16[64,512]{1,0:T(8,128)(2,1)S(1)}, bf16[64,512]{1,0:T(8,128)(2,1)S(1)}, u32[]{:S(2)}, u32[]{:S(2)}) collective-permute-start(bf16[64,512]{1,0:T(8,128)(2,1)S(1)} %pad_maximum_fusion.4.refs_0_), channel_id=1, source_target_pairs={{0,2},{1,3},{2,4},{3,5},{4,6},{5,7},{6,0},{7,1},{8,10},{9,11},{10,... | collective-permute-start | bytes 196616 | tf_op jit(solution)/shard_map/ppermute | solution.py:56
  86.1 9.6 %collective-permute-start.15 = (bf16[4,32,1152]{2,1,0:T(8,128)(2,1)S(1)}, bf16[4,32,1152]{2,1,0:T(8,128)(2,1)S(1)}, u32[]{:S(2)}, u32[]{:S(2)}) collective-permute-start(bf16[4,32,1152]{2,1,0:T(8,128)(2,1)S(1)} %get-tuple-element.53), channel_id=1, source_target_pairs={{0,64},{1,17},{2,66},{3,19},{4,68},{5,21},{6,70},{7,23},{8,72},{9,... | collective-permute-start | bytes 884744 | tf_op jit(solution)/shard_map/ppermute | solution.py:51
  87.1 10.5 %collective-permute-start.16 = (bf16[4,32,1152]{2,1,0:T(8,128)(2,1)S(1)}, bf16[4,32,1152]{2,1,0:T(8,128)(2,1)S(1)}, u32[]{:S(2)}, u32[]{:S(2)}) collective-permute-start(bf16[4,32,1152]{2,1,0:T(8,128)(2,1)S(1)} %get-tuple-element.54), channel_id=1, source_target_pairs={{0,32},{1,9},{2,34},{3,11},{4,36},{5,13},{6,38},{7,15},{8,40},{9,1... | collective-permute-start | bytes 884744 | tf_op jit(solution)/shard_map/ppermute | solution.py:51
  87.9 9.7 %collective-permute-start.17 = (bf16[4,32,1152]{2,1,0:T(8,128)(2,1)S(1)}, bf16[4,32,1152]{2,1,0:T(8,128)(2,1)S(1)}, u32[]{:S(2)}, u32[]{:S(2)}) collective-permute-start(bf16[4,32,1152]{2,1,0:T(8,128)(2,1)S(1)} %get-tuple-element.55), channel_id=1, source_target_pairs={{0,96},{1,25},{2,98},{3,27},{4,100},{5,29},{6,102},{7,31},{8,104},... | collective-permute-start | bytes 884744 | tf_op jit(solution)/shard_map/ppermute | solution.py:51
  150.0 7.8 %collective-permute-start.33 = (bf16[4,3,96,512]{3,2,1,0:T(8,128)(2,1)S(1)}, bf16[4,3,96,512]{3,2,1,0:T(8,128)(2,1)S(1)}, u32[]{:S(2)}, u32[]{:S(2)}) collective-permute-start(bf16[4,3,96,512]{3,2,1,0:T(8,128)(2,1)S(1)} %get-tuple-element.69), channel_id=1, source_target_pairs={{0,1},{1,0},{2,3},{3,2},{4,5},{5,4},{6,7},{7,6},{8,9},{9,8},{10,11... | collective-permute-start | bytes 3538952 | tf_op jit(solution)/shard_map/ppermute | solution.py:22
  150.1 7.7 %collective-permute-start.31 = (bf16[256,512]{1,0:T(8,128)(2,1)S(1)}, bf16[256,512]{1,0:T(8,128)(2,1)S(1)}, u32[]{:S(2)}, u32[]{:S(2)}) collective-permute-start(bf16[256,512]{1,0:T(8,128)(2,1)S(1)} %get-tuple-element.83), channel_id=1, source_target_pairs={{0,2},{1,9},{2,4},{3,11},{4,6},{5,13},{6,0},{7,15},{8,10},{9,17},{... | collective-permute-start | bytes 786440 | tf_op jit(solution)/shard_map/ppermute | solution.py:40
  152.2 8.9 %collective-permute-start.36 = (bf16[256,512]{1,0:T(8,128)(2,1)S(1)}, bf16[256,512]{1,0:T(8,128)(2,1)S(1)}, u32[]{:S(2)}, u32[]{:S(2)}) collective-permute-start(bf16[256,512]{1,0:T(8,128)(2,1)S(1)} %get-tuple-element.82), channel_id=1, source_target_pairs={{0,2},{1,9},{2,4},{3,11},{4,6},{5,13},{6,0},{7,15},{8,10},{9,17},{... | collective-permute-start | bytes 786440 | tf_op jit(solution)/shard_map/ppermute | solution.py:40
  152.2 8.9 %collective-permute-start.37 = (bf16[256,512]{1,0:T(8,128)(2,1)S(1)}, bf16[256,512]{1,0:T(8,128)(2,1)S(1)}, u32[]{:S(2)}, u32[]{:S(2)}) collective-permute-start(bf16[256,512]{1,0:T(8,128)(2,1)S(1)} %get-tuple-element.83), channel_id=1, source_target_pairs={{0,6},{1,25},{2,0},{3,27},{4,2},{5,29},{6,4},{7,31},{8,14},{9,1},{... | collective-permute-start | bytes 786440 | tf_op jit(solution)/shard_map/ppermute | solution.py:40
  157.8 7.6 %collective-permute-start.34 = (bf16[256,512]{1,0:T(8,128)(2,1)S(1)}, bf16[256,512]{1,0:T(8,128)(2,1)S(1)}, u32[]{:S(2)}, u32[]{:S(2)}) collective-permute-start(bf16[256,512]{1,0:T(8,128)(2,1)S(1)} %collective-permute-done.31.refs_1_), channel_id=1, source_target_pairs={{0,2},{1,9},{2,4},{3,11},{4,6},{5,13},{6,0},{7,15},{8,10},{9,17},{... | collective-permute-start | bytes 786440 | tf_op jit(solution)/shard_map/ppermute | solution.py:40
  158.5 6.9 %collective-permute-start.35 = (bf16[256,512]{1,0:T(8,128)(2,1)S(1)}, bf16[256,512]{1,0:T(8,128)(2,1)S(1)}, u32[]{:S(2)}, u32[]{:S(2)}) collective-permute-start(bf16[256,512]{1,0:T(8,128)(2,1)S(1)} %collective-permute-done.32.refs_2_), channel_id=1, source_target_pairs={{0,6},{1,25},{2,0},{3,27},{4,2},{5,29},{6,4},{7,31},{8,14},{9,1},{... | collective-permute-start | bytes 786440 | tf_op jit(solution)/shard_map/ppermute | solution.py:40
  169.2 15.6 %collective-permute-start.41 = (bf16[512,512]{1,0:T(8,128)(2,1)S(1)}, bf16[512,512]{1,0:T(8,128)(2,1)S(1)}, u32[]{:S(2)}, u32[]{:S(2)}) collective-permute-start(bf16[512,512]{1,0:T(8,128)(2,1)S(1)} %convolution_convert_fusion), channel_id=1, source_target_pairs={{0,6},{1,25},{2,0},{3,27},{4,2},{5,29},{6,4},{7,31},{8,14},{9,1},{... | collective-permute-start | bytes 1572872 | tf_op jit(solution)/shard_map/ppermute | solution.py:40
  172.5 16.0 %collective-permute-start.40 = (bf16[512,512]{1,0:T(8,128)(2,1)S(1)}, bf16[512,512]{1,0:T(8,128)(2,1)S(1)}, u32[]{:S(2)}, u32[]{:S(2)}) collective-permute-start(bf16[512,512]{1,0:T(8,128)(2,1)S(1)} %convolution_convert_fusion.1), channel_id=1, source_target_pairs={{0,2},{1,9},{2,4},{3,11},{4,6},{5,13},{6,0},{7,15},{8,10},{9,17},{... | collective-permute-start | bytes 1572872 | tf_op jit(solution)/shard_map/ppermute | solution.py:40
  172.5 16.0 %collective-permute-start.39 = (bf16[512,512]{1,0:T(8,128)(2,1)S(1)}, bf16[512,512]{1,0:T(8,128)(2,1)S(1)}, u32[]{:S(2)}, u32[]{:S(2)}) collective-permute-start(bf16[512,512]{1,0:T(8,128)(2,1)S(1)} %convolution_convert_fusion.2), channel_id=1, source_target_pairs={{0,4},{1,17},{2,6},{3,19},{4,0},{5,21},{6,2},{7,23},{8,12},{9,25},... | collective-permute-start | bytes 1572872 | tf_op jit(solution)/shard_map/ppermute | solution.py:40
  189.8 13.7 %all-to-all-start.3 = ((bf16[16,32,512]{2,1,0:T(8,128)(2,1)}), bf16[16,32,512]{2,1,0:T(8,128)(2,1)S(1)}, u32[]{:S(2)}, u32[]{:S(2)}) async-start(bf16[16,32,512]{2,1,0:T(8,128)(2,1)} %bitcast.38), calls=%async_computation.3 | async-start | bytes 1048576 | tf_op jit(solution)/shard_map/all_to_all | solution.py:60
  (31 other events, 264.0 us)

commit v5 on v3

--- a/solution.py
+++ b/solution.py
@@ -261,7 +261,7 @@
     count, heads, width, _ = past.shape
     inner = heads * width
     rows = pltpu.VMEM((count, inner), f32)
-    table = jax.ShapeDtypeStruct((count, inner), f32)
+    table = pltpu.HBM((count, inner), f32)
     return pl.pallas_call(
         readout_body,
         in_specs=[
@@ -324,7 +324,7 @@
             flops=4 * 10**9, bytes_accessed=8 * 10**6, transcendentals=0
         ),
         name="state",
-    )(forget, value, in_hbm(past))
+    )(in_hbm(forget), in_hbm(value), in_hbm(past))
 
 
 def project_body(gain, *refs):
@@ -442,7 +442,7 @@
     deep = jnp.concatenate([near_w[:, 2], far_w[:, 2]], axis=1)
 
     sums, arrived = {}, []
-    for k in (2, 1, 3, 0):
+    for k in (1, 3, 2, 0):
         sums[k] = lax.dot_general(
             deep[k], hidden, (((0,), (0,)), ((), ())), preferred_element_type=f32
         ).astype(bf16)
@@ -506,9 +506,7 @@
     summed = summed.astype(bf16)
     arrived = [summed[0]] + [shift_kv(summed[m], m, 1) for m in (2, 1, 3)]
     mixed_in, forget, value = read_out(arrived, past_state, forget_floor, head_gain)
-    new_state = update_state(forget, value, past_state)
     gathered = copy_for_each(mixed_in, KV).reshape(-1, mixed_in.shape[1])
-    gathered, new_state = lax.optimization_barrier((gathered, new_state))
     mine, theirs = project_out(gathered, proj_out)
     mixed = (mine.astype(f32) + other_core(theirs).astype(f32)).astype(bf16)
     mixed_sum = mixed[0].astype(f32)
@@ -518,6 +516,7 @@
     near = plane_gather(second)
     near, far_w = lax.optimization_barrier((near, far_w))
     far_w = other_core(far_w)
+    new_state = update_state(forget, value, past_state)
     result = half_step(second, near_w, far_w, gains, near)
     return (result.T, new_state)
 

time: 194 us -> 198 us (1.021)
  waiting for transfers between devices: 56.2 us -> 69.7 us
  starting transfers between devices: 62.9 us -> 54.2 us
    all_to_all x3 -> x2, blocking collectives: 42.8 us -> 27.6 us  [plane_exchange(): lax.all_to_all(pieces, ALL, split_axis=0, concat_axis=0, axis_index_group...]
    all_to_all x0 -> x1, blocking collectives: none -> 13.6 us  [copy_for_each(): return lax.all_to_all(copies, axes, split_axis=0, concat_axis=0, tiled=True)]
    ppermute x18, waiting for transfers between devices: 30.5 us -> 39.8 us  [shift(): return lax.ppermute(value, ALL, pairs)]
    ppermute x18, starting transfers between devices: 32.6 us -> 26.2 us  [shift(): return lax.ppermute(value, ALL, pairs)]
    all_to_all x1 -> x2, waiting for transfers between devices: 3.61 us -> 9.62 us  [plane_exchange(): lax.all_to_all(pieces, ALL, split_axis=0, concat_axis=0, axis_index_group...]
    all_to_all x1 -> x0, starting transfers between devices: 5.3 us -> none  [copy_for_each(): return lax.all_to_all(copies, axes, split_axis=0, concat_axis=0, tiled=True)]
    all_to_all x1 -> x0, waiting for transfers between devices: 4.91 us -> none  [copy_for_each(): return lax.all_to_all(copies, axes, split_axis=0, concat_axis=0, tiled=True)]
    all_to_all x1 -> x2, starting transfers between devices: 8.16 us -> 11.7 us  [plane_exchange(): lax.all_to_all(pieces, ALL, split_axis=0, concat_axis=0, axis_index_group...]
  transfers between devices with their start and end apart: 38 -> 38, of which waited for: 26 -> 26; matrix products, arithmetic and copies ran while one was open for 1% -> 0% of each run, Pallas kernels for 8% -> 9%
where the time goes in v5:
time: 198 us
  waiting for transfers between devices  69.7 us (35%)
  starting transfers between devices  54.2 us (27%)
  blocking collectives  41.2 us (21%)
  Pallas kernels  22 us (11%)
  local copies, waits for them, and re-layouts  3.81 us (2%)
  matrix products  3.61 us (2%)
    ppermute x18, waiting for transfers between devices, shift(): return lax.ppermute(value, ALL, pairs)  39.8 us
    all_to_all x2, blocking collectives, plane_exchange(): lax.all_to_all(pieces, ALL, split_axis=0, concat_axis=0, axis_index_group...  27.6 us
    ppermute x18, starting transfers between devices, shift(): return lax.ppermute(value, ALL, pairs)  26.2 us
    all_to_all x1, blocking collectives, copy_for_each(): return lax.all_to_all(copies, axes, split_axis=0, concat_axis=0, tiled=True)  13.6 us
    all_to_all x2, starting transfers between devices, plane_exchange(): lax.all_to_all(pieces, ALL, split_axis=0, concat_axis=0, axis_index_group...  11.7 us
    pallas_call x2, Pallas kernels, order_weights(): pl.pallas_call(order_body, grid=(4,), in_specs=[whole, whole, pl.BlockSpe...  10.8 us
    all_to_all x2, waiting for transfers between devices, plane_exchange(): lax.all_to_all(pieces, ALL, split_axis=0, concat_axis=0, axis_index_group...  9.62 us
    ppermute x6, waiting for transfers between devices, shift_x(): return lax.ppermute(value, ALL, pairs)  8.43 us
  transfers between devices with their start and end apart: 38, of which 26 were waited for; matrix products, arithmetic and copies ran while one was open for 0% of the time, Pallas kernels for 9%

profile of v5, /device:TPU:0, one launch (start us, length us, event | category | flops | bytes accessed | tf_op | source)
XLA Modules:
  0.0 197.5 jit_solution(3098559509773157604)
XLA Ops:
  2.3 8.2 %all-to-all-start = ((bf16[16,32,512]{2,1,0:T(8,128)(2,1)}), bf16[16,32,512]{2,1,0:T(8,128)(2,1)S(1)}, u32[]{:S(2)}, u32[]{:S(2)}) async-start(bf16[16,32,512]{2,1,0:T(8,128)(2,1)} %broadcast_in_dim.8), calls=%async_computation | async-start | bytes 1048576 | tf_op jit(solution)/shard_map/all_to_all | solution.py:65
  10.5 5.4 %order.2 = (bf16[4,3,96,512]{3,2,1,0:T(8,128)(2,1)S(1)}, bf16[4,3,96,512]{3,2,1,0:T(8,128)(2,1)S(1)}, f32[4,512,128]{2,1,0:T(8,128)S(1)}) custom-call(s32[1,512]{1,0:T(1,128)S(1)} %get-tuple-element.97.mine, s32[1,512]{1,0:T(1,128)S(1)} %get-tuple-element.98.theirs, f32[4,1,1024]{2,1,0:T(1,128)S(1)} %bitcast.80, bf16[88,4096]{1,0:T(8,128)(2,1)} %bitcast.87, ...), custom_call_target="tpu_custom_call" | custom-call | flops 5000000000 | bytes 6000000 | tf_op jit(solution)/shard_map/order/pallas_call | solution.py:126
  17.0 3.6 %all-to-all-done = bf16[16,32,512]{2,1,0:T(8,128)(2,1)S(1)} async-done(((bf16[16,32,512]{2,1,0:T(8,128)(2,1)}), bf16[16,32,512]{2,1,0:T(8,128)(2,1)S(1)}, u32[]{:S(2)}, u32[]{:S(2)}) %all-to-all-start) | async-done | bytes 524320 | tf_op jit(solution)/shard_map/all_to_all | solution.py:65
  27.3 3.7 %collective-permute-done.refs_1_ = bf16[256,512]{1,0:T(8,128)(2,1)S(1)} collective-permute-done((bf16[256,512]{1,0:T(8,128)(2,1)S(1)}, bf16[256,512]{1,0:T(8,128)(2,1)S(1)}, u32[]{:S(2)}, u32[]{:S(2)}) %collective-permute-start) | collective-permute-done | bytes 262176 | tf_op jit(solution)/shard_map/ppermute | solution.py:45
  31.0 3.2 %collective-permute-start.4 = (bf16[256,512]{1,0:T(8,128)(2,1)S(1)}, bf16[256,512]{1,0:T(8,128)(2,1)S(1)}, u32[]{:S(2)}, u32[]{:S(2)}) collective-permute-start(bf16[256,512]{1,0:T(8,128)(2,1)S(1)} %collective-permute-done.1.refs_2_), channel_id=1, source_target_pairs={{0,6},{1,25},{2,0},{3,27},{4,2},{5,29},{6,4},{7,31},{8,14},{9,1},{... | collective-permute-start | bytes 786440 | tf_op jit(solution)/shard_map/ppermute | solution.py:45
  35.1 3.5 %collective-permute-done.3.refs_0_ = bf16[256,512]{1,0:T(8,128)(2,1)S(1)} collective-permute-done((bf16[256,512]{1,0:T(8,128)(2,1)S(1)}, bf16[256,512]{1,0:T(8,128)(2,1)S(1)}, u32[]{:S(2)}, u32[]{:S(2)}) %collective-permute-start.3) | collective-permute-done | bytes 262176 | tf_op jit(solution)/shard_map/ppermute | solution.py:45
  46.4 6.7 %collective-permute-done.10 = bf16[512,512]{1,0:T(8,128)(2,1)S(1)} collective-permute-done((bf16[512,512]{1,0:T(8,128)(2,1)S(1)}, bf16[512,512]{1,0:T(8,128)(2,1)S(1)}, u32[]{:S(2)}, u32[]{:S(2)}) %collective-permute-start.10) | collective-permute-done | bytes 524320 | tf_op jit(solution)/shard_map/ppermute | solution.py:45
  53.1 6.1 %collective-permute-done.9 = bf16[512,512]{1,0:T(8,128)(2,1)S(1)} collective-permute-done((bf16[512,512]{1,0:T(8,128)(2,1)S(1)}, bf16[512,512]{1,0:T(8,128)(2,1)S(1)}, u32[]{:S(2)}, u32[]{:S(2)}) %collective-permute-start.9) | collective-permute-done | bytes 524320 | tf_op jit(solution)/shard_map/ppermute | solution.py:45
  59.7 14.6 %all_to_all.25 = bf16[16,32,512]{2,1,0:T(8,128)(2,1)S(1)} all-to-all(bf16[16,32,512]{2,1,0:T(8,128)(2,1)S(1)} %bitcast.82), channel_id=1, replica_groups={{0,8,16,24,32,40,48,56,64,72,80,88,96,104,112,120},{2,10,18,26,34,42,50..., dimensions={0} | all-to-all | bytes 1048576 | tf_op jit(solution)/shard_map/all_to_all | solution.py:65
  75.8 3.9 %collective-permute-start.13 = (bf16[64,512]{1,0:T(8,128)(2,1)S(1)}, bf16[64,512]{1,0:T(8,128)(2,1)S(1)}, u32[]{:S(2)}, u32[]{:S(2)}) collective-permute-start(bf16[64,512]{1,0:T(8,128)(2,1)S(1)} %pad_maximum_fusion.4.refs_0_), channel_id=1, source_target_pairs={{0,4},{1,5},{2,6},{3,7},{4,0},{5,1},{6,2},{7,3},{8,12},{9,13},{10,... | collective-permute-start | bytes 196616 | tf_op jit(solution)/shard_map/ppermute | solution.py:61
  88.8 5.4 %order.3 = (bf16[4,3,96,512]{3,2,1,0:T(8,128)(2,1)S(1)}, bf16[4,3,96,512]{3,2,1,0:T(8,128)(2,1)S(1)}, f32[4,512,128]{2,1,0:T(8,128)S(1)}) custom-call(s32[1,512]{1,0:T(1,128)S(1)} %get-tuple-element.97.mine, s32[1,512]{1,0:T(1,128)S(1)} %get-tuple-element.98.theirs, f32[4,1,1024]{2,1,0:T(1,128)S(1)} %bitcast.81, bf16[88,4096]{1,0:T(8,128)(2,1)} %bitcast.89, ...), custom_call_target="tpu_custom_call" | custom-call | flops 5000000000 | bytes 6000000 | tf_op jit(solution)/shard_map/order/pallas_call | solution.py:126
  100.7 2.8 %collective-permute-done.19.refs_2_ = bf16[32,1152]{1,0:T(8,128)(2,1)S(1)} collective-permute-done((bf16[32,1152]{1,0:T(8,128)(2,1)S(1)}, bf16[32,1152]{1,0:T(8,128)(2,1)S(1)}, u32[]{:S(2)}, u32[]{:S(2)}) %collective-permute-start.19) | collective-permute-done | bytes 73760 | tf_op jit(solution)/shard_map/ppermute | solution.py:56
  104.3 3.4 %readout.1 = (bf16[32,256]{1,0:T(8,128)(2,1)S(1)}, f32[32,256]{1,0:T(8,128)}, f32[32,256]{1,0:T(8,128)}) custom-call(bf16[32,1152]{1,0:T(8,128)(2,1)S(1)} %get-tuple-element.89.refs_0_, bf16[32,1152]{1,0:T(8,128)(2,1)S(1)} %collective-permute-done.18.refs_1_, bf16[32,1152]{1,0:T(8,128)(2,1)S(1)} %collective-permute-done.19.refs_2_, ...), custom_call_target="tpu_custom_call" | custom-call | tf_op jit(solution)/shard_map/readout/pallas_call | solution.py:265
  107.7 13.6 %all_to_all.26 = bf16[16,32,256]{2,1,0:T(8,128)(2,1)S(1)} all-to-all(bf16[16,32,256]{2,1,0:T(8,128)(2,1)S(1)} %broadcast_in_dim.19), channel_id=1, replica_groups=mesh['z'=4,'y'=4,'x'=4,'c'=2] {'z','y'}, dimensions={0} | all-to-all | bytes 524288 | tf_op jit(solution)/shard_map/all_to_all | solution.py:23
  128.8 3.2 %collective-permute-done.23 = bf16[32,512]{1,0:T(8,128)(2,1)S(1)} collective-permute-done((bf16[32,512]{1,0:T(8,128)(2,1)S(1)}, bf16[32,512]{1,0:T(8,128)(2,1)S(1)}, u32[]{:S(2)}, u32[]{:S(2)}) %collective-permute-start.23) | collective-permute-done | bytes 32800 | tf_op jit(solution)/shard_map/ppermute | solution.py:61
  132.1 13.0 %all_to_all.27 = bf16[16,32,512]{2,1,0:T(8,128)(2,1)S(1)} all-to-all(bf16[16,32,512]{2,1,0:T(8,128)(2,1)S(1)} %broadcast_in_dim.20), channel_id=1, replica_groups={{0,8,16,24,32,40,48,56,64,72,80,88,96,104,112,120},{2,10,18,26,34,42,50..., dimensions={0} | all-to-all | bytes 1048576 | tf_op jit(solution)/shard_map/all_to_all | solution.py:65
  147.3 3.2 %collective-permute-start.31 = (bf16[256,512]{1,0:T(8,128)(2,1)S(1)}, bf16[256,512]{1,0:T(8,128)(2,1)S(1)}, u32[]{:S(2)}, u32[]{:S(2)}) collective-permute-start(bf16[256,512]{1,0:T(8,128)(2,1)S(1)} %get-tuple-element.83), channel_id=1, source_target_pairs={{0,6},{1,25},{2,0},{3,27},{4,2},{5,29},{6,4},{7,31},{8,14},{9,1},{... | collective-permute-start | bytes 786440 | tf_op jit(solution)/shard_map/ppermute | solution.py:45
  153.6 2.9 %collective-permute-start.29 = (bf16[256,512]{1,0:T(8,128)(2,1)S(1)}, bf16[256,512]{1,0:T(8,128)(2,1)S(1)}, u32[]{:S(2)}, u32[]{:S(2)}) collective-permute-start(bf16[256,512]{1,0:T(8,128)(2,1)S(1)} %collective-permute-done.26.refs_2_), channel_id=1, source_target_pairs={{0,6},{1,25},{2,0},{3,27},{4,2},{5,29},{6,4},{7,31},{8,14},{9,1},{... | collective-permute-start | bytes 786440 | tf_op jit(solution)/shard_map/ppermute | solution.py:45
  157.4 3.5 %collective-permute-done.28.refs_0_ = bf16[256,512]{1,0:T(8,128)(2,1)S(1)} collective-permute-done((bf16[256,512]{1,0:T(8,128)(2,1)S(1)}, bf16[256,512]{1,0:T(8,128)(2,1)S(1)}, u32[]{:S(2)}, u32[]{:S(2)}) %collective-permute-start.28) | collective-permute-done | bytes 262176 | tf_op jit(solution)/shard_map/ppermute | solution.py:45
  168.7 6.7 %collective-permute-done.35 = bf16[512,512]{1,0:T(8,128)(2,1)S(1)} collective-permute-done((bf16[512,512]{1,0:T(8,128)(2,1)S(1)}, bf16[512,512]{1,0:T(8,128)(2,1)S(1)}, u32[]{:S(2)}, u32[]{:S(2)}) %collective-permute-start.35) | collective-permute-done | bytes 524320 | tf_op jit(solution)/shard_map/ppermute | solution.py:45
  175.4 6.1 %collective-permute-done.34 = bf16[512,512]{1,0:T(8,128)(2,1)S(1)} collective-permute-done((bf16[512,512]{1,0:T(8,128)(2,1)S(1)}, bf16[512,512]{1,0:T(8,128)(2,1)S(1)}, u32[]{:S(2)}, u32[]{:S(2)}) %collective-permute-start.34) | collective-permute-done | bytes 524320 | tf_op jit(solution)/shard_map/ppermute | solution.py:45
  182.7 3.6 %all-to-all-start.4 = ((bf16[16,32,512]{2,1,0:T(8,128)(2,1)}), bf16[16,32,512]{2,1,0:T(8,128)(2,1)S(1)}, u32[]{:S(2)}, u32[]{:S(2)}) async-start(bf16[16,32,512]{2,1,0:T(8,128)(2,1)} %bitcast.35), calls=%async_computation.4 | async-start | bytes 1048576 | tf_op jit(solution)/shard_map/all_to_all | solution.py:65
  186.3 4.5 %state.1 = f32[32,2,128,128]{3,2,1,0:T(8,128)} custom-call(f32[32,256]{1,0:T(8,128)} %get-tuple-element.76.forget, f32[32,256]{1,0:T(8,128)} %get-tuple-element.77.value, f32[32,2,128,128]{3,2,1,0:T(8,128)} %past.1), custom_call_target="tpu_custom_call" | custom-call | flops 4000000000 | bytes 8000000 | tf_op jit(solution)/shard_map/state/pallas_call | solution.py:311
  190.8 6.0 %all-to-all-done.4 = bf16[16,32,512]{2,1,0:T(8,128)(2,1)S(1)} async-done(((bf16[16,32,512]{2,1,0:T(8,128)(2,1)}), bf16[16,32,512]{2,1,0:T(8,128)(2,1)S(1)}, u32[]{:S(2)}, u32[]{:S(2)}) %all-to-all-start.4) | async-done | bytes 524320 | tf_op jit(solution)/shard_map/all_to_all | solution.py:65
  (125 shorter events, 59.5 us)
Async XLA Ops:
  2.3 18.3 %all-to-all-start = ((bf16[16,32,512]{2,1,0:T(8,128)(2,1)}), bf16[16,32,512]{2,1,0:T(8,128)(2,1)S(1)}, u32[]{:S(2)}, u32[]{:S(2)}) async-start(bf16[16,32,512]{2,1,0:T(8,128)(2,1)} %broadcast_in_dim.8), calls=%async_computation | async-start | bytes 1048576 | tf_op jit(solution)/shard_map/all_to_all | solution.py:65
  20.6 10.5 %collective-permute-start.2 = (bf16[4,3,96,512]{3,2,1,0:T(8,128)(2,1)}, bf16[4,3,96,512]{3,2,1,0:T(8,128)(2,1)S(1)}, u32[]{:S(2)}, u32[]{:S(2)}) collective-permute-start(bf16[4,3,96,512]{3,2,1,0:T(8,128)(2,1)} %copy-done.7), channel_id=1, source_target_pairs={{0,1},{1,0},{2,3},{3,2},{4,5},{5,4},{6,7},{7,6},{8,9},{9,8},{10,11... | collective-permute-start | bytes 3538952 | tf_op jit(solution)/shard_map/ppermute | solution.py:27
  23.4 7.6 %collective-permute-start = (bf16[256,512]{1,0:T(8,128)(2,1)S(1)}, bf16[256,512]{1,0:T(8,128)(2,1)S(1)}, u32[]{:S(2)}, u32[]{:S(2)}) collective-permute-start(bf16[256,512]{1,0:T(8,128)(2,1)S(1)} %get-tuple-element.85), channel_id=1, source_target_pairs={{0,2},{1,9},{2,4},{3,11},{4,6},{5,13},{6,0},{7,15},{8,10},{9,17},{... | collective-permute-start | bytes 786440 | tf_op jit(solution)/shard_map/ppermute | solution.py:45
  23.4 10.8 %collective-permute-start.5 = (bf16[256,512]{1,0:T(8,128)(2,1)S(1)}, bf16[256,512]{1,0:T(8,128)(2,1)S(1)}, u32[]{:S(2)}, u32[]{:S(2)}) collective-permute-start(bf16[256,512]{1,0:T(8,128)(2,1)S(1)} %get-tuple-element.84), channel_id=1, source_target_pairs={{0,2},{1,9},{2,4},{3,11},{4,6},{5,13},{6,0},{7,15},{8,10},{9,17},{... | collective-permute-start | bytes 786440 | tf_op jit(solution)/shard_map/ppermute | solution.py:45
  24.2 10.1 %collective-permute-start.6 = (bf16[256,512]{1,0:T(8,128)(2,1)S(1)}, bf16[256,512]{1,0:T(8,128)(2,1)S(1)}, u32[]{:S(2)}, u32[]{:S(2)}) collective-permute-start(bf16[256,512]{1,0:T(8,128)(2,1)S(1)} %get-tuple-element.85), channel_id=1, source_target_pairs={{0,6},{1,25},{2,0},{3,27},{4,2},{5,29},{6,4},{7,31},{8,14},{9,1},{... | collective-permute-start | bytes 786440 | tf_op jit(solution)/shard_map/ppermute | solution.py:45
  31.0 7.6 %collective-permute-start.3 = (bf16[256,512]{1,0:T(8,128)(2,1)S(1)}, bf16[256,512]{1,0:T(8,128)(2,1)S(1)}, u32[]{:S(2)}, u32[]{:S(2)}) collective-permute-start(bf16[256,512]{1,0:T(8,128)(2,1)S(1)} %collective-permute-done.refs_1_), channel_id=1, source_target_pairs={{0,2},{1,9},{2,4},{3,11},{4,6},{5,13},{6,0},{7,15},{8,10},{9,17},{... | collective-permute-start | bytes 786440 | tf_op jit(solution)/shard_map/ppermute | solution.py:45
  31.0 7.6 %collective-permute-start.4 = (bf16[256,512]{1,0:T(8,128)(2,1)S(1)}, bf16[256,512]{1,0:T(8,128)(2,1)S(1)}, u32[]{:S(2)}, u32[]{:S(2)}) collective-permute-start(bf16[256,512]{1,0:T(8,128)(2,1)S(1)} %collective-permute-done.1.refs_2_), channel_id=1, source_target_pairs={{0,6},{1,25},{2,0},{3,27},{4,2},{5,29},{6,4},{7,31},{8,14},{9,1},{... | collective-permute-start | bytes 786440 | tf_op jit(solution)/shard_map/ppermute | solution.py:45
  42.3 10.9 %collective-permute-start.10 = (bf16[512,512]{1,0:T(8,128)(2,1)S(1)}, bf16[512,512]{1,0:T(8,128)(2,1)S(1)}, u32[]{:S(2)}, u32[]{:S(2)}) collective-permute-start(bf16[512,512]{1,0:T(8,128)(2,1)S(1)} %convolution_convert_fusion.4), channel_id=1, source_target_pairs={{0,4},{1,17},{2,6},{3,19},{4,0},{5,21},{6,2},{7,23},{8,12},{9,25},... | collective-permute-start | bytes 1572872 | tf_op jit(solution)/shard_map/ppermute | solution.py:45
  43.8 15.4 %collective-permute-start.9 = (bf16[512,512]{1,0:T(8,128)(2,1)S(1)}, bf16[512,512]{1,0:T(8,128)(2,1)S(1)}, u32[]{:S(2)}, u32[]{:S(2)}) collective-permute-start(bf16[512,512]{1,0:T(8,128)(2,1)S(1)} %convolution_convert_fusion.5), channel_id=1, source_target_pairs={{0,6},{1,25},{2,0},{3,27},{4,2},{5,29},{6,4},{7,31},{8,14},{9,1},{... | collective-permute-start | bytes 1572872 | tf_op jit(solution)/shard_map/ppermute | solution.py:45
  45.7 13.6 %collective-permute-start.8 = (bf16[512,512]{1,0:T(8,128)(2,1)S(1)}, bf16[512,512]{1,0:T(8,128)(2,1)S(1)}, u32[]{:S(2)}, u32[]{:S(2)}) collective-permute-start(bf16[512,512]{1,0:T(8,128)(2,1)S(1)} %convolution_convert_fusion.6), channel_id=1, source_target_pairs={{0,2},{1,9},{2,4},{3,11},{4,6},{5,13},{6,0},{7,15},{8,10},{9,17},{... | collective-permute-start | bytes 1572872 | tf_op jit(solution)/shard_map/ppermute | solution.py:45
  75.8 7.4 %collective-permute-start.13 = (bf16[64,512]{1,0:T(8,128)(2,1)S(1)}, bf16[64,512]{1,0:T(8,128)(2,1)S(1)}, u32[]{:S(2)}, u32[]{:S(2)}) collective-permute-start(bf16[64,512]{1,0:T(8,128)(2,1)S(1)} %pad_maximum_fusion.4.refs_0_), channel_id=1, source_target_pairs={{0,4},{1,5},{2,6},{3,7},{4,0},{5,1},{6,2},{7,3},{8,12},{9,13},{10,... | collective-permute-start | bytes 196616 | tf_op jit(solution)/shard_map/ppermute | solution.py:61
  84.6 9.6 %collective-permute-start.15 = (bf16[4,32,1152]{2,1,0:T(8,128)(2,1)S(1)}, bf16[4,32,1152]{2,1,0:T(8,128)(2,1)S(1)}, u32[]{:S(2)}, u32[]{:S(2)}) collective-permute-start(bf16[4,32,1152]{2,1,0:T(8,128)(2,1)S(1)} %get-tuple-element.53), channel_id=1, source_target_pairs={{0,64},{1,17},{2,66},{3,19},{4,68},{5,21},{6,70},{7,23},{8,72},{9,... | collective-permute-start | bytes 884744 | tf_op jit(solution)/shard_map/ppermute | solution.py:56
  85.5 10.5 %collective-permute-start.16 = (bf16[4,32,1152]{2,1,0:T(8,128)(2,1)S(1)}, bf16[4,32,1152]{2,1,0:T(8,128)(2,1)S(1)}, u32[]{:S(2)}, u32[]{:S(2)}) collective-permute-start(bf16[4,32,1152]{2,1,0:T(8,128)(2,1)S(1)} %get-tuple-element.54), channel_id=1, source_target_pairs={{0,32},{1,9},{2,34},{3,11},{4,36},{5,13},{6,38},{7,15},{8,40},{9,1... | collective-permute-start | bytes 884744 | tf_op jit(solution)/shard_map/ppermute | solution.py:56
  86.4 9.7 %collective-permute-start.17 = (bf16[4,32,1152]{2,1,0:T(8,128)(2,1)S(1)}, bf16[4,32,1152]{2,1,0:T(8,128)(2,1)S(1)}, u32[]{:S(2)}, u32[]{:S(2)}) collective-permute-start(bf16[4,32,1152]{2,1,0:T(8,128)(2,1)S(1)} %get-tuple-element.55), channel_id=1, source_target_pairs={{0,96},{1,25},{2,98},{3,27},{4,100},{5,29},{6,102},{7,31},{8,104},... | collective-permute-start | bytes 884744 | tf_op jit(solution)/shard_map/ppermute | solution.py:56
  145.1 8.2 %collective-permute-start.27 = (bf16[4,3,96,512]{3,2,1,0:T(8,128)(2,1)S(1)}, bf16[4,3,96,512]{3,2,1,0:T(8,128)(2,1)S(1)}, u32[]{:S(2)}, u32[]{:S(2)}) collective-permute-start(bf16[4,3,96,512]{3,2,1,0:T(8,128)(2,1)S(1)} %get-tuple-element.69), channel_id=1, source_target_pairs={{0,1},{1,0},{2,3},{3,2},{4,5},{5,4},{6,7},{7,6},{8,9},{9,8},{10,11... | collective-permute-start | bytes 3538952 | tf_op jit(solution)/shard_map/ppermute | solution.py:27
  145.7 7.6 %collective-permute-start.25 = (bf16[256,512]{1,0:T(8,128)(2,1)S(1)}, bf16[256,512]{1,0:T(8,128)(2,1)S(1)}, u32[]{:S(2)}, u32[]{:S(2)}) collective-permute-start(bf16[256,512]{1,0:T(8,128)(2,1)S(1)} %get-tuple-element.83), channel_id=1, source_target_pairs={{0,2},{1,9},{2,4},{3,11},{4,6},{5,13},{6,0},{7,15},{8,10},{9,17},{... | collective-permute-start | bytes 786440 | tf_op jit(solution)/shard_map/ppermute | solution.py:45
  147.2 9.3 %collective-permute-start.30 = (bf16[256,512]{1,0:T(8,128)(2,1)S(1)}, bf16[256,512]{1,0:T(8,128)(2,1)S(1)}, u32[]{:S(2)}, u32[]{:S(2)}) collective-permute-start(bf16[256,512]{1,0:T(8,128)(2,1)S(1)} %get-tuple-element.82), channel_id=1, source_target_pairs={{0,2},{1,9},{2,4},{3,11},{4,6},{5,13},{6,0},{7,15},{8,10},{9,17},{... | collective-permute-start | bytes 786440 | tf_op jit(solution)/shard_map/ppermute | solution.py:45
  147.3 9.3 %collective-permute-start.31 = (bf16[256,512]{1,0:T(8,128)(2,1)S(1)}, bf16[256,512]{1,0:T(8,128)(2,1)S(1)}, u32[]{:S(2)}, u32[]{:S(2)}) collective-permute-start(bf16[256,512]{1,0:T(8,128)(2,1)S(1)} %get-tuple-element.83), channel_id=1, source_target_pairs={{0,6},{1,25},{2,0},{3,27},{4,2},{5,29},{6,4},{7,31},{8,14},{9,1},{... | collective-permute-start | bytes 786440 | tf_op jit(solution)/shard_map/ppermute | solution.py:45
  153.3 7.6 %collective-permute-start.28 = (bf16[256,512]{1,0:T(8,128)(2,1)S(1)}, bf16[256,512]{1,0:T(8,128)(2,1)S(1)}, u32[]{:S(2)}, u32[]{:S(2)}) collective-permute-start(bf16[256,512]{1,0:T(8,128)(2,1)S(1)} %collective-permute-done.25.refs_1_), channel_id=1, source_target_pairs={{0,2},{1,9},{2,4},{3,11},{4,6},{5,13},{6,0},{7,15},{8,10},{9,17},{... | collective-permute-start | bytes 786440 | tf_op jit(solution)/shard_map/ppermute | solution.py:45
  153.6 7.3 %collective-permute-start.29 = (bf16[256,512]{1,0:T(8,128)(2,1)S(1)}, bf16[256,512]{1,0:T(8,128)(2,1)S(1)}, u32[]{:S(2)}, u32[]{:S(2)}) collective-permute-start(bf16[256,512]{1,0:T(8,128)(2,1)S(1)} %collective-permute-done.26.refs_2_), channel_id=1, source_target_pairs={{0,6},{1,25},{2,0},{3,27},{4,2},{5,29},{6,4},{7,31},{8,14},{9,1},{... | collective-permute-start | bytes 786440 | tf_op jit(solution)/shard_map/ppermute | solution.py:45
  164.5 10.9 %collective-permute-start.35 = (bf16[512,512]{1,0:T(8,128)(2,1)S(1)}, bf16[512,512]{1,0:T(8,128)(2,1)S(1)}, u32[]{:S(2)}, u32[]{:S(2)}) collective-permute-start(bf16[512,512]{1,0:T(8,128)(2,1)S(1)} %convolution_convert_fusion), channel_id=1, source_target_pairs={{0,4},{1,17},{2,6},{3,19},{4,0},{5,21},{6,2},{7,23},{8,12},{9,25},... | collective-permute-start | bytes 1572872 | tf_op jit(solution)/shard_map/ppermute | solution.py:45
  166.1 15.4 %collective-permute-start.34 = (bf16[512,512]{1,0:T(8,128)(2,1)S(1)}, bf16[512,512]{1,0:T(8,128)(2,1)S(1)}, u32[]{:S(2)}, u32[]{:S(2)}) collective-permute-start(bf16[512,512]{1,0:T(8,128)(2,1)S(1)} %convolution_convert_fusion.1), channel_id=1, source_target_pairs={{0,6},{1,25},{2,0},{3,27},{4,2},{5,29},{6,4},{7,31},{8,14},{9,1},{... | collective-permute-start | bytes 1572872 | tf_op jit(solution)/shard_map/ppermute | solution.py:45
  167.9 13.6 %collective-permute-start.33 = (bf16[512,512]{1,0:T(8,128)(2,1)S(1)}, bf16[512,512]{1,0:T(8,128)(2,1)S(1)}, u32[]{:S(2)}, u32[]{:S(2)}) collective-permute-start(bf16[512,512]{1,0:T(8,128)(2,1)S(1)} %convolution_convert_fusion.2), channel_id=1, source_target_pairs={{0,2},{1,9},{2,4},{3,11},{4,6},{5,13},{6,0},{7,15},{8,10},{9,17},{... | collective-permute-start | bytes 1572872 | tf_op jit(solution)/shard_map/ppermute | solution.py:45
  182.7 14.1 %all-to-all-start.4 = ((bf16[16,32,512]{2,1,0:T(8,128)(2,1)}), bf16[16,32,512]{2,1,0:T(8,128)(2,1)S(1)}, u32[]{:S(2)}, u32[]{:S(2)}) async-start(bf16[16,32,512]{2,1,0:T(8,128)(2,1)} %bitcast.35), calls=%async_computation.4 | async-start | bytes 1048576 | tf_op jit(solution)/shard_map/all_to_all | solution.py:65
  (25 other events, 234.8 us)
